TPU v7x, 256 devices: a whole 4x4x8 slice. The times are simulated.
256 devices in a mesh: kv: 64 (over z, y, core), tp: 4 (over x).
Axes of the slice: x: 4, y: 4, z: 8, core: 2. Of those that a mesh axis runs over, the one named last changes fastest.
Arguments:
- tokens: bfloat16 [24576, 1024], P('kv', 'tp'), may hold values from -6 to 6
- query_weight: bfloat16 [1024, 512], P(None, 'tp'), may hold values from -0.1875 to 0.1875
- key_weight: bfloat16 [1024, 512], P(None, 'tp'), may hold values from -0.1875 to 0.1875
- value_weight: bfloat16 [1024, 512], P(None, 'tp'), may hold values from -0.1875 to 0.1875
- out_weight: bfloat16 [512, 1024], P('tp'), may hold values from -0.25 to 0.25
- norm_gain: float32 [512], P('tp'), may hold values from 0.1 to 1.9
- chosen_owner: int32 [384, 8], P('kv'), may hold values from 0 to 63, all different within a row; in each aligned block of 6 rows (0 to 5, 6 to 11, ...) at most 1 rows name the same one
- chosen_local: int32 [384, 8], P('kv'), may hold values from 0 to 5
Outputs:
- attended_out: bfloat16 [24576, 1024], P('kv', 'tp')
Inputs may be any that keep to these rules, and one draw needn't show every extreme that they name: `chosen_owner`: each row names 8 different owners; among the 6 rows of one device no owner is named by more than 1 rows, and in some device's rows one owner is named by exactly 1. `chosen_local`: any index of a key block within its owner.
All inputs are finite; a program needn't handle non-finite values.
Results may differ from a plain program's by a relative error of at most 0.015.
Values may be sent and summed in bfloat16 or wider, within the bound.
No kernel may reach another device: no remote copies, remote signals or barrier semaphores. Data moves between devices by JAX's collectives and lax.ppermute only.
A program may use at most 64 MiB of HBM per device.

v0:
```python
import functools

import jax
import jax.numpy as jnp
from jax import lax
from jax.experimental import pallas as pl
from jax.experimental.pallas import tpu as pltpu
from jax.sharding import Mesh
from jax.sharding import PartitionSpec as P

HEADS = 8
HEAD_SIZE = 64
BLOCK = 64
Z, Y, C, X = 8, 4, 2, 4

lowest = -1e30
eps_norm = 1e-06
VMEM = pltpu.VMEM
SMEM = pltpu.SMEM


def vmem(a):
    return pltpu.with_memory_space_constraint(a, VMEM)


def shift(n, s):
    return [(i, (i + s) % n) for i in range(n)]


def full(space=VMEM):
    return pl.BlockSpec(memory_space=space)


def head_turn(rows):
    turned = rows.T
    return jnp.concatenate([turned[:HEAD_SIZE], turned[HEAD_SIZE:]], axis=1)


def head_unturn(rows):
    return jnp.concatenate([rows[:, :HEAD_SIZE], rows[:, HEAD_SIZE:]], axis=0).T


def project_kernel(blocks, at, t0, t1, t2, t3, wq, wk, wv, q_out, kv_out):
    pieces = [ref[...] for ref in (t0, t1, t2, t3)]
    starts = [pl.multiple_of(at[s] * 256, 256) for s in range(4)]

    def summed(weight):
        total = None
        for piece, start in zip(pieces, starts):
            term = jnp.dot(piece, weight[pl.ds(start, 256), :], preferred_element_type=jnp.float32)
            total = term if total is None else total + term
        return total

    half = blocks * BLOCK
    kv_out[:half, :] = summed(wk).astype(jnp.bfloat16)
    values = summed(wv)
    for b in range(blocks):
        turned = head_turn(values[b * 64 : b * 64 + 64])
        kv_out[half + b * 64 : half + b * 64 + 64, :] = turned.astype(jnp.bfloat16)
    queries = summed(wq).astype(jnp.bfloat16).astype(jnp.float32) * (HEAD_SIZE ** (-0.5))
    for b in range(blocks):
        q_out[b * 64 : b * 64 + 64, :] = head_turn(queries[b * 64 : b * 64 + 64]).astype(
            jnp.bfloat16
        )


def project(at, pieces, weights):
    rows = pieces[0].shape[0]
    return pl.pallas_call(
        functools.partial(project_kernel, rows // BLOCK),
        out_shape=(VMEM((rows, 128), jnp.bfloat16), VMEM((2 * rows, 128), jnp.bfloat16)),
        in_specs=[full(SMEM)] + [full()] * 7,
        out_specs=(full(),) * 2,
        name="project",
    )(at, *[vmem(a) for a in (*pieces, *weights)])


def spread_heads(rows, lane):
    none = jnp.zeros_like(rows)
    return jnp.concatenate(
        [jnp.where(lane < HEAD_SIZE, rows, none), jnp.where(lane < HEAD_SIZE, none, rows)], axis=0
    )


def one_pair(q, k, v, lane, mask=None):
    scores = jnp.dot(k, spread_heads(q, lane), preferred_element_type=jnp.float32)
    if mask is not None:
        scores = jnp.where(mask, scores, lowest)
    highest = jnp.max(scores, axis=0, keepdims=True)
    weights = jnp.exp(scores - highest)
    mass = jnp.sum(weights, axis=0, keepdims=True)
    blended = jnp.dot(
        v, spread_heads(weights.astype(jnp.bfloat16), lane), preferred_element_type=jnp.float32
    )
    return highest, mass, blended


def attend_kernel(blocks, owners, first, last, *refs):
    refs = list(refs)
    table = refs.pop(0)
    q = [refs.pop(0) for _ in range(Y)]
    kv = [refs.pop(0) for _ in range(owners)]
    half = blocks * BLOCK
    carry = None if first else [refs.pop(0) for _ in range(3)]
    if last:
        out = [refs.pop(0) for _ in range(Y)]
    top, mass, total = refs
    lane = lax.broadcasted_iota(jnp.int32, (BLOCK, 128), 1)

    if first:
        for g in range(blocks, Y * blocks):
            top[g] = jnp.full((8, 128), lowest, jnp.float32)
            mass[g] = jnp.zeros((8, 128), jnp.float32)
            total[g] = jnp.zeros((BLOCK, 128), jnp.float32)
        spot = lax.broadcasted_iota(jnp.int32, (BLOCK, 128), 0)
        seen = spot <= (lane & (HEAD_SIZE - 1))
        for b in range(blocks):
            here = slice(b * 64, b * 64 + 64)
            after = slice(half + b * 64, half + b * 64 + 64)
            m, l, o = one_pair(q[0][here, :], kv[0][here, :], kv[0][after, :], lane, seen)
            top[b] = jnp.broadcast_to(m, (8, 128))
            mass[b] = jnp.broadcast_to(l, (8, 128))
            total[b] = o
    else:
        for src, dst in zip(carry, (top, mass, total)):
            dst[...] = src[...]

    for owner in range(owners):
        found = []
        for p in range(Y):
            code = table[owner * Y + p]
            row = jnp.maximum(code - 1, 0)
            local = pl.multiple_of((row & 7) * BLOCK, BLOCK)
            row = row >> 3
            m, l, o = one_pair(
                q[p][pl.ds(pl.multiple_of(row * BLOCK, BLOCK), BLOCK), :],
                kv[owner][pl.ds(local, BLOCK), :],
                kv[owner][pl.ds(half + local, BLOCK), :],
                lane,
            )
            found.append((code > 0, p * blocks + row, m, l, o))
        for real, g, m, l, o in found:
            m = jnp.where(real, m, lowest)
            before = top[g]
            now = jnp.maximum(before, m)
            keep = jnp.exp(before - now)
            add = jnp.where(real, jnp.exp(m - now), 0.0)
            top[g] = now
            mass[g] = mass[g] * keep + l * add
            total[g] = total[g] * keep[:1] + o * add[:1]

    if last:
        line = lax.broadcasted_iota(jnp.int32, (8, 128), 0)
        for p in range(Y):
            stats = []
            for b in range(blocks):
                g = p * blocks + b
                out[p][b * 64 : b * 64 + 64, :] = total[g].astype(jnp.bfloat16)
                tile = jnp.zeros((8, 128), jnp.float32)
                for at, value in ((0, top[g]), (3, mass[g])):
                    for i in range(3):
                        part = value.astype(jnp.bfloat16).astype(jnp.float32)
                        tile = jnp.where(line == at + i, part, tile)
                        value = value - part
                stats.append(tile)
            out[p][blocks * 64 :, :] = jnp.concatenate(stats, axis=0).astype(jnp.bfloat16)


def attend(table, q, kv, carry, last):
    rows = q[0].shape[0]
    blocks = rows // BLOCK
    groups = Y * blocks
    state = [
        jax.ShapeDtypeStruct((groups, 8, 128), jnp.float32),
        jax.ShapeDtypeStruct((groups, 8, 128), jnp.float32),
        jax.ShapeDtypeStruct((groups, BLOCK, 128), jnp.float32),
    ]
    if last:
        outs = [jax.ShapeDtypeStruct((rows + 8 * blocks, 128), jnp.bfloat16)] * Y
        scratch = [VMEM(s.shape, s.dtype) for s in state]
    else:
        outs, scratch = state, []
    outs = [VMEM(s.shape, s.dtype) for s in outs]
    args = [table] + [vmem(a) for a in (*q, *kv, *(carry or ()))]
    return pl.pallas_call(
        functools.partial(attend_kernel, blocks, len(kv), carry is None, last),
        out_shape=tuple(outs),
        in_specs=[full(SMEM)] + [full()] * (len(args) - 1),
        out_specs=(full(),) * len(outs),
        scratch_shapes=scratch,
        name="attend_late" if last else "attend_early",
    )(*args)


def merge_kernel(blocks, *refs):
    parts, out = refs[:-1], refs[-1]
    stats = [part[blocks * 64 :, :].astype(jnp.float32) for part in parts]
    for b in range(blocks):
        tops, masses = [], []
        for s in stats:
            t = s[b * 8 : b * 8 + 8]
            tops.append(t[0:1] + t[1:2] + t[2:3])
            masses.append(t[3:4] + t[4:5] + t[5:6])
        highest = functools.reduce(jnp.maximum, tops)
        mass, blended = 0.0, 0.0
        for part, m, l in zip(parts, tops, masses):
            scale = jnp.exp(m - highest)
            mass = mass + l * scale
            blended = blended + part[b * 64 : b * 64 + 64, :].astype(jnp.float32) * scale
        out[b * 64 : b * 64 + 64, :] = head_unturn(blended / mass).astype(jnp.bfloat16)


def merge(parts, blocks):
    return pl.pallas_call(
        functools.partial(merge_kernel, blocks),
        out_shape=VMEM((blocks * BLOCK, 128), jnp.bfloat16),
        in_specs=[full()] * len(parts),
        out_specs=full(),
        name="merge",
    )(*[vmem(a) for a in parts])


def finish_kernel(a0, a1, a2, a3, w0, w1, w2, w3, out):
    squares, summed = None, None
    for a, w in ((a0, w0), (a1, w1), (a2, w2), (a3, w3)):
        rows = a[...]
        wide = rows.astype(jnp.float32)
        term = jnp.dot(rows, w[...], preferred_element_type=jnp.float32)
        squares = wide * wide if squares is None else squares + wide * wide
        summed = term if summed is None else summed + term
    mean_sq = jnp.sum(squares, axis=1, keepdims=True) / (HEADS * HEAD_SIZE)
    out[...] = (summed * lax.rsqrt(mean_sq + eps_norm)).astype(jnp.bfloat16)


def finish(pieces, weights):
    rows, cols = pieces[0].shape[0], weights[0].shape[1]
    return pl.pallas_call(
        finish_kernel,
        out_shape=jax.ShapeDtypeStruct((rows, cols), jnp.bfloat16),
        in_specs=[full()] * 8,
        out_specs=full(),
        name="finish",
    )(*[vmem(a) for a in (*pieces, *weights)])


def on_device(
    tokens,
    query_weight,
    key_weight,
    value_weight,
    out_weight,
    norm_gain,
    chosen_owner,
    chosen_local,
):
    rows = tokens.shape[0]
    blocks = rows // BLOCK
    x, z, y, c = (lax.axis_index(name) for name in ("x", "z", "y", "c"))

    pieces = [tokens] + [lax.ppermute(tokens, "x", shift(X, s)) for s in (1, 2, 3)]
    at = jnp.stack([(x - s) % X for s in range(X)]).astype(jnp.int32)

    picked = chosen_owner * 8 + chosen_local
    picks = [picked] + [lax.ppermute(picked, "y", shift(Y, s)) for s in (1, 2, 3)]

    width = out_weight.shape[1] // X
    gained = []
    for s in range(X):
        columns = lax.dynamic_slice_in_dim(out_weight, ((x + s) % X) * width, width, 1)
        gained.append((columns.astype(jnp.float32) * norm_gain[:, None]).astype(jnp.bfloat16))
    weights = [gained[0]] + [lax.ppermute(gained[s], "x", shift(X, s)) for s in (1, 2, 3)]

    q, kv = project(at, pieces, (query_weight, key_weight, value_weight))

    places = [(i, j) for i in range(Z) for j in range(C)]

    def onward(k):
        return [(C * i + j, C * ((i + (k if j == 0 else -k)) % Z) + j) for i, j in places]

    def swap(a):
        return lax.ppermute(a, "c", [(0, 1), (1, 0)])

    same, cross = [kv], [swap(kv)]
    held = [(0, 0, kv), (0, 1, cross[0])]
    for step in (1, 2, 3):
        same.append(lax.ppermute(same[-1], ("z", "c"), onward(1)))
        cross.append(lax.ppermute(cross[-1], ("z", "c"), onward(1)))
        held += [(step, 0, same[-1]), (step, 1, cross[-1])]
        held += [(-step, 1, swap(same[-1])), (-step, 0, swap(cross[-1]))]
    far = lax.ppermute(same[2], ("z", "c"), onward(2))
    held += [(4, 0, far), (4, 1, swap(far))]

    queries = [q] + [lax.ppermute(q, "y", shift(Y, s)) for s in (1, 2, 3)]

    toward = 2 * c - 1
    column = jnp.stack(
        [((z + toward * d) % Z) * (Y * C) + y * C + (c ^ cc) for d, cc, _ in held]
    ).astype(jnp.int32)
    picks = jnp.stack(picks)
    code = 1 + 8 * jnp.arange(blocks, dtype=jnp.int32)[None, :, None] + (picks & 7)
    hit = (picks >> 3)[None] == column[:, None, None, None]
    table = jnp.sum(jnp.where(hit, code[None], 0), axis=(2, 3)).reshape(-1)

    early = 10
    arrays = [a for _, _, a in held]
    carry = attend(table[: early * Y], queries, arrays[:early], None, False)
    parts = attend(table[early * Y :], queries, arrays[early:], carry, True)

    back = [parts[0]] + [lax.ppermute(parts[s], "y", shift(Y, -s)) for s in (1, 2, 3)]
    attended = merge(back, blocks)
    spread = [attended] + [lax.ppermute(attended, "x", shift(X, s)) for s in (1, 2, 3)]
    return finish(spread, weights)


def solution(mesh):
    fine = Mesh(mesh.devices.reshape(Z, Y, C, X), ("z", "y", "c", "x"))
    kv = ("z", "y", "c")
    return jax.shard_map(
        on_device,
        mesh=fine,
        in_specs=(
            P(kv, "x"),
            P(None, "x"),
            P(None, "x"),
            P(None, "x"),
            P("x", None),
            P("x"),
            P(kv, None),
            P(kv, None),
        ),
        out_specs=P(kv, "x"),
        check_vma=False,
    )
```

profile of v0, /device:TPU:1, one launch (start us, length us, event | category | flops | bytes accessed | tf_op | source)
XLA Modules:
  0.0 96.9 jit_solution(4579406939051862149)
XLA Ops:
  0.0 2.0 %collective-permute-start.3 = (bf16[384,256]{1,0:T(8,128)(2,1)}, bf16[384,256]{1,0:T(8,128)(2,1)S(1)}, u32[]{:S(2)}, u32[]{:S(2)}) collective-permute-start(bf16[384,256]{1,0:T(8,128)(2,1)} %t0.1), channel_id=1, source_target_pairs={{0,1},{1,2},{2,3},{3,0},{4,5},{5,6},{6,7},{7,4},{8,9},{9,10},{10,1... | collective-permute-start | bytes 589832 | tf_op jit(solution)/shard_map/ppermute | solution.py:260
  2.0 2.5 %collective-permute-start.4 = (bf16[384,256]{1,0:T(8,128)(2,1)}, bf16[384,256]{1,0:T(8,128)(2,1)S(1)}, u32[]{:S(2)}, u32[]{:S(2)}) collective-permute-start(bf16[384,256]{1,0:T(8,128)(2,1)} %t0.1), channel_id=1, source_target_pairs={{0,2},{1,3},{2,0},{3,1},{4,6},{5,7},{6,4},{7,5},{8,10},{9,11},{10,... | collective-permute-start | bytes 589832 | tf_op jit(solution)/shard_map/ppermute | solution.py:260
  6.6 6.7 %collective-permute-done.4.t2 = bf16[384,256]{1,0:T(8,128)(2,1)S(1)} collective-permute-done((bf16[384,256]{1,0:T(8,128)(2,1)}, bf16[384,256]{1,0:T(8,128)(2,1)S(1)}, u32[]{:S(2)}, u32[]{:S(2)}) %collective-permute-start.4) | collective-permute-done | bytes 196640 | tf_op jit(solution)/shard_map/ppermute | solution.py:260
  17.0 2.0 %project.1 = (bf16[384,128]{1,0:T(8,128)(2,1)S(1)}, bf16[768,128]{1,0:T(8,128)(2,1)S(1)}) custom-call(s32[4]{0:T(128)} %pad_add_fusion.1.at, bf16[384,256]{1,0:T(8,128)(2,1)S(1)} %copy-done.9, bf16[384,256]{1,0:T(8,128)(2,1)S(1)} %collective-permute-done.3.t1, bf16[384,256]{1,0:T(8,128)(2,1)S(1)} %collective-permute-done.4.t2, ...), custom_call_target="tpu_custom_call" | custom-call | tf_op jit(solution)/shard_map/project/pallas_call | solution.py:69
  19.0 1.6 %collective-permute-start.12 = (bf16[768,128]{1,0:T(8,128)(2,1)S(1)}, bf16[768,128]{1,0:T(8,128)(2,1)S(1)}, u32[]{:S(2)}, u32[]{:S(2)}) collective-permute-start(bf16[768,128]{1,0:T(8,128)(2,1)S(1)} %get-tuple-element.15.refs_5_), channel_id=1, source_target_pairs={{0,4},{4,0},{1,5},{5,1},{2,6},{6,2},{3,7},{7,3},{8,12},{12,8},{9,1... | collective-permute-start | bytes 589832 | tf_op jit(solution)/shard_map/ppermute | solution.py:281
  20.6 5.6 %collective-permute-start.9 = (bf16[768,128]{1,0:T(8,128)(2,1)S(1)}, bf16[768,128]{1,0:T(8,128)(2,1)S(1)}, u32[]{:S(2)}, u32[]{:S(2)}) collective-permute-start(bf16[768,128]{1,0:T(8,128)(2,1)S(1)} %get-tuple-element.15.refs_5_), channel_id=1, source_target_pairs={{0,32},{4,228},{32,64},{36,4},{64,96},{68,36},{96,128},{100,68},{1... | collective-permute-start | bytes 589832 | tf_op jit(solution)/shard_map/ppermute | solution.py:286
  27.3 1.5 %collective-permute-done.9.refs_7_ = bf16[768,128]{1,0:T(8,128)(2,1)S(1)} collective-permute-done((bf16[768,128]{1,0:T(8,128)(2,1)S(1)}, bf16[768,128]{1,0:T(8,128)(2,1)S(1)}, u32[]{:S(2)}, u32[]{:S(2)}) %collective-permute-start.9) | collective-permute-done | bytes 196640 | tf_op jit(solution)/shard_map/ppermute | solution.py:286
  28.8 3.1 %collective-permute-start.10 = (bf16[768,128]{1,0:T(8,128)(2,1)S(1)}, bf16[768,128]{1,0:T(8,128)(2,1)S(1)}, u32[]{:S(2)}, u32[]{:S(2)}) collective-permute-start(bf16[768,128]{1,0:T(8,128)(2,1)S(1)} %collective-permute-done.9.refs_7_), channel_id=1, source_target_pairs={{0,32},{4,228},{32,64},{36,4},{64,96},{68,36},{96,128},{100,68},{1... | collective-permute-start | bytes 589832 | tf_op jit(solution)/shard_map/ppermute | solution.py:286
  31.9 2.1 %collective-permute-start.14 = (bf16[768,128]{1,0:T(8,128)(2,1)S(1)}, bf16[768,128]{1,0:T(8,128)(2,1)S(1)}, u32[]{:S(2)}, u32[]{:S(2)}) collective-permute-start(bf16[768,128]{1,0:T(8,128)(2,1)S(1)} %collective-permute-done.13.refs_8_), channel_id=1, source_target_pairs={{0,32},{4,228},{32,64},{36,4},{64,96},{68,36},{96,128},{100,68},{1... | collective-permute-start | bytes 589832 | tf_op jit(solution)/shard_map/ppermute | solution.py:287
  35.4 2.6 %collective-permute-start.1 = (s32[6,8]{1,0:T(8,128)S(1)}, s32[6,8]{1,0:T(8,128)S(1)}, u32[]{:S(2)}, u32[]{:S(2)}) collective-permute-start(s32[6,8]{1,0:T(8,128)S(1)} %multiply_add_fusion), channel_id=1, source_target_pairs={{0,16},{8,24},{16,0},{24,8},{1,17},{9,25},{17,1},{25,9},{2,18},{10... | collective-permute-start | bytes 584 | tf_op jit(solution)/shard_map/ppermute | solution.py:264
  39.5 2.6 %collective-permute-start.7 = (bf16[384,128]{1,0:T(8,128)(2,1)S(1)}, bf16[384,128]{1,0:T(8,128)(2,1)S(1)}, u32[]{:S(2)}, u32[]{:S(2)}) collective-permute-start(bf16[384,128]{1,0:T(8,128)(2,1)S(1)} %get-tuple-element.14.refs_1_), channel_id=1, source_target_pairs={{0,16},{8,24},{16,0},{24,8},{1,17},{9,25},{17,1},{25,9},{2,18},{10... | collective-permute-start | bytes 294920 | tf_op jit(solution)/shard_map/ppermute | solution.py:293
  43.1 3.5 %collective-permute-done.6.refs_2_ = bf16[384,128]{1,0:T(8,128)(2,1)S(1)} collective-permute-done((bf16[384,128]{1,0:T(8,128)(2,1)S(1)}, bf16[384,128]{1,0:T(8,128)(2,1)S(1)}, u32[]{:S(2)}, u32[]{:S(2)}) %collective-permute-start.6) | collective-permute-done | bytes 98336 | tf_op jit(solution)/shard_map/ppermute | solution.py:293
  50.2 2.3 %collective-permute-start.22 = (bf16[768,128]{1,0:T(8,128)(2,1)S(1)}, bf16[768,128]{1,0:T(8,128)(2,1)S(1)}, u32[]{:S(2)}, u32[]{:S(2)}) collective-permute-start(bf16[768,128]{1,0:T(8,128)(2,1)S(1)} %collective-permute-done.10.refs_11_), channel_id=1, source_target_pairs={{0,4},{4,0},{1,5},{5,1},{2,6},{6,2},{3,7},{7,3},{8,12},{12,8},{9,1... | collective-permute-start | bytes 589832 | tf_op jit(solution)/shard_map/ppermute | solution.py:281
  52.7 3.7 %collective-permute-start.16 = (bf16[768,128]{1,0:T(8,128)(2,1)S(1)}, bf16[768,128]{1,0:T(8,128)(2,1)}, u32[]{:S(2)}, u32[]{:S(2)}) collective-permute-start(bf16[768,128]{1,0:T(8,128)(2,1)S(1)} %collective-permute-done.11.refs_5_), channel_id=1, source_target_pairs={{0,4},{4,0},{1,5},{5,1},{2,6},{6,2},{3,7},{7,3},{8,12},{12,8},{9,1... | collective-permute-start | bytes 589832 | tf_op jit(solution)/shard_map/ppermute | solution.py:281
  56.4 2.0 %collective-permute-done.15.refs_6_ = bf16[768,128]{1,0:T(8,128)(2,1)} collective-permute-done((bf16[768,128]{1,0:T(8,128)(2,1)S(1)}, bf16[768,128]{1,0:T(8,128)(2,1)}, u32[]{:S(2)}, u32[]{:S(2)}) %collective-permute-start.15) | collective-permute-done | bytes 196640 | tf_op jit(solution)/shard_map/ppermute | solution.py:287
  58.4 2.3 %collective-permute-start.17 = (bf16[768,128]{1,0:T(8,128)(2,1)}, bf16[768,128]{1,0:T(8,128)(2,1)}, u32[]{:S(2)}, u32[]{:S(2)}) collective-permute-start(bf16[768,128]{1,0:T(8,128)(2,1)} %collective-permute-done.15.refs_6_), channel_id=1, source_target_pairs={{0,4},{4,0},{1,5},{5,1},{2,6},{6,2},{3,7},{7,3},{8,12},{12,8},{9,1... | collective-permute-start | bytes 589832 | tf_op jit(solution)/shard_map/ppermute | solution.py:281
  64.3 1.8 %attend_early.1 = (f32[24,8,128]{2,1,0:T(8,128)S(1)}, f32[24,8,128]{2,1,0:T(8,128)S(1)}, f32[24,64,128]{2,1,0:T(8,128)S(1)}) custom-call(s32[40]{0:T(128)} %slice.15.refs_0_, bf16[384,128]{1,0:T(8,128)(2,1)S(1)} %get-tuple-element.14.refs_1_, bf16[384,128]{1,0:T(8,128)(2,1)S(1)} %collective-permute-done.6.refs_2_, ...), custom_call_target="tpu_custom_call" | custom-call | tf_op jit(solution)/shard_map/attend_early/pallas_call | solution.py:185
  72.1 2.1 %attend_late.1 = (bf16[432,128]{1,0:T(8,128)(2,1)S(1)}, bf16[432,128]{1,0:T(8,128)(2,1)S(1)}, bf16[432,128]{1,0:T(8,128)(2,1)S(1)}, bf16[432,128]{1,0:T(8,128)(2,1)S(1)}) custom-call(s32[24]{0:T(128)} %slice.13.refs_0_, bf16[384,128]{1,0:T(8,128)(2,1)S(1)} %get-tuple-element.14.refs_1_, bf16[384,128]{1,0:T(8,128)(2,1)S(1)} %collective-permute-done.6.refs_2_, ...), custom_call_target="tpu_custom_call" | custom-call | tf_op jit(solution)/shard_map/attend_late/pallas_call | solution.py:185
  79.0 2.7 %collective-permute-done.25.refs_2_ = bf16[432,128]{1,0:T(8,128)(2,1)S(1)} collective-permute-done((bf16[432,128]{1,0:T(8,128)(2,1)S(1)}, bf16[432,128]{1,0:T(8,128)(2,1)S(1)}, u32[]{:S(2)}, u32[]{:S(2)}) %collective-permute-start.25) | collective-permute-done | bytes 110624 | tf_op jit(solution)/shard_map/ppermute | solution.py:309
  81.7 3.0 %collective-permute-done.26.refs_3_ = bf16[432,128]{1,0:T(8,128)(2,1)S(1)} collective-permute-done((bf16[432,128]{1,0:T(8,128)(2,1)S(1)}, bf16[432,128]{1,0:T(8,128)(2,1)S(1)}, u32[]{:S(2)}, u32[]{:S(2)}) %collective-permute-start.26) | collective-permute-done | bytes 110624 | tf_op jit(solution)/shard_map/ppermute | solution.py:309
  86.1 2.1 %collective-permute-start.28 = (bf16[384,128]{1,0:T(8,128)(2,1)S(1)}, bf16[384,128]{1,0:T(8,128)(2,1)S(1)}, u32[]{:S(2)}, u32[]{:S(2)}) collective-permute-start(bf16[384,128]{1,0:T(8,128)(2,1)S(1)} %merge.1.a0), channel_id=1, source_target_pairs={{0,2},{1,3},{2,0},{3,1},{4,6},{5,7},{6,4},{7,5},{8,10},{9,11},{10,... | collective-permute-start | bytes 294920 | tf_op jit(solution)/shard_map/ppermute | solution.py:311
  90.1 2.0 %collective-permute-start.32 = (bf16[128,256]{1,0:T(8,128)(2,1)S(1)}, bf16[128,256]{1,0:T(8,128)(2,1)S(1)}, u32[]{:S(2)}, u32[]{:S(2)}) collective-permute-start(bf16[128,256]{1,0:T(8,128)(2,1)S(1)} %get-tuple-element.23), channel_id=1, source_target_pairs={{0,3},{1,0},{2,1},{3,2},{4,7},{5,4},{6,5},{7,6},{8,11},{9,8},{10,9... | collective-permute-start | bytes 196616 | tf_op jit(solution)/shard_map/ppermute | solution.py:271
  92.1 2.0 %collective-permute-done.31.w2 = bf16[128,256]{1,0:T(8,128)(2,1)S(1)} collective-permute-done((bf16[128,256]{1,0:T(8,128)(2,1)S(1)}, bf16[128,256]{1,0:T(8,128)(2,1)S(1)}, u32[]{:S(2)}, u32[]{:S(2)}) %collective-permute-start.31) | collective-permute-done | bytes 65568 | tf_op jit(solution)/shard_map/ppermute | solution.py:271
  94.1 1.7 %collective-permute-done.32.w3 = bf16[128,256]{1,0:T(8,128)(2,1)S(1)} collective-permute-done((bf16[128,256]{1,0:T(8,128)(2,1)S(1)}, bf16[128,256]{1,0:T(8,128)(2,1)S(1)}, u32[]{:S(2)}, u32[]{:S(2)}) %collective-permute-start.32) | collective-permute-done | bytes 65568 | tf_op jit(solution)/shard_map/ppermute | solution.py:271
  (99 shorter events, 33.4 us)
Async XLA Ops:
  0.0 6.6 %collective-permute-start.3 = (bf16[384,256]{1,0:T(8,128)(2,1)}, bf16[384,256]{1,0:T(8,128)(2,1)S(1)}, u32[]{:S(2)}, u32[]{:S(2)}) collective-permute-start(bf16[384,256]{1,0:T(8,128)(2,1)} %t0.1), channel_id=1, source_target_pairs={{0,1},{1,2},{2,3},{3,0},{4,5},{5,6},{6,7},{7,4},{8,9},{9,10},{10,1... | collective-permute-start | bytes 589832 | tf_op jit(solution)/shard_map/ppermute | solution.py:260
  2.0 11.2 %collective-permute-start.4 = (bf16[384,256]{1,0:T(8,128)(2,1)}, bf16[384,256]{1,0:T(8,128)(2,1)S(1)}, u32[]{:S(2)}, u32[]{:S(2)}) collective-permute-start(bf16[384,256]{1,0:T(8,128)(2,1)} %t0.1), channel_id=1, source_target_pairs={{0,2},{1,3},{2,0},{3,1},{4,6},{5,7},{6,4},{7,5},{8,10},{9,11},{10,... | collective-permute-start | bytes 589832 | tf_op jit(solution)/shard_map/ppermute | solution.py:260
  4.5 8.7 %collective-permute-start.5 = (bf16[384,256]{1,0:T(8,128)(2,1)}, bf16[384,256]{1,0:T(8,128)(2,1)S(1)}, u32[]{:S(2)}, u32[]{:S(2)}) collective-permute-start(bf16[384,256]{1,0:T(8,128)(2,1)} %t0.1), channel_id=1, source_target_pairs={{0,3},{1,0},{2,1},{3,2},{4,7},{5,4},{6,5},{7,6},{8,11},{9,8},{10,9... | collective-permute-start | bytes 589832 | tf_op jit(solution)/shard_map/ppermute | solution.py:260
  19.0 7.2 %collective-permute-start.12 = (bf16[768,128]{1,0:T(8,128)(2,1)S(1)}, bf16[768,128]{1,0:T(8,128)(2,1)S(1)}, u32[]{:S(2)}, u32[]{:S(2)}) collective-permute-start(bf16[768,128]{1,0:T(8,128)(2,1)S(1)} %get-tuple-element.15.refs_5_), channel_id=1, source_target_pairs={{0,4},{4,0},{1,5},{5,1},{2,6},{6,2},{3,7},{7,3},{8,12},{12,8},{9,1... | collective-permute-start | bytes 589832 | tf_op jit(solution)/shard_map/ppermute | solution.py:281
  20.6 8.2 %collective-permute-start.9 = (bf16[768,128]{1,0:T(8,128)(2,1)S(1)}, bf16[768,128]{1,0:T(8,128)(2,1)S(1)}, u32[]{:S(2)}, u32[]{:S(2)}) collective-permute-start(bf16[768,128]{1,0:T(8,128)(2,1)S(1)} %get-tuple-element.15.refs_5_), channel_id=1, source_target_pairs={{0,32},{4,228},{32,64},{36,4},{64,96},{68,36},{96,128},{100,68},{1... | collective-permute-start | bytes 589832 | tf_op jit(solution)/shard_map/ppermute | solution.py:286
  28.8 18.3 %collective-permute-start.10 = (bf16[768,128]{1,0:T(8,128)(2,1)S(1)}, bf16[768,128]{1,0:T(8,128)(2,1)S(1)}, u32[]{:S(2)}, u32[]{:S(2)}) collective-permute-start(bf16[768,128]{1,0:T(8,128)(2,1)S(1)} %collective-permute-done.9.refs_7_), channel_id=1, source_target_pairs={{0,32},{4,228},{32,64},{36,4},{64,96},{68,36},{96,128},{100,68},{1... | collective-permute-start | bytes 589832 | tf_op jit(solution)/shard_map/ppermute | solution.py:286
  31.9 17.2 %collective-permute-start.14 = (bf16[768,128]{1,0:T(8,128)(2,1)S(1)}, bf16[768,128]{1,0:T(8,128)(2,1)S(1)}, u32[]{:S(2)}, u32[]{:S(2)}) collective-permute-start(bf16[768,128]{1,0:T(8,128)(2,1)S(1)} %collective-permute-done.13.refs_8_), channel_id=1, source_target_pairs={{0,32},{4,228},{32,64},{36,4},{64,96},{68,36},{96,128},{100,68},{1... | collective-permute-start | bytes 589832 | tf_op jit(solution)/shard_map/ppermute | solution.py:287
  39.1 7.4 %collective-permute-start.6 = (bf16[384,128]{1,0:T(8,128)(2,1)S(1)}, bf16[384,128]{1,0:T(8,128)(2,1)S(1)}, u32[]{:S(2)}, u32[]{:S(2)}) collective-permute-start(bf16[384,128]{1,0:T(8,128)(2,1)S(1)} %get-tuple-element.14.refs_1_), channel_id=1, source_target_pairs={{0,8},{8,16},{16,24},{24,0},{1,9},{9,17},{17,25},{25,1},{2,10},{10... | collective-permute-start | bytes 294920 | tf_op jit(solution)/shard_map/ppermute | solution.py:293
  39.5 7.3 %collective-permute-start.7 = (bf16[384,128]{1,0:T(8,128)(2,1)S(1)}, bf16[384,128]{1,0:T(8,128)(2,1)S(1)}, u32[]{:S(2)}, u32[]{:S(2)}) collective-permute-start(bf16[384,128]{1,0:T(8,128)(2,1)S(1)} %get-tuple-element.14.refs_1_), channel_id=1, source_target_pairs={{0,16},{8,24},{16,0},{24,8},{1,17},{9,25},{17,1},{25,9},{2,18},{10... | collective-permute-start | bytes 294920 | tf_op jit(solution)/shard_map/ppermute | solution.py:293
  42.1 6.1 %collective-permute-start.8 = (bf16[384,128]{1,0:T(8,128)(2,1)S(1)}, bf16[384,128]{1,0:T(8,128)(2,1)S(1)}, u32[]{:S(2)}, u32[]{:S(2)}) collective-permute-start(bf16[384,128]{1,0:T(8,128)(2,1)S(1)} %get-tuple-element.14.refs_1_), channel_id=1, source_target_pairs={{0,24},{8,0},{16,8},{24,16},{1,25},{9,1},{17,9},{25,17},{2,26},{10... | collective-permute-start | bytes 294920 | tf_op jit(solution)/shard_map/ppermute | solution.py:293
  48.2 8.2 %collective-permute-start.18 = (bf16[768,128]{1,0:T(8,128)(2,1)S(1)}, bf16[768,128]{1,0:T(8,128)(2,1)}, u32[]{:S(2)}, u32[]{:S(2)}) collective-permute-start(bf16[768,128]{1,0:T(8,128)(2,1)S(1)} %collective-permute-done.10.refs_11_), channel_id=1, source_target_pairs={{0,64},{4,196},{32,96},{36,228},{64,128},{68,4},{96,160},{100,36},... | collective-permute-start | bytes 589832 | tf_op jit(solution)/shard_map/ppermute | solution.py:290
  49.2 9.2 %collective-permute-start.15 = (bf16[768,128]{1,0:T(8,128)(2,1)S(1)}, bf16[768,128]{1,0:T(8,128)(2,1)}, u32[]{:S(2)}, u32[]{:S(2)}) collective-permute-start(bf16[768,128]{1,0:T(8,128)(2,1)S(1)} %collective-permute-done.14.refs_12_), channel_id=1, source_target_pairs={{0,32},{4,228},{32,64},{36,4},{64,96},{68,36},{96,128},{100,68},{1... | collective-permute-start | bytes 589832 | tf_op jit(solution)/shard_map/ppermute | solution.py:287
  50.2 12.2 %collective-permute-start.22 = (bf16[768,128]{1,0:T(8,128)(2,1)S(1)}, bf16[768,128]{1,0:T(8,128)(2,1)S(1)}, u32[]{:S(2)}, u32[]{:S(2)}) collective-permute-start(bf16[768,128]{1,0:T(8,128)(2,1)S(1)} %collective-permute-done.10.refs_11_), channel_id=1, source_target_pairs={{0,4},{4,0},{1,5},{5,1},{2,6},{6,2},{3,7},{7,3},{8,12},{12,8},{9,1... | collective-permute-start | bytes 589832 | tf_op jit(solution)/shard_map/ppermute | solution.py:281
  52.6 9.9 %collective-permute-start.23 = (bf16[768,128]{1,0:T(8,128)(2,1)S(1)}, bf16[768,128]{1,0:T(8,128)(2,1)S(1)}, u32[]{:S(2)}, u32[]{:S(2)}) collective-permute-start(bf16[768,128]{1,0:T(8,128)(2,1)S(1)} %collective-permute-done.14.refs_12_), channel_id=1, source_target_pairs={{0,4},{4,0},{1,5},{5,1},{2,6},{6,2},{3,7},{7,3},{8,12},{12,8},{9,1... | collective-permute-start | bytes 589832 | tf_op jit(solution)/shard_map/ppermute | solution.py:281
  52.7 15.6 %collective-permute-start.16 = (bf16[768,128]{1,0:T(8,128)(2,1)S(1)}, bf16[768,128]{1,0:T(8,128)(2,1)}, u32[]{:S(2)}, u32[]{:S(2)}) collective-permute-start(bf16[768,128]{1,0:T(8,128)(2,1)S(1)} %collective-permute-done.11.refs_5_), channel_id=1, source_target_pairs={{0,4},{4,0},{1,5},{5,1},{2,6},{6,2},{3,7},{7,3},{8,12},{12,8},{9,1... | collective-permute-start | bytes 589832 | tf_op jit(solution)/shard_map/ppermute | solution.py:281
  56.3 11.9 %collective-permute-start.19 = (bf16[768,128]{1,0:T(8,128)(2,1)}, bf16[768,128]{1,0:T(8,128)(2,1)}, u32[]{:S(2)}, u32[]{:S(2)}) collective-permute-start(bf16[768,128]{1,0:T(8,128)(2,1)} %collective-permute-done.18.refs_9_), channel_id=1, source_target_pairs={{0,4},{4,0},{1,5},{5,1},{2,6},{6,2},{3,7},{7,3},{8,12},{12,8},{9,1... | collective-permute-start | bytes 589832 | tf_op jit(solution)/shard_map/ppermute | solution.py:281
  58.4 9.9 %collective-permute-start.17 = (bf16[768,128]{1,0:T(8,128)(2,1)}, bf16[768,128]{1,0:T(8,128)(2,1)}, u32[]{:S(2)}, u32[]{:S(2)}) collective-permute-start(bf16[768,128]{1,0:T(8,128)(2,1)} %collective-permute-done.15.refs_6_), channel_id=1, source_target_pairs={{0,4},{4,0},{1,5},{5,1},{2,6},{6,2},{3,7},{7,3},{8,12},{12,8},{9,1... | collective-permute-start | bytes 589832 | tf_op jit(solution)/shard_map/ppermute | solution.py:281
  75.8 5.8 %collective-permute-start.25 = (bf16[432,128]{1,0:T(8,128)(2,1)S(1)}, bf16[432,128]{1,0:T(8,128)(2,1)S(1)}, u32[]{:S(2)}, u32[]{:S(2)}) collective-permute-start(bf16[432,128]{1,0:T(8,128)(2,1)S(1)} %get-tuple-element.21), channel_id=1, source_target_pairs={{0,16},{8,24},{16,0},{24,8},{1,17},{9,25},{17,1},{25,9},{2,18},{10... | collective-permute-start | bytes 331784 | tf_op jit(solution)/shard_map/ppermute | solution.py:309
  77.0 7.6 %collective-permute-start.26 = (bf16[432,128]{1,0:T(8,128)(2,1)S(1)}, bf16[432,128]{1,0:T(8,128)(2,1)S(1)}, u32[]{:S(2)}, u32[]{:S(2)}) collective-permute-start(bf16[432,128]{1,0:T(8,128)(2,1)S(1)} %get-tuple-element.22), channel_id=1, source_target_pairs={{0,8},{8,16},{16,24},{24,0},{1,9},{9,17},{17,25},{25,1},{2,10},{10... | collective-permute-start | bytes 331784 | tf_op jit(solution)/shard_map/ppermute | solution.py:309
  77.3 12.8 %collective-permute-start.30 = (bf16[128,256]{1,0:T(8,128)(2,1)S(1)}, bf16[128,256]{1,0:T(8,128)(2,1)S(1)}, u32[]{:S(2)}, u32[]{:S(2)}) collective-permute-start(bf16[128,256]{1,0:T(8,128)(2,1)S(1)} %get-tuple-element.24), channel_id=1, source_target_pairs={{0,1},{1,2},{2,3},{3,0},{4,5},{5,6},{6,7},{7,4},{8,9},{9,10},{10,1... | collective-permute-start | bytes 196616 | tf_op jit(solution)/shard_map/ppermute | solution.py:271
  85.0 10.9 %collective-permute-start.27 = (bf16[384,128]{1,0:T(8,128)(2,1)S(1)}, bf16[384,128]{1,0:T(8,128)(2,1)S(1)}, u32[]{:S(2)}, u32[]{:S(2)}) collective-permute-start(bf16[384,128]{1,0:T(8,128)(2,1)S(1)} %merge.1.a0), channel_id=1, source_target_pairs={{0,1},{1,2},{2,3},{3,0},{4,5},{5,6},{6,7},{7,4},{8,9},{9,10},{10,1... | collective-permute-start | bytes 294920 | tf_op jit(solution)/shard_map/ppermute | solution.py:311
  86.1 9.7 %collective-permute-start.28 = (bf16[384,128]{1,0:T(8,128)(2,1)S(1)}, bf16[384,128]{1,0:T(8,128)(2,1)S(1)}, u32[]{:S(2)}, u32[]{:S(2)}) collective-permute-start(bf16[384,128]{1,0:T(8,128)(2,1)S(1)} %merge.1.a0), channel_id=1, source_target_pairs={{0,2},{1,3},{2,0},{3,1},{4,6},{5,7},{6,4},{7,5},{8,10},{9,11},{10,... | collective-permute-start | bytes 294920 | tf_op jit(solution)/shard_map/ppermute | solution.py:311
  88.2 7.6 %collective-permute-start.29 = (bf16[384,128]{1,0:T(8,128)(2,1)S(1)}, bf16[384,128]{1,0:T(8,128)(2,1)S(1)}, u32[]{:S(2)}, u32[]{:S(2)}) collective-permute-start(bf16[384,128]{1,0:T(8,128)(2,1)S(1)} %merge.1.a0), channel_id=1, source_target_pairs={{0,3},{1,0},{2,1},{3,2},{4,7},{5,4},{6,5},{7,6},{8,11},{9,8},{10,9... | collective-permute-start | bytes 294920 | tf_op jit(solution)/shard_map/ppermute | solution.py:311
  90.1 5.7 %collective-permute-start.32 = (bf16[128,256]{1,0:T(8,128)(2,1)S(1)}, bf16[128,256]{1,0:T(8,128)(2,1)S(1)}, u32[]{:S(2)}, u32[]{:S(2)}) collective-permute-start(bf16[128,256]{1,0:T(8,128)(2,1)S(1)} %get-tuple-element.23), channel_id=1, source_target_pairs={{0,3},{1,0},{2,1},{3,2},{4,7},{5,4},{6,5},{7,6},{8,11},{9,8},{10,9... | collective-permute-start | bytes 196616 | tf_op jit(solution)/shard_map/ppermute | solution.py:271
  (29 other events, 143.4 us)
where the time goes:
time: 97.3 us; the launch traced here: 96.9 us
  starting transfers between devices  51.3 us (53%)
  waiting for transfers between devices  23.9 us (25%)
  local copies, waits for them, and re-layouts  13.3 us (14%)
  Pallas kernels  7.25 us (7%)
    unnamed x40, local copies, waits for them, and re-layouts  11.7 us
    ppermute x8, starting transfers between devices, swap(): return lax.ppermute(a, 'c', [(0, 1), (1, 0)])  10.6 us
    ppermute x3, starting transfers between devices, on_device(): same.append(lax.ppermute(same[-1], ('z', 'c'), onward(1)))  9.8 us
    ppermute x3, waiting for transfers between devices, on_device(): lax.ppermute(tokens, 'x', shift(X, s))  6.94 us
    ppermute x3, waiting for transfers between devices, on_device(): lax.ppermute(parts[s], 'y', shift(Y, -s))  6.15 us
    ppermute x3, starting transfers between devices, on_device(): lax.ppermute(tokens, 'x', shift(X, s))  5.63 us
    ppermute x3, starting transfers between devices, on_device(): lax.ppermute(picked, 'y', shift(Y, s))  5.06 us
    ppermute x3, starting transfers between devices, on_device(): lax.ppermute(attended, 'x', shift(X, s))  4.53 us
  transfers between devices with their start and end apart: 33, of which 10 were waited for; matrix products, arithmetic and copies ran while one was open for 3% of the time, Pallas kernels for 2%

commit v1 on v0

--- a/solution.py
+++ b/solution.py
@@ -19,6 +19,9 @@
 SMEM = pltpu.SMEM
 
 
+PARAMS = pltpu.CompilerParams(vmem_limit_bytes=16 * 1024 * 1024)
+
+
 def vmem(a):
     return pltpu.with_memory_space_constraint(a, VMEM)
 
@@ -40,39 +43,55 @@
     return jnp.concatenate([rows[:, :HEAD_SIZE], rows[:, HEAD_SIZE:]], axis=0).T
 
 
-def project_kernel(blocks, at, t0, t1, t2, t3, wq, wk, wv, q_out, kv_out):
-    pieces = [ref[...] for ref in (t0, t1, t2, t3)]
-    starts = [pl.multiple_of(at[s] * 256, 256) for s in range(4)]
-
-    def summed(weight):
-        total = None
-        for piece, start in zip(pieces, starts):
-            term = jnp.dot(piece, weight[pl.ds(start, 256), :], preferred_element_type=jnp.float32)
-            total = term if total is None else total + term
-        return total
-
+def stage_kernel(tokens, wq, wk, wv, tokens_out, w_out):
+    tokens_out[...] = tokens[...]
+    for i, ref in enumerate((wq, wk, wv)):
+        w_out[:, i * 128 : i * 128 + 128] = ref[...]
+
+
+def stage(tokens, weights):
+    depth, width = weights[0].shape
+    return pl.pallas_call(
+        stage_kernel,
+        out_shape=(
+            VMEM(tokens.shape, tokens.dtype),
+            VMEM((depth, 3 * width), jnp.bfloat16),
+        ),
+        in_specs=[full()] * 4,
+        out_specs=(full(),) * 2,
+        name="stage",
+        compiler_params=PARAMS,
+    )(*[pltpu.with_memory_space_constraint(a, pltpu.HBM) for a in (tokens, *weights)])
+
+
+def project_kernel(blocks, at, t0, t1, t2, t3, weight, q_out, kv_out):
+    total = None
+    for s, piece in enumerate((t0, t1, t2, t3)):
+        start = pl.multiple_of(at[s] * 256, 256)
+        term = jnp.dot(
+            piece[...], weight[pl.ds(start, 256), :], preferred_element_type=jnp.float32
+        )
+        total = term if total is None else total + term
     half = blocks * BLOCK
-    kv_out[:half, :] = summed(wk).astype(jnp.bfloat16)
-    values = summed(wv)
+    kv_out[:half, :] = total[:, 128:256].astype(jnp.bfloat16)
+    queries = total[:, :128].astype(jnp.bfloat16).astype(jnp.float32) * (HEAD_SIZE ** (-0.5))
+    values = total[:, 256:]
     for b in range(blocks):
-        turned = head_turn(values[b * 64 : b * 64 + 64])
-        kv_out[half + b * 64 : half + b * 64 + 64, :] = turned.astype(jnp.bfloat16)
-    queries = summed(wq).astype(jnp.bfloat16).astype(jnp.float32) * (HEAD_SIZE ** (-0.5))
-    for b in range(blocks):
-        q_out[b * 64 : b * 64 + 64, :] = head_turn(queries[b * 64 : b * 64 + 64]).astype(
-            jnp.bfloat16
-        )
-
-
-def project(at, pieces, weights):
+        here = slice(b * 64, b * 64 + 64)
+        kv_out[half + b * 64 : half + b * 64 + 64, :] = head_turn(values[here]).astype(jnp.bfloat16)
+        q_out[here, :] = head_turn(queries[here]).astype(jnp.bfloat16)
+
+
+def project(at, pieces, weight):
     rows = pieces[0].shape[0]
     return pl.pallas_call(
         functools.partial(project_kernel, rows // BLOCK),
         out_shape=(VMEM((rows, 128), jnp.bfloat16), VMEM((2 * rows, 128), jnp.bfloat16)),
-        in_specs=[full(SMEM)] + [full()] * 7,
+        in_specs=[full(SMEM)] + [full()] * 5,
         out_specs=(full(),) * 2,
         name="project",
-    )(at, *[vmem(a) for a in (*pieces, *weights)])
+        compiler_params=PARAMS,
+    )(at, *[vmem(a) for a in (*pieces, weight)])
 
 
 def spread_heads(rows, lane):
@@ -95,16 +114,18 @@
     return highest, mass, blended
 
 
-def attend_kernel(blocks, owners, first, last, *refs):
+def attend_kernel(blocks, owners, begin, last, *refs):
     refs = list(refs)
+    first = begin == 0
     table = refs.pop(0)
     q = [refs.pop(0) for _ in range(Y)]
     kv = [refs.pop(0) for _ in range(owners)]
     half = blocks * BLOCK
-    carry = None if first else [refs.pop(0) for _ in range(3)]
+    carry = None if first else refs.pop(0)
     if last:
         out = [refs.pop(0) for _ in range(Y)]
-    top, mass, total = refs
+    (state,) = refs
+    total, top, mass = (state.at[:, a:b, :] for a, b in ((0, 64), (64, 72), (72, 80)))
     lane = lax.broadcasted_iota(jnp.int32, (BLOCK, 128), 1)
 
     if first:
@@ -122,13 +143,12 @@
             mass[b] = jnp.broadcast_to(l, (8, 128))
             total[b] = o
     else:
-        for src, dst in zip(carry, (top, mass, total)):
-            dst[...] = src[...]
+        state[...] = carry[...]
 
     for owner in range(owners):
         found = []
         for p in range(Y):
-            code = table[owner * Y + p]
+            code = table[p * (Z * C) + begin + owner]
             row = jnp.maximum(code - 1, 0)
             local = pl.multiple_of((row & 7) * BLOCK, BLOCK)
             row = row >> 3
@@ -166,29 +186,26 @@
             out[p][blocks * 64 :, :] = jnp.concatenate(stats, axis=0).astype(jnp.bfloat16)
 
 
-def attend(table, q, kv, carry, last):
+def attend(table, begin, q, kv, carry, last):
     rows = q[0].shape[0]
     blocks = rows // BLOCK
     groups = Y * blocks
-    state = [
-        jax.ShapeDtypeStruct((groups, 8, 128), jnp.float32),
-        jax.ShapeDtypeStruct((groups, 8, 128), jnp.float32),
-        jax.ShapeDtypeStruct((groups, BLOCK, 128), jnp.float32),
-    ]
+    state = [jax.ShapeDtypeStruct((groups, BLOCK + 16, 128), jnp.float32)]
     if last:
         outs = [jax.ShapeDtypeStruct((rows + 8 * blocks, 128), jnp.bfloat16)] * Y
         scratch = [VMEM(s.shape, s.dtype) for s in state]
     else:
         outs, scratch = state, []
     outs = [VMEM(s.shape, s.dtype) for s in outs]
-    args = [table] + [vmem(a) for a in (*q, *kv, *(carry or ()))]
-    return pl.pallas_call(
-        functools.partial(attend_kernel, blocks, len(kv), carry is None, last),
+    args = [table] + [vmem(a) for a in (*q, *kv, *carry)]
+    return pl.pallas_call(
+        functools.partial(attend_kernel, blocks, len(kv), begin, last),
         out_shape=tuple(outs),
         in_specs=[full(SMEM)] + [full()] * (len(args) - 1),
         out_specs=(full(),) * len(outs),
         scratch_shapes=scratch,
         name="attend_late" if last else "attend_early",
+        compiler_params=PARAMS,
     )(*args)
 
 
@@ -217,6 +234,7 @@
         in_specs=[full()] * len(parts),
         out_specs=full(),
         name="merge",
+        compiler_params=PARAMS,
     )(*[vmem(a) for a in parts])
 
 
@@ -240,6 +258,7 @@
         in_specs=[full()] * 8,
         out_specs=full(),
         name="finish",
+        compiler_params=PARAMS,
     )(*[vmem(a) for a in (*pieces, *weights)])
 
 
@@ -270,7 +289,8 @@
         gained.append((columns.astype(jnp.float32) * norm_gain[:, None]).astype(jnp.bfloat16))
     weights = [gained[0]] + [lax.ppermute(gained[s], "x", shift(X, s)) for s in (1, 2, 3)]
 
-    q, kv = project(at, pieces, (query_weight, key_weight, value_weight))
+    staged, weight = stage(tokens, (query_weight, key_weight, value_weight))
+    q, kv = project(at, [staged] + pieces[1:], weight)
 
     places = [(i, j) for i in range(Z) for j in range(C)]
 
@@ -296,15 +316,17 @@
     column = jnp.stack(
         [((z + toward * d) % Z) * (Y * C) + y * C + (c ^ cc) for d, cc, _ in held]
     ).astype(jnp.int32)
-    picks = jnp.stack(picks)
-    code = 1 + 8 * jnp.arange(blocks, dtype=jnp.int32)[None, :, None] + (picks & 7)
-    hit = (picks >> 3)[None] == column[:, None, None, None]
-    table = jnp.sum(jnp.where(hit, code[None], 0), axis=(2, 3)).reshape(-1)
+    picks = jnp.stack(picks).reshape(Y, 1, -1)
+    chosen = chosen_owner.shape[1]
+    row = jnp.arange(blocks * chosen, dtype=jnp.int32) // chosen
+    code = 1 + 8 * row + (picks & 7)
+    hit = (picks >> 3) == column[None, :, None]
+    table = jnp.sum(jnp.where(hit, code, 0), axis=2).reshape(-1)
 
     early = 10
     arrays = [a for _, _, a in held]
-    carry = attend(table[: early * Y], queries, arrays[:early], None, False)
-    parts = attend(table[early * Y :], queries, arrays[early:], carry, True)
+    carry = attend(table, 0, queries, arrays[:early], (), False)
+    parts = attend(table, early, queries, arrays[early:], carry, True)
 
     back = [parts[0]] + [lax.ppermute(parts[s], "y", shift(Y, -s)) for s in (1, 2, 3)]
     attended = merge(back, blocks)

time: 97.3 us -> 83.2 us (0.86)
  local copies, waits for them, and re-layouts: 13.3 us -> 1.54 us
  starting transfers between devices: 51.3 us -> 49.3 us
    unnamed x40 -> x8, local copies, waits for them, and re-layouts: 11.7 us -> 0.02 us
    ppermute x8, starting transfers between devices: 10.6 us -> 8.62 us  [swap(): return lax.ppermute(a, 'c', [(0, 1), (1, 0)])]
    slice x5 -> x0, local copies, waits for them, and re-layouts: 1.6 us -> none  [the longest x3 0.82 us: on_device(): parts = attend(table[early * Y:], queries, arrays[early:], carry, True)]
    another operation x0 -> x4, local copies, waits for them, and re-layouts: none -> 1.34 us  [on_device(): picks = jnp.stack(picks).reshape(Y, 1, -1)]
    pallas_call x2 -> x3, Pallas kernels: 3.89 us -> 4.52 us  [the longest x2 3.17 us: attend(): pl.pallas_call(functools.partial(attend_kernel, blocks, len(kv), begin, l...]
  transfers between devices with their start and end apart: 33 -> 33, of which waited for: 10 -> 9; matrix products, arithmetic and copies ran while one was open for 3% -> 4% of each run, Pallas kernels for 2% -> 4%
where the time goes in v1:
time: 83.2 us; the launch traced here: 83.1 us
  starting transfers between devices  49.3 us (59%)
  waiting for transfers between devices  23.1 us (28%)
  Pallas kernels  7.39 us (9%)
  other arithmetic  1.66 us (2%)
  local copies, waits for them, and re-layouts  1.54 us (2%)
    ppermute x3, starting transfers between devices, on_device(): same.append(lax.ppermute(same[-1], ('z', 'c'), onward(1)))  9.8 us
    ppermute x8, starting transfers between devices, swap(): return lax.ppermute(a, 'c', [(0, 1), (1, 0)])  8.62 us
    ppermute x3, waiting for transfers between devices, on_device(): lax.ppermute(tokens, 'x', shift(X, s))  6.16 us
    ppermute x3, waiting for transfers between devices, on_device(): lax.ppermute(parts[s], 'y', shift(Y, -s))  6.13 us
    ppermute x3, starting transfers between devices, on_device(): lax.ppermute(tokens, 'x', shift(X, s))  5.63 us
    ppermute x3, starting transfers between devices, on_device(): lax.ppermute(picked, 'y', shift(Y, s))  5.06 us
    ppermute x3, starting transfers between devices, on_device(): lax.ppermute(attended, 'x', shift(X, s))  4.53 us
    ppermute x3, starting transfers between devices, on_device(): cross.append(lax.ppermute(cross[-1], ('z', 'c'), onward(1)))  4.1 us
  transfers between devices with their start and end apart: 33, of which 9 were waited for; matrix products, arithmetic and copies ran while one was open for 4% of the time, Pallas kernels for 4%

profile of v1, /device:TPU:1, one launch (start us, length us, event | category | flops | bytes accessed | tf_op | source)
XLA Modules:
  0.0 83.1 jit_solution(5900192244558490972)
XLA Ops:
  0.0 2.0 %collective-permute-start.3 = (bf16[384,256]{1,0:T(8,128)(2,1)}, bf16[384,256]{1,0:T(8,128)(2,1)S(1)}, u32[]{:S(2)}, u32[]{:S(2)}) collective-permute-start(bf16[384,256]{1,0:T(8,128)(2,1)} %tokens.1), channel_id=1, source_target_pairs={{0,1},{1,2},{2,3},{3,0},{4,5},{5,6},{6,7},{7,4},{8,9},{9,10},{10,1... | collective-permute-start | bytes 589832 | tf_op jit(solution)/shard_map/ppermute | solution.py:279
  2.0 2.5 %collective-permute-start.4 = (bf16[384,256]{1,0:T(8,128)(2,1)}, bf16[384,256]{1,0:T(8,128)(2,1)S(1)}, u32[]{:S(2)}, u32[]{:S(2)}) collective-permute-start(bf16[384,256]{1,0:T(8,128)(2,1)} %tokens.1), channel_id=1, source_target_pairs={{0,2},{1,3},{2,0},{3,1},{4,6},{5,7},{6,4},{7,5},{8,10},{9,11},{10,... | collective-permute-start | bytes 589832 | tf_op jit(solution)/shard_map/ppermute | solution.py:279
  7.1 6.2 %collective-permute-done.4.t2 = bf16[384,256]{1,0:T(8,128)(2,1)S(1)} collective-permute-done((bf16[384,256]{1,0:T(8,128)(2,1)}, bf16[384,256]{1,0:T(8,128)(2,1)S(1)}, u32[]{:S(2)}, u32[]{:S(2)}) %collective-permute-start.4) | collective-permute-done | bytes 196640 | tf_op jit(solution)/shard_map/ppermute | solution.py:279
  13.2 1.5 %project.1 = (bf16[384,128]{1,0:T(8,128)(2,1)S(1)}, bf16[768,128]{1,0:T(8,128)(2,1)S(1)}) custom-call(s32[4]{0:T(128)S(1)} %pad_add_fusion.1.at, bf16[384,256]{1,0:T(8,128)(2,1)S(1)} %get-tuple-element.13.t0, bf16[384,256]{1,0:T(8,128)(2,1)S(1)} %collective-permute-done.3.t1, bf16[384,256]{1,0:T(8,128)(2,1)S(1)} %collective-permute-done.4.t2, ...), custom_call_target="tpu_custom_call" | custom-call | tf_op jit(solution)/shard_map/project/pallas_call | solution.py:87
  14.7 1.6 %collective-permute-start.12 = (bf16[768,128]{1,0:T(8,128)(2,1)S(1)}, bf16[768,128]{1,0:T(8,128)(2,1)S(1)}, u32[]{:S(2)}, u32[]{:S(2)}) collective-permute-start(bf16[768,128]{1,0:T(8,128)(2,1)S(1)} %get-tuple-element.16.refs_5_), channel_id=1, source_target_pairs={{0,4},{4,0},{1,5},{5,1},{2,6},{6,2},{3,7},{7,3},{8,12},{12,8},{9,1... | collective-permute-start | bytes 589832 | tf_op jit(solution)/shard_map/ppermute | solution.py:301
  16.3 5.6 %collective-permute-start.9 = (bf16[768,128]{1,0:T(8,128)(2,1)S(1)}, bf16[768,128]{1,0:T(8,128)(2,1)S(1)}, u32[]{:S(2)}, u32[]{:S(2)}) collective-permute-start(bf16[768,128]{1,0:T(8,128)(2,1)S(1)} %get-tuple-element.16.refs_5_), channel_id=1, source_target_pairs={{0,32},{4,228},{32,64},{36,4},{64,96},{68,36},{96,128},{100,68},{1... | collective-permute-start | bytes 589832 | tf_op jit(solution)/shard_map/ppermute | solution.py:306
  23.0 1.5 %collective-permute-done.9.refs_7_ = bf16[768,128]{1,0:T(8,128)(2,1)S(1)} collective-permute-done((bf16[768,128]{1,0:T(8,128)(2,1)S(1)}, bf16[768,128]{1,0:T(8,128)(2,1)S(1)}, u32[]{:S(2)}, u32[]{:S(2)}) %collective-permute-start.9) | collective-permute-done | bytes 196640 | tf_op jit(solution)/shard_map/ppermute | solution.py:306
  24.5 3.1 %collective-permute-start.10 = (bf16[768,128]{1,0:T(8,128)(2,1)S(1)}, bf16[768,128]{1,0:T(8,128)(2,1)S(1)}, u32[]{:S(2)}, u32[]{:S(2)}) collective-permute-start(bf16[768,128]{1,0:T(8,128)(2,1)S(1)} %collective-permute-done.9.refs_7_), channel_id=1, source_target_pairs={{0,32},{4,228},{32,64},{36,4},{64,96},{68,36},{96,128},{100,68},{1... | collective-permute-start | bytes 589832 | tf_op jit(solution)/shard_map/ppermute | solution.py:306
  27.6 2.1 %collective-permute-start.14 = (bf16[768,128]{1,0:T(8,128)(2,1)S(1)}, bf16[768,128]{1,0:T(8,128)(2,1)S(1)}, u32[]{:S(2)}, u32[]{:S(2)}) collective-permute-start(bf16[768,128]{1,0:T(8,128)(2,1)S(1)} %collective-permute-done.13.refs_8_), channel_id=1, source_target_pairs={{0,32},{4,228},{32,64},{36,4},{64,96},{68,36},{96,128},{100,68},{1... | collective-permute-start | bytes 589832 | tf_op jit(solution)/shard_map/ppermute | solution.py:307
  31.1 2.6 %collective-permute-start.1 = (s32[6,8]{1,0:T(8,128)S(1)}, s32[6,8]{1,0:T(8,128)S(1)}, u32[]{:S(2)}, u32[]{:S(2)}) collective-permute-start(s32[6,8]{1,0:T(8,128)S(1)} %multiply_add_fusion), channel_id=1, source_target_pairs={{0,16},{8,24},{16,0},{24,8},{1,17},{9,25},{17,1},{25,9},{2,18},{10... | collective-permute-start | bytes 584 | tf_op jit(solution)/shard_map/ppermute | solution.py:283
  35.2 2.6 %collective-permute-start.7 = (bf16[384,128]{1,0:T(8,128)(2,1)S(1)}, bf16[384,128]{1,0:T(8,128)(2,1)S(1)}, u32[]{:S(2)}, u32[]{:S(2)}) collective-permute-start(bf16[384,128]{1,0:T(8,128)(2,1)S(1)} %get-tuple-element.15.refs_1_), channel_id=1, source_target_pairs={{0,16},{8,24},{16,0},{24,8},{1,17},{9,25},{17,1},{25,9},{2,18},{10... | collective-permute-start | bytes 294920 | tf_op jit(solution)/shard_map/ppermute | solution.py:313
  38.8 3.5 %collective-permute-done.6.refs_2_ = bf16[384,128]{1,0:T(8,128)(2,1)S(1)} collective-permute-done((bf16[384,128]{1,0:T(8,128)(2,1)S(1)}, bf16[384,128]{1,0:T(8,128)(2,1)S(1)}, u32[]{:S(2)}, u32[]{:S(2)}) %collective-permute-start.6) | collective-permute-done | bytes 98336 | tf_op jit(solution)/shard_map/ppermute | solution.py:313
  47.8 2.3 %collective-permute-start.22 = (bf16[768,128]{1,0:T(8,128)(2,1)S(1)}, bf16[768,128]{1,0:T(8,128)(2,1)S(1)}, u32[]{:S(2)}, u32[]{:S(2)}) collective-permute-start(bf16[768,128]{1,0:T(8,128)(2,1)S(1)} %collective-permute-done.10.refs_11_), channel_id=1, source_target_pairs={{0,4},{4,0},{1,5},{5,1},{2,6},{6,2},{3,7},{7,3},{8,12},{12,8},{9,1... | collective-permute-start | bytes 589832 | tf_op jit(solution)/shard_map/ppermute | solution.py:301
  50.2 1.9 %collective-permute-start.16 = (bf16[768,128]{1,0:T(8,128)(2,1)S(1)}, bf16[768,128]{1,0:T(8,128)(2,1)S(1)}, u32[]{:S(2)}, u32[]{:S(2)}) collective-permute-start(bf16[768,128]{1,0:T(8,128)(2,1)S(1)} %collective-permute-done.11.refs_5_), channel_id=1, source_target_pairs={{0,4},{4,0},{1,5},{5,1},{2,6},{6,2},{3,7},{7,3},{8,12},{12,8},{9,1... | collective-permute-start | bytes 589832 | tf_op jit(solution)/shard_map/ppermute | solution.py:301
  52.1 1.9 %collective-permute-done.15.refs_6_ = bf16[768,128]{1,0:T(8,128)(2,1)S(1)} collective-permute-done((bf16[768,128]{1,0:T(8,128)(2,1)S(1)}, bf16[768,128]{1,0:T(8,128)(2,1)S(1)}, u32[]{:S(2)}, u32[]{:S(2)}) %collective-permute-start.15) | collective-permute-done | bytes 196640 | tf_op jit(solution)/shard_map/ppermute | solution.py:307
  54.0 2.3 %collective-permute-start.17 = (bf16[768,128]{1,0:T(8,128)(2,1)S(1)}, bf16[768,128]{1,0:T(8,128)(2,1)S(1)}, u32[]{:S(2)}, u32[]{:S(2)}) collective-permute-start(bf16[768,128]{1,0:T(8,128)(2,1)S(1)} %collective-permute-done.15.refs_6_), channel_id=1, source_target_pairs={{0,4},{4,0},{1,5},{5,1},{2,6},{6,2},{3,7},{7,3},{8,12},{12,8},{9,1... | collective-permute-start | bytes 589832 | tf_op jit(solution)/shard_map/ppermute | solution.py:301
  57.3 1.8 %attend_early.1.refs_11_ = f32[24,80,128]{2,1,0:T(8,128)S(1)} custom-call(s32[64]{0:T(128)S(1)} %reshape.123.refs_0_, bf16[384,128]{1,0:T(8,128)(2,1)S(1)} %get-tuple-element.15.refs_1_, bf16[384,128]{1,0:T(8,128)(2,1)S(1)} %collective-permute-done.6.refs_2_, bf16[384,128]{1,0:T(8,128)(2,1)S(1)} %collective-permute-done.7.refs_3_, ...), custom_call_target="tpu_custom_call" | custom-call | tf_op jit(solution)/shard_map/attend_early/pallas_call | solution.py:201
  60.5 1.5 %collective-permute-start.24 = (bf16[432,128]{1,0:T(8,128)(2,1)S(1)}, bf16[432,128]{1,0:T(8,128)(2,1)S(1)}, u32[]{:S(2)}, u32[]{:S(2)}) collective-permute-start(bf16[432,128]{1,0:T(8,128)(2,1)S(1)} %get-tuple-element.18), channel_id=1, source_target_pairs={{0,24},{8,0},{16,8},{24,16},{1,25},{9,1},{17,9},{25,17},{2,26},{10... | collective-permute-start | bytes 331784 | tf_op jit(solution)/shard_map/ppermute | solution.py:331
  65.2 2.7 %collective-permute-done.25.refs_2_ = bf16[432,128]{1,0:T(8,128)(2,1)S(1)} collective-permute-done((bf16[432,128]{1,0:T(8,128)(2,1)S(1)}, bf16[432,128]{1,0:T(8,128)(2,1)S(1)}, u32[]{:S(2)}, u32[]{:S(2)}) %collective-permute-start.25) | collective-permute-done | bytes 110624 | tf_op jit(solution)/shard_map/ppermute | solution.py:331
  67.9 3.0 %collective-permute-done.26.refs_3_ = bf16[432,128]{1,0:T(8,128)(2,1)S(1)} collective-permute-done((bf16[432,128]{1,0:T(8,128)(2,1)S(1)}, bf16[432,128]{1,0:T(8,128)(2,1)S(1)}, u32[]{:S(2)}, u32[]{:S(2)}) %collective-permute-start.26) | collective-permute-done | bytes 110624 | tf_op jit(solution)/shard_map/ppermute | solution.py:331
  72.3 2.1 %collective-permute-start.28 = (bf16[384,128]{1,0:T(8,128)(2,1)S(1)}, bf16[384,128]{1,0:T(8,128)(2,1)S(1)}, u32[]{:S(2)}, u32[]{:S(2)}) collective-permute-start(bf16[384,128]{1,0:T(8,128)(2,1)S(1)} %merge.1.a0), channel_id=1, source_target_pairs={{0,2},{1,3},{2,0},{3,1},{4,6},{5,7},{6,4},{7,5},{8,10},{9,11},{10,... | collective-permute-start | bytes 294920 | tf_op jit(solution)/shard_map/ppermute | solution.py:333
  76.3 2.0 %collective-permute-start.32 = (bf16[128,256]{1,0:T(8,128)(2,1)S(1)}, bf16[128,256]{1,0:T(8,128)(2,1)S(1)}, u32[]{:S(2)}, u32[]{:S(2)}) collective-permute-start(bf16[128,256]{1,0:T(8,128)(2,1)S(1)} %get-tuple-element.21), channel_id=1, source_target_pairs={{0,3},{1,0},{2,1},{3,2},{4,7},{5,4},{6,5},{7,6},{8,11},{9,8},{10,9... | collective-permute-start | bytes 196616 | tf_op jit(solution)/shard_map/ppermute | solution.py:290
  78.3 2.0 %collective-permute-done.31.w2 = bf16[128,256]{1,0:T(8,128)(2,1)S(1)} collective-permute-done((bf16[128,256]{1,0:T(8,128)(2,1)S(1)}, bf16[128,256]{1,0:T(8,128)(2,1)S(1)}, u32[]{:S(2)}, u32[]{:S(2)}) %collective-permute-start.31) | collective-permute-done | bytes 65568 | tf_op jit(solution)/shard_map/ppermute | solution.py:290
  80.3 1.7 %collective-permute-done.32.w3 = bf16[128,256]{1,0:T(8,128)(2,1)S(1)} collective-permute-done((bf16[128,256]{1,0:T(8,128)(2,1)S(1)}, bf16[128,256]{1,0:T(8,128)(2,1)S(1)}, u32[]{:S(2)}, u32[]{:S(2)}) %collective-permute-start.32) | collective-permute-done | bytes 65568 | tf_op jit(solution)/shard_map/ppermute | solution.py:290
  (68 shorter events, 23.1 us)
Async XLA Ops:
  0.0 7.1 %collective-permute-start.3 = (bf16[384,256]{1,0:T(8,128)(2,1)}, bf16[384,256]{1,0:T(8,128)(2,1)S(1)}, u32[]{:S(2)}, u32[]{:S(2)}) collective-permute-start(bf16[384,256]{1,0:T(8,128)(2,1)} %tokens.1), channel_id=1, source_target_pairs={{0,1},{1,2},{2,3},{3,0},{4,5},{5,6},{6,7},{7,4},{8,9},{9,10},{10,1... | collective-permute-start | bytes 589832 | tf_op jit(solution)/shard_map/ppermute | solution.py:279
  2.0 11.2 %collective-permute-start.4 = (bf16[384,256]{1,0:T(8,128)(2,1)}, bf16[384,256]{1,0:T(8,128)(2,1)S(1)}, u32[]{:S(2)}, u32[]{:S(2)}) collective-permute-start(bf16[384,256]{1,0:T(8,128)(2,1)} %tokens.1), channel_id=1, source_target_pairs={{0,2},{1,3},{2,0},{3,1},{4,6},{5,7},{6,4},{7,5},{8,10},{9,11},{10,... | collective-permute-start | bytes 589832 | tf_op jit(solution)/shard_map/ppermute | solution.py:279
  4.5 8.7 %collective-permute-start.5 = (bf16[384,256]{1,0:T(8,128)(2,1)}, bf16[384,256]{1,0:T(8,128)(2,1)S(1)}, u32[]{:S(2)}, u32[]{:S(2)}) collective-permute-start(bf16[384,256]{1,0:T(8,128)(2,1)} %tokens.1), channel_id=1, source_target_pairs={{0,3},{1,0},{2,1},{3,2},{4,7},{5,4},{6,5},{7,6},{8,11},{9,8},{10,9... | collective-permute-start | bytes 589832 | tf_op jit(solution)/shard_map/ppermute | solution.py:279
  14.7 7.2 %collective-permute-start.12 = (bf16[768,128]{1,0:T(8,128)(2,1)S(1)}, bf16[768,128]{1,0:T(8,128)(2,1)S(1)}, u32[]{:S(2)}, u32[]{:S(2)}) collective-permute-start(bf16[768,128]{1,0:T(8,128)(2,1)S(1)} %get-tuple-element.16.refs_5_), channel_id=1, source_target_pairs={{0,4},{4,0},{1,5},{5,1},{2,6},{6,2},{3,7},{7,3},{8,12},{12,8},{9,1... | collective-permute-start | bytes 589832 | tf_op jit(solution)/shard_map/ppermute | solution.py:301
  16.3 8.2 %collective-permute-start.9 = (bf16[768,128]{1,0:T(8,128)(2,1)S(1)}, bf16[768,128]{1,0:T(8,128)(2,1)S(1)}, u32[]{:S(2)}, u32[]{:S(2)}) collective-permute-start(bf16[768,128]{1,0:T(8,128)(2,1)S(1)} %get-tuple-element.16.refs_5_), channel_id=1, source_target_pairs={{0,32},{4,228},{32,64},{36,4},{64,96},{68,36},{96,128},{100,68},{1... | collective-permute-start | bytes 589832 | tf_op jit(solution)/shard_map/ppermute | solution.py:306
  24.5 18.3 %collective-permute-start.10 = (bf16[768,128]{1,0:T(8,128)(2,1)S(1)}, bf16[768,128]{1,0:T(8,128)(2,1)S(1)}, u32[]{:S(2)}, u32[]{:S(2)}) collective-permute-start(bf16[768,128]{1,0:T(8,128)(2,1)S(1)} %collective-permute-done.9.refs_7_), channel_id=1, source_target_pairs={{0,32},{4,228},{32,64},{36,4},{64,96},{68,36},{96,128},{100,68},{1... | collective-permute-start | bytes 589832 | tf_op jit(solution)/shard_map/ppermute | solution.py:306
  27.6 17.2 %collective-permute-start.14 = (bf16[768,128]{1,0:T(8,128)(2,1)S(1)}, bf16[768,128]{1,0:T(8,128)(2,1)S(1)}, u32[]{:S(2)}, u32[]{:S(2)}) collective-permute-start(bf16[768,128]{1,0:T(8,128)(2,1)S(1)} %collective-permute-done.13.refs_8_), channel_id=1, source_target_pairs={{0,32},{4,228},{32,64},{36,4},{64,96},{68,36},{96,128},{100,68},{1... | collective-permute-start | bytes 589832 | tf_op jit(solution)/shard_map/ppermute | solution.py:307
  34.8 7.4 %collective-permute-start.6 = (bf16[384,128]{1,0:T(8,128)(2,1)S(1)}, bf16[384,128]{1,0:T(8,128)(2,1)S(1)}, u32[]{:S(2)}, u32[]{:S(2)}) collective-permute-start(bf16[384,128]{1,0:T(8,128)(2,1)S(1)} %get-tuple-element.15.refs_1_), channel_id=1, source_target_pairs={{0,8},{8,16},{16,24},{24,0},{1,9},{9,17},{17,25},{25,1},{2,10},{10... | collective-permute-start | bytes 294920 | tf_op jit(solution)/shard_map/ppermute | solution.py:313
  35.2 7.3 %collective-permute-start.7 = (bf16[384,128]{1,0:T(8,128)(2,1)S(1)}, bf16[384,128]{1,0:T(8,128)(2,1)S(1)}, u32[]{:S(2)}, u32[]{:S(2)}) collective-permute-start(bf16[384,128]{1,0:T(8,128)(2,1)S(1)} %get-tuple-element.15.refs_1_), channel_id=1, source_target_pairs={{0,16},{8,24},{16,0},{24,8},{1,17},{9,25},{17,1},{25,9},{2,18},{10... | collective-permute-start | bytes 294920 | tf_op jit(solution)/shard_map/ppermute | solution.py:313
  37.8 6.1 %collective-permute-start.8 = (bf16[384,128]{1,0:T(8,128)(2,1)S(1)}, bf16[384,128]{1,0:T(8,128)(2,1)S(1)}, u32[]{:S(2)}, u32[]{:S(2)}) collective-permute-start(bf16[384,128]{1,0:T(8,128)(2,1)S(1)} %get-tuple-element.15.refs_1_), channel_id=1, source_target_pairs={{0,24},{8,0},{16,8},{24,16},{1,25},{9,1},{17,9},{25,17},{2,26},{10... | collective-permute-start | bytes 294920 | tf_op jit(solution)/shard_map/ppermute | solution.py:313
  42.5 7.5 %collective-permute-start.21 = (bf16[768,128]{1,0:T(8,128)(2,1)S(1)}, bf16[768,128]{1,0:T(8,128)(2,1)S(1)}, u32[]{:S(2)}, u32[]{:S(2)}) collective-permute-start(bf16[768,128]{1,0:T(8,128)(2,1)S(1)} %collective-permute-done.13.refs_8_), channel_id=1, source_target_pairs={{0,4},{4,0},{1,5},{5,1},{2,6},{6,2},{3,7},{7,3},{8,12},{12,8},{9,1... | collective-permute-start | bytes 589832 | tf_op jit(solution)/shard_map/ppermute | solution.py:301
  42.8 7.4 %collective-permute-start.11 = (bf16[768,128]{1,0:T(8,128)(2,1)S(1)}, bf16[768,128]{1,0:T(8,128)(2,1)S(1)}, u32[]{:S(2)}, u32[]{:S(2)}) collective-permute-start(bf16[768,128]{1,0:T(8,128)(2,1)S(1)} %collective-permute-done.10.refs_11_), channel_id=1, source_target_pairs={{0,32},{4,228},{32,64},{36,4},{64,96},{68,36},{96,128},{100,68},{1... | collective-permute-start | bytes 589832 | tf_op jit(solution)/shard_map/ppermute | solution.py:306
  43.9 8.2 %collective-permute-start.18 = (bf16[768,128]{1,0:T(8,128)(2,1)S(1)}, bf16[768,128]{1,0:T(8,128)(2,1)S(1)}, u32[]{:S(2)}, u32[]{:S(2)}) collective-permute-start(bf16[768,128]{1,0:T(8,128)(2,1)S(1)} %collective-permute-done.10.refs_11_), channel_id=1, source_target_pairs={{0,64},{4,196},{32,96},{36,228},{64,128},{68,4},{96,160},{100,36},... | collective-permute-start | bytes 589832 | tf_op jit(solution)/shard_map/ppermute | solution.py:310
  44.9 9.1 %collective-permute-start.15 = (bf16[768,128]{1,0:T(8,128)(2,1)S(1)}, bf16[768,128]{1,0:T(8,128)(2,1)S(1)}, u32[]{:S(2)}, u32[]{:S(2)}) collective-permute-start(bf16[768,128]{1,0:T(8,128)(2,1)S(1)} %collective-permute-done.14.refs_12_), channel_id=1, source_target_pairs={{0,32},{4,228},{32,64},{36,4},{64,96},{68,36},{96,128},{100,68},{1... | collective-permute-start | bytes 589832 | tf_op jit(solution)/shard_map/ppermute | solution.py:307
  47.8 9.4 %collective-permute-start.22 = (bf16[768,128]{1,0:T(8,128)(2,1)S(1)}, bf16[768,128]{1,0:T(8,128)(2,1)S(1)}, u32[]{:S(2)}, u32[]{:S(2)}) collective-permute-start(bf16[768,128]{1,0:T(8,128)(2,1)S(1)} %collective-permute-done.10.refs_11_), channel_id=1, source_target_pairs={{0,4},{4,0},{1,5},{5,1},{2,6},{6,2},{3,7},{7,3},{8,12},{12,8},{9,1... | collective-permute-start | bytes 589832 | tf_op jit(solution)/shard_map/ppermute | solution.py:301
  50.1 7.2 %collective-permute-start.23 = (bf16[768,128]{1,0:T(8,128)(2,1)S(1)}, bf16[768,128]{1,0:T(8,128)(2,1)S(1)}, u32[]{:S(2)}, u32[]{:S(2)}) collective-permute-start(bf16[768,128]{1,0:T(8,128)(2,1)S(1)} %collective-permute-done.14.refs_12_), channel_id=1, source_target_pairs={{0,4},{4,0},{1,5},{5,1},{2,6},{6,2},{3,7},{7,3},{8,12},{12,8},{9,1... | collective-permute-start | bytes 589832 | tf_op jit(solution)/shard_map/ppermute | solution.py:301
  50.2 8.9 %collective-permute-start.16 = (bf16[768,128]{1,0:T(8,128)(2,1)S(1)}, bf16[768,128]{1,0:T(8,128)(2,1)S(1)}, u32[]{:S(2)}, u32[]{:S(2)}) collective-permute-start(bf16[768,128]{1,0:T(8,128)(2,1)S(1)} %collective-permute-done.11.refs_5_), channel_id=1, source_target_pairs={{0,4},{4,0},{1,5},{5,1},{2,6},{6,2},{3,7},{7,3},{8,12},{12,8},{9,1... | collective-permute-start | bytes 589832 | tf_op jit(solution)/shard_map/ppermute | solution.py:301
  52.1 7.0 %collective-permute-start.19 = (bf16[768,128]{1,0:T(8,128)(2,1)S(1)}, bf16[768,128]{1,0:T(8,128)(2,1)S(1)}, u32[]{:S(2)}, u32[]{:S(2)}) collective-permute-start(bf16[768,128]{1,0:T(8,128)(2,1)S(1)} %collective-permute-done.18.refs_9_), channel_id=1, source_target_pairs={{0,4},{4,0},{1,5},{5,1},{2,6},{6,2},{3,7},{7,3},{8,12},{12,8},{9,1... | collective-permute-start | bytes 589832 | tf_op jit(solution)/shard_map/ppermute | solution.py:301
  62.0 5.8 %collective-permute-start.25 = (bf16[432,128]{1,0:T(8,128)(2,1)S(1)}, bf16[432,128]{1,0:T(8,128)(2,1)S(1)}, u32[]{:S(2)}, u32[]{:S(2)}) collective-permute-start(bf16[432,128]{1,0:T(8,128)(2,1)S(1)} %get-tuple-element.19), channel_id=1, source_target_pairs={{0,16},{8,24},{16,0},{24,8},{1,17},{9,25},{17,1},{25,9},{2,18},{10... | collective-permute-start | bytes 331784 | tf_op jit(solution)/shard_map/ppermute | solution.py:331
  63.2 7.6 %collective-permute-start.26 = (bf16[432,128]{1,0:T(8,128)(2,1)S(1)}, bf16[432,128]{1,0:T(8,128)(2,1)S(1)}, u32[]{:S(2)}, u32[]{:S(2)}) collective-permute-start(bf16[432,128]{1,0:T(8,128)(2,1)S(1)} %get-tuple-element.20), channel_id=1, source_target_pairs={{0,8},{8,16},{16,24},{24,0},{1,9},{9,17},{17,25},{25,1},{2,10},{10... | collective-permute-start | bytes 331784 | tf_op jit(solution)/shard_map/ppermute | solution.py:331
  63.6 12.8 %collective-permute-start.30 = (bf16[128,256]{1,0:T(8,128)(2,1)S(1)}, bf16[128,256]{1,0:T(8,128)(2,1)S(1)}, u32[]{:S(2)}, u32[]{:S(2)}) collective-permute-start(bf16[128,256]{1,0:T(8,128)(2,1)S(1)} %get-tuple-element.22), channel_id=1, source_target_pairs={{0,1},{1,2},{2,3},{3,0},{4,5},{5,6},{6,7},{7,4},{8,9},{9,10},{10,1... | collective-permute-start | bytes 196616 | tf_op jit(solution)/shard_map/ppermute | solution.py:290
  71.2 10.9 %collective-permute-start.27 = (bf16[384,128]{1,0:T(8,128)(2,1)S(1)}, bf16[384,128]{1,0:T(8,128)(2,1)S(1)}, u32[]{:S(2)}, u32[]{:S(2)}) collective-permute-start(bf16[384,128]{1,0:T(8,128)(2,1)S(1)} %merge.1.a0), channel_id=1, source_target_pairs={{0,1},{1,2},{2,3},{3,0},{4,5},{5,6},{6,7},{7,4},{8,9},{9,10},{10,1... | collective-permute-start | bytes 294920 | tf_op jit(solution)/shard_map/ppermute | solution.py:333
  72.3 9.7 %collective-permute-start.28 = (bf16[384,128]{1,0:T(8,128)(2,1)S(1)}, bf16[384,128]{1,0:T(8,128)(2,1)S(1)}, u32[]{:S(2)}, u32[]{:S(2)}) collective-permute-start(bf16[384,128]{1,0:T(8,128)(2,1)S(1)} %merge.1.a0), channel_id=1, source_target_pairs={{0,2},{1,3},{2,0},{3,1},{4,6},{5,7},{6,4},{7,5},{8,10},{9,11},{10,... | collective-permute-start | bytes 294920 | tf_op jit(solution)/shard_map/ppermute | solution.py:333
  74.4 7.6 %collective-permute-start.29 = (bf16[384,128]{1,0:T(8,128)(2,1)S(1)}, bf16[384,128]{1,0:T(8,128)(2,1)S(1)}, u32[]{:S(2)}, u32[]{:S(2)}) collective-permute-start(bf16[384,128]{1,0:T(8,128)(2,1)S(1)} %merge.1.a0), channel_id=1, source_target_pairs={{0,3},{1,0},{2,1},{3,2},{4,7},{5,4},{6,5},{7,6},{8,11},{9,8},{10,9... | collective-permute-start | bytes 294920 | tf_op jit(solution)/shard_map/ppermute | solution.py:333
  (13 other events, 83.5 us)

commit v2 on v1

--- a/solution.py
+++ b/solution.py
@@ -64,34 +64,42 @@
     )(*[pltpu.with_memory_space_constraint(a, pltpu.HBM) for a in (tokens, *weights)])
 
 
-def project_kernel(blocks, at, t0, t1, t2, t3, weight, q_out, kv_out):
+def summed(at, pieces, weight, columns):
     total = None
-    for s, piece in enumerate((t0, t1, t2, t3)):
-        start = pl.multiple_of(at[s] * 256, 256)
-        term = jnp.dot(
-            piece[...], weight[pl.ds(start, 256), :], preferred_element_type=jnp.float32
-        )
+    for s, piece in enumerate(pieces):
+        rows = pl.ds(pl.multiple_of(at[s] * 256, 256), 256)
+        term = jnp.dot(piece[...], weight[rows, columns], preferred_element_type=jnp.float32)
         total = term if total is None else total + term
+    return total
+
+
+def project_kernel(blocks, at, t0, t1, t2, t3, weight, kv_out):
+    total = summed(at, (t0, t1, t2, t3), weight, slice(128, 384))
     half = blocks * BLOCK
-    kv_out[:half, :] = total[:, 128:256].astype(jnp.bfloat16)
-    queries = total[:, :128].astype(jnp.bfloat16).astype(jnp.float32) * (HEAD_SIZE ** (-0.5))
-    values = total[:, 256:]
+    kv_out[:half, :] = total[:, :128].astype(jnp.bfloat16)
+    for b in range(blocks):
+        turned = head_turn(total[b * 64 : b * 64 + 64, 128:])
+        kv_out[half + b * 64 : half + b * 64 + 64, :] = turned.astype(jnp.bfloat16)
+
+
+def query_kernel(blocks, at, t0, t1, t2, t3, weight, picks, q_out):
+    total = summed(at, (t0, t1, t2, t3), weight, slice(0, 128))
+    total = total.astype(jnp.bfloat16).astype(jnp.float32) * (HEAD_SIZE ** (-0.5))
     for b in range(blocks):
         here = slice(b * 64, b * 64 + 64)
-        kv_out[half + b * 64 : half + b * 64 + 64, :] = head_turn(values[here]).astype(jnp.bfloat16)
-        q_out[here, :] = head_turn(queries[here]).astype(jnp.bfloat16)
-
-
-def project(at, pieces, weight):
-    rows = pieces[0].shape[0]
-    return pl.pallas_call(
-        functools.partial(project_kernel, rows // BLOCK),
-        out_shape=(VMEM((rows, 128), jnp.bfloat16), VMEM((2 * rows, 128), jnp.bfloat16)),
-        in_specs=[full(SMEM)] + [full()] * 5,
-        out_specs=(full(),) * 2,
-        name="project",
-        compiler_params=PARAMS,
-    )(at, *[vmem(a) for a in (*pieces, weight)])
+        q_out[here, :] = head_turn(total[here]).astype(jnp.bfloat16)
+    q_out[blocks * BLOCK :, :] = picks[...]
+
+
+def project(kernel, rows, at, *arrays):
+    blocks = arrays[0].shape[0] // BLOCK
+    return pl.pallas_call(
+        functools.partial(kernel, blocks),
+        out_shape=VMEM((rows, 128), jnp.bfloat16),
+        in_specs=[full(SMEM)] + [full()] * len(arrays),
+        out_specs=full(),
+        compiler_params=PARAMS,
+    )(at, *[vmem(a) for a in arrays])
 
 
 def spread_heads(rows, lane):
@@ -186,25 +194,17 @@
             out[p][blocks * 64 :, :] = jnp.concatenate(stats, axis=0).astype(jnp.bfloat16)
 
 
-def attend(table, begin, q, kv, carry, last):
-    rows = q[0].shape[0]
-    blocks = rows // BLOCK
-    groups = Y * blocks
-    state = [jax.ShapeDtypeStruct((groups, BLOCK + 16, 128), jnp.float32)]
-    if last:
-        outs = [jax.ShapeDtypeStruct((rows + 8 * blocks, 128), jnp.bfloat16)] * Y
-        scratch = [VMEM(s.shape, s.dtype) for s in state]
-    else:
-        outs, scratch = state, []
-    outs = [VMEM(s.shape, s.dtype) for s in outs]
+def attend(table, begin, q, kv, carry, last, blocks):
+    rows = blocks * BLOCK
+    state = VMEM((Y * blocks, BLOCK + 16, 128), jnp.float32)
+    outs = [VMEM((rows + 8 * blocks, 128), jnp.bfloat16)] * Y if last else [state]
     args = [table] + [vmem(a) for a in (*q, *kv, *carry)]
     return pl.pallas_call(
         functools.partial(attend_kernel, blocks, len(kv), begin, last),
         out_shape=tuple(outs),
         in_specs=[full(SMEM)] + [full()] * (len(args) - 1),
         out_specs=(full(),) * len(outs),
-        scratch_shapes=scratch,
-        name="attend_late" if last else "attend_early",
+        scratch_shapes=[state] if last else [],
         compiler_params=PARAMS,
     )(*args)
 
@@ -279,9 +279,6 @@
     pieces = [tokens] + [lax.ppermute(tokens, "x", shift(X, s)) for s in (1, 2, 3)]
     at = jnp.stack([(x - s) % X for s in range(X)]).astype(jnp.int32)
 
-    picked = chosen_owner * 8 + chosen_local
-    picks = [picked] + [lax.ppermute(picked, "y", shift(Y, s)) for s in (1, 2, 3)]
-
     width = out_weight.shape[1] // X
     gained = []
     for s in range(X):
@@ -290,7 +287,12 @@
     weights = [gained[0]] + [lax.ppermute(gained[s], "x", shift(X, s)) for s in (1, 2, 3)]
 
     staged, weight = stage(tokens, (query_weight, key_weight, value_weight))
-    q, kv = project(at, [staged] + pieces[1:], weight)
+    pieces[0] = staged
+    kv = project(project_kernel, 2 * rows, at, *pieces, weight)
+    chosen = jnp.stack([chosen_owner.reshape(-1), chosen_local.reshape(-1)])
+    count = chosen.shape[1]
+    chosen = jnp.pad(chosen.astype(jnp.bfloat16), ((0, 14), (0, 128 - count)))
+    q = project(query_kernel, rows + 16, at, *pieces, weight, chosen)
 
     places = [(i, j) for i in range(Z) for j in range(C)]
 
@@ -303,10 +305,11 @@
     same, cross = [kv], [swap(kv)]
     held = [(0, 0, kv), (0, 1, cross[0])]
     for step in (1, 2, 3):
-        same.append(lax.ppermute(same[-1], ("z", "c"), onward(1)))
-        cross.append(lax.ppermute(cross[-1], ("z", "c"), onward(1)))
-        held += [(step, 0, same[-1]), (step, 1, cross[-1])]
-        held += [(-step, 1, swap(same[-1])), (-step, 0, swap(cross[-1]))]
+        reach = (0, 1, 2, 1)[step]
+        same.append(lax.ppermute(same[step - reach], ("z", "c"), onward(reach)))
+        cross.append(lax.ppermute(cross[step - reach], ("z", "c"), onward(reach)))
+        held += [(step, 0, same[-1]), (-step, 1, swap(same[-1]))]
+        held += [(step, 1, cross[-1]), (-step, 0, swap(cross[-1]))]
     far = lax.ppermute(same[2], ("z", "c"), onward(2))
     held += [(4, 0, far), (4, 1, swap(far))]
 
@@ -316,17 +319,18 @@
     column = jnp.stack(
         [((z + toward * d) % Z) * (Y * C) + y * C + (c ^ cc) for d, cc, _ in held]
     ).astype(jnp.int32)
-    picks = jnp.stack(picks).reshape(Y, 1, -1)
-    chosen = chosen_owner.shape[1]
-    row = jnp.arange(blocks * chosen, dtype=jnp.int32) // chosen
-    code = 1 + 8 * row + (picks & 7)
-    hit = (picks >> 3) == column[None, :, None]
-    table = jnp.sum(jnp.where(hit, code, 0), axis=2).reshape(-1)
-
-    early = 10
+    picks = [a[rows:].astype(jnp.float32).astype(jnp.int32) for a in queries]
+    owner = jnp.stack([a[0, :count] for a in picks])[:, None, :]
+    local = jnp.stack([a[1, :count] for a in picks])[:, None, :]
+    row = jnp.arange(count, dtype=jnp.int32) // chosen_owner.shape[1]
+    hit = owner == column[None, :, None]
+    table = jnp.sum(jnp.where(hit, 1 + 8 * row + local, 0), axis=2).reshape(-1)
+
     arrays = [a for _, _, a in held]
-    carry = attend(table, 0, queries, arrays[:early], (), False)
-    parts = attend(table, early, queries, arrays[early:], carry, True)
+    carry, begin = (), 0
+    for name, end in (("early", 10), ("middle", 12), ("late", Z * C)):
+        parts = attend(table, begin, queries, arrays[begin:end], carry, name == "late", blocks)
+        carry, begin = parts[-1:], end
 
     back = [parts[0]] + [lax.ppermute(parts[s], "y", shift(Y, -s)) for s in (1, 2, 3)]
     attended = merge(back, blocks)

time: 83.2 us -> 83.5 us (level)
  the two profiles are of different devices: /device:TPU:1 before, /device:TPU:6 now
where the time goes in v2:
time: 83.5 us; the launch traced here: 83.3 us
  starting transfers between devices  36.1 us (43%)
  waiting for transfers between devices  35.5 us (43%)
  Pallas kernels  9.43 us (11%)
  local copies, waits for them, and re-layouts  1.67 us (2%)
    ppermute x3, waiting for transfers between devices, on_device(): cross.append(lax.ppermute(cross[step - reach], ('z', 'c'), onward(reach)))  8.41 us
    ppermute x3, starting transfers between devices, on_device(): same.append(lax.ppermute(same[step - reach], ('z', 'c'), onward(reach)))  6.96 us
    ppermute x3, waiting for transfers between devices, on_device(): lax.ppermute(parts[s], 'y', shift(Y, -s))  6.63 us
    ppermute x3, waiting for transfers between devices, on_device(): lax.ppermute(tokens, 'x', shift(X, s))  6.5 us
    ppermute x3, starting transfers between devices, on_device(): queries = [q] + [lax.ppermute(q, 'y', shift(Y, s)) for s in (1, 2, 3)]  6.42 us
    ppermute x3, starting transfers between devices, on_device(): cross.append(lax.ppermute(cross[step - reach], ('z', 'c'), onward(reach)))  5.38 us
    ppermute x3, waiting for transfers between devices, on_device(): queries = [q] + [lax.ppermute(q, 'y', shift(Y, s)) for s in (1, 2, 3)]  5.06 us
    ppermute x3, starting transfers between devices, on_device(): lax.ppermute(gained[s], 'x', shift(X, s))  5.01 us
  transfers between devices with their start and end apart: 30, of which 15 were waited for; matrix products, arithmetic and copies ran while one was open for 1% of the time, Pallas kernels for 7%

profile of v2, /device:TPU:6, one launch (start us, length us, event | category | flops | bytes accessed | tf_op | source)
XLA Modules:
  0.0 83.3 jit_solution(6574244596288965711)
XLA Ops:
  0.0 2.2 %collective-permute-start = (bf16[384,256]{1,0:T(8,128)(2,1)}, bf16[384,256]{1,0:T(8,128)(2,1)S(1)}, u32[]{:S(2)}, u32[]{:S(2)}) collective-permute-start(bf16[384,256]{1,0:T(8,128)(2,1)} %tokens.1), channel_id=1, source_target_pairs={{0,1},{1,2},{2,3},{3,0},{4,5},{5,6},{6,7},{7,4},{8,9},{9,10},{10,1... | collective-permute-start | bytes 589832 | tf_op jit(solution)/shard_map/ppermute | solution.py:279
  6.1 1.9 %collective-permute-done.t1 = bf16[384,256]{1,0:T(8,128)(2,1)S(1)} collective-permute-done((bf16[384,256]{1,0:T(8,128)(2,1)}, bf16[384,256]{1,0:T(8,128)(2,1)S(1)}, u32[]{:S(2)}, u32[]{:S(2)}) %collective-permute-start) | collective-permute-done | bytes 196640 | tf_op jit(solution)/shard_map/ppermute | solution.py:279
  8.0 2.6 %collective-permute-done.1.t2 = bf16[384,256]{1,0:T(8,128)(2,1)S(1)} collective-permute-done((bf16[384,256]{1,0:T(8,128)(2,1)}, bf16[384,256]{1,0:T(8,128)(2,1)S(1)}, u32[]{:S(2)}, u32[]{:S(2)}) %collective-permute-start.1) | collective-permute-done | bytes 196640 | tf_op jit(solution)/shard_map/ppermute | solution.py:279
  10.6 2.0 %collective-permute-done.2.t3 = bf16[384,256]{1,0:T(8,128)(2,1)S(1)} collective-permute-done((bf16[384,256]{1,0:T(8,128)(2,1)}, bf16[384,256]{1,0:T(8,128)(2,1)S(1)}, u32[]{:S(2)}, u32[]{:S(2)}) %collective-permute-start.2) | collective-permute-done | bytes 196640 | tf_op jit(solution)/shard_map/ppermute | solution.py:279
  13.8 2.2 %collective-permute-start.15 = (bf16[768,128]{1,0:T(8,128)(2,1)S(1)}, bf16[768,128]{1,0:T(8,128)(2,1)S(1)}, u32[]{:S(2)}, u32[]{:S(2)}) collective-permute-start(bf16[768,128]{1,0:T(8,128)(2,1)S(1)} %shard_map.83.refs_5_), channel_id=1, source_target_pairs={{0,32},{4,228},{32,64},{36,4},{64,96},{68,36},{96,128},{100,68},{1... | collective-permute-start | bytes 589832 | tf_op jit(solution)/shard_map/ppermute | solution.py:309
  16.0 3.3 %collective-permute-start.10 = (bf16[768,128]{1,0:T(8,128)(2,1)S(1)}, bf16[768,128]{1,0:T(8,128)(2,1)S(1)}, u32[]{:S(2)}, u32[]{:S(2)}) collective-permute-start(bf16[768,128]{1,0:T(8,128)(2,1)S(1)} %shard_map.83.refs_5_), channel_id=1, source_target_pairs={{0,64},{4,196},{32,96},{36,228},{64,128},{68,4},{96,160},{100,36},... | collective-permute-start | bytes 589832 | tf_op jit(solution)/shard_map/ppermute | solution.py:309
  20.4 1.7 %collective-permute-start.3 = (bf16[400,128]{1,0:T(8,128)(2,1)S(1)}, bf16[400,128]{1,0:T(8,128)(2,1)S(1)}, u32[]{:S(2)}, u32[]{:S(2)}) collective-permute-start(bf16[400,128]{1,0:T(8,128)(2,1)S(1)} %shard_map.82.refs_1_), channel_id=1, source_target_pairs={{0,8},{8,16},{16,24},{24,0},{1,9},{9,17},{17,25},{25,1},{2,10},{10... | collective-permute-start | bytes 307208 | tf_op jit(solution)/shard_map/ppermute | solution.py:316
  22.1 2.9 %collective-permute-start.4 = (bf16[400,128]{1,0:T(8,128)(2,1)S(1)}, bf16[400,128]{1,0:T(8,128)(2,1)S(1)}, u32[]{:S(2)}, u32[]{:S(2)}) collective-permute-start(bf16[400,128]{1,0:T(8,128)(2,1)S(1)} %shard_map.82.refs_1_), channel_id=1, source_target_pairs={{0,16},{8,24},{16,0},{24,8},{1,17},{9,25},{17,1},{25,9},{2,18},{10... | collective-permute-start | bytes 307208 | tf_op jit(solution)/shard_map/ppermute | solution.py:316
  26.4 1.9 %collective-permute-start.5 = (bf16[400,128]{1,0:T(8,128)(2,1)S(1)}, bf16[400,128]{1,0:T(8,128)(2,1)S(1)}, u32[]{:S(2)}, u32[]{:S(2)}) collective-permute-start(bf16[400,128]{1,0:T(8,128)(2,1)S(1)} %shard_map.82.refs_1_), channel_id=1, source_target_pairs={{0,24},{8,0},{16,8},{24,16},{1,25},{9,1},{17,9},{25,17},{2,26},{10... | collective-permute-start | bytes 307208 | tf_op jit(solution)/shard_map/ppermute | solution.py:316
  28.3 1.6 %collective-permute-done.4.refs_3_ = bf16[400,128]{1,0:T(8,128)(2,1)S(1)} collective-permute-done((bf16[400,128]{1,0:T(8,128)(2,1)S(1)}, bf16[400,128]{1,0:T(8,128)(2,1)S(1)}, u32[]{:S(2)}, u32[]{:S(2)}) %collective-permute-start.4) | collective-permute-done | bytes 102432 | tf_op jit(solution)/shard_map/ppermute | solution.py:316
  29.9 2.0 %collective-permute-done.5.refs_4_ = bf16[400,128]{1,0:T(8,128)(2,1)S(1)} collective-permute-done((bf16[400,128]{1,0:T(8,128)(2,1)S(1)}, bf16[400,128]{1,0:T(8,128)(2,1)S(1)}, u32[]{:S(2)}, u32[]{:S(2)}) %collective-permute-start.5) | collective-permute-done | bytes 102432 | tf_op jit(solution)/shard_map/ppermute | solution.py:316
  32.0 2.8 %collective-permute-start.17 = (bf16[768,128]{1,0:T(8,128)(2,1)S(1)}, bf16[768,128]{1,0:T(8,128)(2,1)S(1)}, u32[]{:S(2)}, u32[]{:S(2)}) collective-permute-start(bf16[768,128]{1,0:T(8,128)(2,1)S(1)} %collective-permute-done.6.refs_6_), channel_id=1, source_target_pairs={{0,32},{4,228},{32,64},{36,4},{64,96},{68,36},{96,128},{100,68},{1... | collective-permute-start | bytes 589832 | tf_op jit(solution)/shard_map/ppermute | solution.py:310
  35.8 1.5 %collective-permute-start.13 = (bf16[768,128]{1,0:T(8,128)(2,1)S(1)}, bf16[768,128]{1,0:T(8,128)(2,1)S(1)}, u32[]{:S(2)}, u32[]{:S(2)}) collective-permute-start(bf16[768,128]{1,0:T(8,128)(2,1)S(1)} %collective-permute-done.10.refs_11_), channel_id=1, source_target_pairs={{0,32},{4,228},{32,64},{36,4},{64,96},{68,36},{96,128},{100,68},{1... | collective-permute-start | bytes 589832 | tf_op jit(solution)/shard_map/ppermute | solution.py:309
  39.1 4.9 %collective-permute-done.7.refs_13_ = bf16[768,128]{1,0:T(8,128)(2,1)S(1)} collective-permute-done((bf16[768,128]{1,0:T(8,128)(2,1)S(1)}, bf16[768,128]{1,0:T(8,128)(2,1)S(1)}, u32[]{:S(2)}, u32[]{:S(2)}) %collective-permute-start.7) | collective-permute-done | bytes 196640 | tf_op jit(solution)/shard_map/ppermute | solution.py:310
  44.1 1.6 %collective-permute-start.8 = (bf16[768,128]{1,0:T(8,128)(2,1)S(1)}, bf16[768,128]{1,0:T(8,128)(2,1)S(1)}, u32[]{:S(2)}, u32[]{:S(2)}) collective-permute-start(bf16[768,128]{1,0:T(8,128)(2,1)S(1)} %collective-permute-done.7.refs_13_), channel_id=1, source_target_pairs={{0,32},{4,228},{32,64},{36,4},{64,96},{68,36},{96,128},{100,68},{1... | collective-permute-start | bytes 589832 | tf_op jit(solution)/shard_map/ppermute | solution.py:310
  46.4 4.0 %collective-permute-done.11.refs_7_ = bf16[768,128]{1,0:T(8,128)(2,1)S(1)} collective-permute-done((bf16[768,128]{1,0:T(8,128)(2,1)S(1)}, bf16[768,128]{1,0:T(8,128)(2,1)S(1)}, u32[]{:S(2)}, u32[]{:S(2)}) %collective-permute-start.11) | collective-permute-done | bytes 196640 | tf_op jit(solution)/shard_map/ppermute | solution.py:313
  50.4 2.2 %collective-permute-done.8.refs_5_ = bf16[768,128]{1,0:T(8,128)(2,1)S(1)} collective-permute-done((bf16[768,128]{1,0:T(8,128)(2,1)S(1)}, bf16[768,128]{1,0:T(8,128)(2,1)S(1)}, u32[]{:S(2)}, u32[]{:S(2)}) %collective-permute-start.8) | collective-permute-done | bytes 196640 | tf_op jit(solution)/shard_map/ppermute | solution.py:310
  53.0 1.8 %shard_map.84.refs_7_ = f32[24,80,128]{2,1,0:T(8,128)S(1)} custom-call(s32[64]{0:T(128)S(1)} %reshape.65.refs_0_, bf16[400,128]{1,0:T(8,128)(2,1)S(1)} %shard_map.82.refs_1_, bf16[400,128]{1,0:T(8,128)(2,1)S(1)} %collective-permute-done.3.refs_2_, bf16[400,128]{1,0:T(8,128)(2,1)S(1)} %collective-permute-done.4.refs_3_, ...), custom_call_target="tpu_custom_call" | custom-call | tf_op jit(solution)/shard_map/pallas_call | solution.py:202
  57.4 3.7 %collective-permute-start.21 = (bf16[432,128]{1,0:T(8,128)(2,1)S(1)}, bf16[432,128]{1,0:T(8,128)(2,1)S(1)}, u32[]{:S(2)}, u32[]{:S(2)}) collective-permute-start(bf16[432,128]{1,0:T(8,128)(2,1)S(1)} %get-tuple-element.14), channel_id=1, source_target_pairs={{0,24},{8,0},{16,8},{24,16},{1,25},{9,1},{17,9},{25,17},{2,26},{10... | collective-permute-start | bytes 331784 | tf_op jit(solution)/shard_map/ppermute | solution.py:335
  63.2 3.2 %collective-permute-done.21.refs_1_ = bf16[432,128]{1,0:T(8,128)(2,1)S(1)} collective-permute-done((bf16[432,128]{1,0:T(8,128)(2,1)S(1)}, bf16[432,128]{1,0:T(8,128)(2,1)S(1)}, u32[]{:S(2)}, u32[]{:S(2)}) %collective-permute-start.21) | collective-permute-done | bytes 110624 | tf_op jit(solution)/shard_map/ppermute | solution.py:335
  66.5 2.1 %collective-permute-done.22.refs_2_ = bf16[432,128]{1,0:T(8,128)(2,1)S(1)} collective-permute-done((bf16[432,128]{1,0:T(8,128)(2,1)S(1)}, bf16[432,128]{1,0:T(8,128)(2,1)S(1)}, u32[]{:S(2)}, u32[]{:S(2)}) %collective-permute-start.22) | collective-permute-done | bytes 110624 | tf_op jit(solution)/shard_map/ppermute | solution.py:335
  71.3 2.1 %collective-permute-start.25 = (bf16[384,128]{1,0:T(8,128)(2,1)S(1)}, bf16[384,128]{1,0:T(8,128)(2,1)S(1)}, u32[]{:S(2)}, u32[]{:S(2)}) collective-permute-start(bf16[384,128]{1,0:T(8,128)(2,1)S(1)} %merge.1.a0), channel_id=1, source_target_pairs={{0,2},{1,3},{2,0},{3,1},{4,6},{5,7},{6,4},{7,5},{8,10},{9,11},{10,... | collective-permute-start | bytes 294920 | tf_op jit(solution)/shard_map/ppermute | solution.py:337
  73.5 3.0 %collective-permute-start.28 = (bf16[128,256]{1,0:T(8,128)(2,1)S(1)}, bf16[128,256]{1,0:T(8,128)(2,1)S(1)}, u32[]{:S(2)}, u32[]{:S(2)}) collective-permute-start(bf16[128,256]{1,0:T(8,128)(2,1)S(1)} %get-tuple-element.20), channel_id=1, source_target_pairs={{0,2},{1,3},{2,0},{3,1},{4,6},{5,7},{6,4},{7,5},{8,10},{9,11},{10,... | collective-permute-start | bytes 196616 | tf_op jit(solution)/shard_map/ppermute | solution.py:287
  77.5 4.0 %collective-permute-done.28.w2 = bf16[128,256]{1,0:T(8,128)(2,1)S(1)} collective-permute-done((bf16[128,256]{1,0:T(8,128)(2,1)S(1)}, bf16[128,256]{1,0:T(8,128)(2,1)S(1)}, u32[]{:S(2)}, u32[]{:S(2)}) %collective-permute-start.28) | collective-permute-done | bytes 65568 | tf_op jit(solution)/shard_map/ppermute | solution.py:287
  (73 shorter events, 22.0 us)
Async XLA Ops:
  0.0 8.0 %collective-permute-start = (bf16[384,256]{1,0:T(8,128)(2,1)}, bf16[384,256]{1,0:T(8,128)(2,1)S(1)}, u32[]{:S(2)}, u32[]{:S(2)}) collective-permute-start(bf16[384,256]{1,0:T(8,128)(2,1)} %tokens.1), channel_id=1, source_target_pairs={{0,1},{1,2},{2,3},{3,0},{4,5},{5,6},{6,7},{7,4},{8,9},{9,10},{10,1... | collective-permute-start | bytes 589832 | tf_op jit(solution)/shard_map/ppermute | solution.py:279
  2.2 8.4 %collective-permute-start.1 = (bf16[384,256]{1,0:T(8,128)(2,1)}, bf16[384,256]{1,0:T(8,128)(2,1)S(1)}, u32[]{:S(2)}, u32[]{:S(2)}) collective-permute-start(bf16[384,256]{1,0:T(8,128)(2,1)} %tokens.1), channel_id=1, source_target_pairs={{0,2},{1,3},{2,0},{3,1},{4,6},{5,7},{6,4},{7,5},{8,10},{9,11},{10,... | collective-permute-start | bytes 589832 | tf_op jit(solution)/shard_map/ppermute | solution.py:279
  2.9 9.7 %collective-permute-start.2 = (bf16[384,256]{1,0:T(8,128)(2,1)}, bf16[384,256]{1,0:T(8,128)(2,1)S(1)}, u32[]{:S(2)}, u32[]{:S(2)}) collective-permute-start(bf16[384,256]{1,0:T(8,128)(2,1)} %tokens.1), channel_id=1, source_target_pairs={{0,3},{1,0},{2,1},{3,2},{4,7},{5,4},{6,5},{7,6},{8,11},{9,8},{10,9... | collective-permute-start | bytes 589832 | tf_op jit(solution)/shard_map/ppermute | solution.py:279
  13.7 18.2 %collective-permute-start.6 = (bf16[768,128]{1,0:T(8,128)(2,1)S(1)}, bf16[768,128]{1,0:T(8,128)(2,1)S(1)}, u32[]{:S(2)}, u32[]{:S(2)}) collective-permute-start(bf16[768,128]{1,0:T(8,128)(2,1)S(1)} %shard_map.83.refs_5_), channel_id=1, source_target_pairs={{0,4},{4,0},{1,5},{5,1},{2,6},{6,2},{3,7},{7,3},{8,12},{12,8},{9,1... | collective-permute-start | bytes 589832 | tf_op jit(solution)/shard_map/ppermute | solution.py:303
  13.8 23.4 %collective-permute-start.15 = (bf16[768,128]{1,0:T(8,128)(2,1)S(1)}, bf16[768,128]{1,0:T(8,128)(2,1)S(1)}, u32[]{:S(2)}, u32[]{:S(2)}) collective-permute-start(bf16[768,128]{1,0:T(8,128)(2,1)S(1)} %shard_map.83.refs_5_), channel_id=1, source_target_pairs={{0,32},{4,228},{32,64},{36,4},{64,96},{68,36},{96,128},{100,68},{1... | collective-permute-start | bytes 589832 | tf_op jit(solution)/shard_map/ppermute | solution.py:309
  16.0 19.7 %collective-permute-start.10 = (bf16[768,128]{1,0:T(8,128)(2,1)S(1)}, bf16[768,128]{1,0:T(8,128)(2,1)S(1)}, u32[]{:S(2)}, u32[]{:S(2)}) collective-permute-start(bf16[768,128]{1,0:T(8,128)(2,1)S(1)} %shard_map.83.refs_5_), channel_id=1, source_target_pairs={{0,64},{4,196},{32,96},{36,228},{64,128},{68,4},{96,160},{100,36},... | collective-permute-start | bytes 589832 | tf_op jit(solution)/shard_map/ppermute | solution.py:309
  22.1 7.8 %collective-permute-start.4 = (bf16[400,128]{1,0:T(8,128)(2,1)S(1)}, bf16[400,128]{1,0:T(8,128)(2,1)S(1)}, u32[]{:S(2)}, u32[]{:S(2)}) collective-permute-start(bf16[400,128]{1,0:T(8,128)(2,1)S(1)} %shard_map.82.refs_1_), channel_id=1, source_target_pairs={{0,16},{8,24},{16,0},{24,8},{1,17},{9,25},{17,1},{25,9},{2,18},{10... | collective-permute-start | bytes 307208 | tf_op jit(solution)/shard_map/ppermute | solution.py:316
  32.0 7.0 %collective-permute-start.17 = (bf16[768,128]{1,0:T(8,128)(2,1)S(1)}, bf16[768,128]{1,0:T(8,128)(2,1)S(1)}, u32[]{:S(2)}, u32[]{:S(2)}) collective-permute-start(bf16[768,128]{1,0:T(8,128)(2,1)S(1)} %collective-permute-done.6.refs_6_), channel_id=1, source_target_pairs={{0,32},{4,228},{32,64},{36,4},{64,96},{68,36},{96,128},{100,68},{1... | collective-permute-start | bytes 589832 | tf_op jit(solution)/shard_map/ppermute | solution.py:310
  34.8 9.3 %collective-permute-start.7 = (bf16[768,128]{1,0:T(8,128)(2,1)S(1)}, bf16[768,128]{1,0:T(8,128)(2,1)S(1)}, u32[]{:S(2)}, u32[]{:S(2)}) collective-permute-start(bf16[768,128]{1,0:T(8,128)(2,1)S(1)} %collective-permute-done.6.refs_6_), channel_id=1, source_target_pairs={{0,64},{4,196},{32,96},{36,228},{64,128},{68,4},{96,160},{100,36},... | collective-permute-start | bytes 589832 | tf_op jit(solution)/shard_map/ppermute | solution.py:310
  35.8 10.0 %collective-permute-start.19 = (bf16[768,128]{1,0:T(8,128)(2,1)S(1)}, bf16[768,128]{1,0:T(8,128)(2,1)S(1)}, u32[]{:S(2)}, u32[]{:S(2)}) collective-permute-start(bf16[768,128]{1,0:T(8,128)(2,1)S(1)} %collective-permute-done.10.refs_11_), channel_id=1, source_target_pairs={{0,4},{4,0},{1,5},{5,1},{2,6},{6,2},{3,7},{7,3},{8,12},{12,8},{9,1... | collective-permute-start | bytes 589832 | tf_op jit(solution)/shard_map/ppermute | solution.py:303
  35.8 10.5 %collective-permute-start.13 = (bf16[768,128]{1,0:T(8,128)(2,1)S(1)}, bf16[768,128]{1,0:T(8,128)(2,1)S(1)}, u32[]{:S(2)}, u32[]{:S(2)}) collective-permute-start(bf16[768,128]{1,0:T(8,128)(2,1)S(1)} %collective-permute-done.10.refs_11_), channel_id=1, source_target_pairs={{0,32},{4,228},{32,64},{36,4},{64,96},{68,36},{96,128},{100,68},{1... | collective-permute-start | bytes 589832 | tf_op jit(solution)/shard_map/ppermute | solution.py:309
  37.3 13.2 %collective-permute-start.11 = (bf16[768,128]{1,0:T(8,128)(2,1)S(1)}, bf16[768,128]{1,0:T(8,128)(2,1)S(1)}, u32[]{:S(2)}, u32[]{:S(2)}) collective-permute-start(bf16[768,128]{1,0:T(8,128)(2,1)S(1)} %collective-permute-done.10.refs_11_), channel_id=1, source_target_pairs={{0,64},{4,196},{32,96},{36,228},{64,128},{68,4},{96,160},{100,36},... | collective-permute-start | bytes 589832 | tf_op jit(solution)/shard_map/ppermute | solution.py:313
  44.1 8.6 %collective-permute-start.8 = (bf16[768,128]{1,0:T(8,128)(2,1)S(1)}, bf16[768,128]{1,0:T(8,128)(2,1)S(1)}, u32[]{:S(2)}, u32[]{:S(2)}) collective-permute-start(bf16[768,128]{1,0:T(8,128)(2,1)S(1)} %collective-permute-done.7.refs_13_), channel_id=1, source_target_pairs={{0,32},{4,228},{32,64},{36,4},{64,96},{68,36},{96,128},{100,68},{1... | collective-permute-start | bytes 589832 | tf_op jit(solution)/shard_map/ppermute | solution.py:310
  45.7 7.3 %collective-permute-start.20 = (bf16[768,128]{1,0:T(8,128)(2,1)S(1)}, bf16[768,128]{1,0:T(8,128)(2,1)S(1)}, u32[]{:S(2)}, u32[]{:S(2)}) collective-permute-start(bf16[768,128]{1,0:T(8,128)(2,1)S(1)} %collective-permute-done.7.refs_13_), channel_id=1, source_target_pairs={{0,4},{4,0},{1,5},{5,1},{2,6},{6,2},{3,7},{7,3},{8,12},{12,8},{9,1... | collective-permute-start | bytes 589832 | tf_op jit(solution)/shard_map/ppermute | solution.py:303
  45.8 7.1 %collective-permute-start.18 = (bf16[768,128]{1,0:T(8,128)(2,1)S(1)}, bf16[768,128]{1,0:T(8,128)(2,1)S(1)}, u32[]{:S(2)}, u32[]{:S(2)}) collective-permute-start(bf16[768,128]{1,0:T(8,128)(2,1)S(1)} %collective-permute-done.17.refs_9_), channel_id=1, source_target_pairs={{0,4},{4,0},{1,5},{5,1},{2,6},{6,2},{3,7},{7,3},{8,12},{12,8},{9,1... | collective-permute-start | bytes 589832 | tf_op jit(solution)/shard_map/ppermute | solution.py:303
  46.3 8.4 %collective-permute-start.14 = (bf16[768,128]{1,0:T(8,128)(2,1)S(1)}, bf16[768,128]{1,0:T(8,128)(2,1)}, u32[]{:S(2)}, u32[]{:S(2)}) collective-permute-start(bf16[768,128]{1,0:T(8,128)(2,1)S(1)} %collective-permute-done.13.refs_5_), channel_id=1, source_target_pairs={{0,4},{4,0},{1,5},{5,1},{2,6},{6,2},{3,7},{7,3},{8,12},{12,8},{9,1... | collective-permute-start | bytes 589832 | tf_op jit(solution)/shard_map/ppermute | solution.py:303
  57.4 9.1 %collective-permute-start.21 = (bf16[432,128]{1,0:T(8,128)(2,1)S(1)}, bf16[432,128]{1,0:T(8,128)(2,1)S(1)}, u32[]{:S(2)}, u32[]{:S(2)}) collective-permute-start(bf16[432,128]{1,0:T(8,128)(2,1)S(1)} %get-tuple-element.14), channel_id=1, source_target_pairs={{0,24},{8,0},{16,8},{24,16},{1,25},{9,1},{17,9},{25,17},{2,26},{10... | collective-permute-start | bytes 331784 | tf_op jit(solution)/shard_map/ppermute | solution.py:335
  61.1 7.5 %collective-permute-start.22 = (bf16[432,128]{1,0:T(8,128)(2,1)S(1)}, bf16[432,128]{1,0:T(8,128)(2,1)S(1)}, u32[]{:S(2)}, u32[]{:S(2)}) collective-permute-start(bf16[432,128]{1,0:T(8,128)(2,1)S(1)} %get-tuple-element.15), channel_id=1, source_target_pairs={{0,16},{8,24},{16,0},{24,8},{1,17},{9,25},{17,1},{25,9},{2,18},{10... | collective-permute-start | bytes 331784 | tf_op jit(solution)/shard_map/ppermute | solution.py:335
  61.1 8.8 %collective-permute-start.23 = (bf16[432,128]{1,0:T(8,128)(2,1)S(1)}, bf16[432,128]{1,0:T(8,128)(2,1)S(1)}, u32[]{:S(2)}, u32[]{:S(2)}) collective-permute-start(bf16[432,128]{1,0:T(8,128)(2,1)S(1)} %get-tuple-element.16), channel_id=1, source_target_pairs={{0,8},{8,16},{16,24},{24,0},{1,9},{9,17},{17,25},{25,1},{2,10},{10... | collective-permute-start | bytes 331784 | tf_op jit(solution)/shard_map/ppermute | solution.py:335
  62.2 14.3 %collective-permute-start.27 = (bf16[128,256]{1,0:T(8,128)(2,1)S(1)}, bf16[128,256]{1,0:T(8,128)(2,1)S(1)}, u32[]{:S(2)}, u32[]{:S(2)}) collective-permute-start(bf16[128,256]{1,0:T(8,128)(2,1)S(1)} %get-tuple-element.18), channel_id=1, source_target_pairs={{0,1},{1,2},{2,3},{3,0},{4,5},{5,6},{6,7},{7,4},{8,9},{9,10},{10,1... | collective-permute-start | bytes 196616 | tf_op jit(solution)/shard_map/ppermute | solution.py:287
  70.2 12.0 %collective-permute-start.24 = (bf16[384,128]{1,0:T(8,128)(2,1)S(1)}, bf16[384,128]{1,0:T(8,128)(2,1)S(1)}, u32[]{:S(2)}, u32[]{:S(2)}) collective-permute-start(bf16[384,128]{1,0:T(8,128)(2,1)S(1)} %merge.1.a0), channel_id=1, source_target_pairs={{0,1},{1,2},{2,3},{3,0},{4,5},{5,6},{6,7},{7,4},{8,9},{9,10},{10,1... | collective-permute-start | bytes 294920 | tf_op jit(solution)/shard_map/ppermute | solution.py:337
  71.3 11.0 %collective-permute-start.25 = (bf16[384,128]{1,0:T(8,128)(2,1)S(1)}, bf16[384,128]{1,0:T(8,128)(2,1)S(1)}, u32[]{:S(2)}, u32[]{:S(2)}) collective-permute-start(bf16[384,128]{1,0:T(8,128)(2,1)S(1)} %merge.1.a0), channel_id=1, source_target_pairs={{0,2},{1,3},{2,0},{3,1},{4,6},{5,7},{6,4},{7,5},{8,10},{9,11},{10,... | collective-permute-start | bytes 294920 | tf_op jit(solution)/shard_map/ppermute | solution.py:337
  73.4 8.9 %collective-permute-start.26 = (bf16[384,128]{1,0:T(8,128)(2,1)S(1)}, bf16[384,128]{1,0:T(8,128)(2,1)S(1)}, u32[]{:S(2)}, u32[]{:S(2)}) collective-permute-start(bf16[384,128]{1,0:T(8,128)(2,1)S(1)} %merge.1.a0), channel_id=1, source_target_pairs={{0,3},{1,0},{2,1},{3,2},{4,7},{5,4},{6,5},{7,6},{8,11},{9,8},{10,9... | collective-permute-start | bytes 294920 | tf_op jit(solution)/shard_map/ppermute | solution.py:337
  73.5 8.0 %collective-permute-start.28 = (bf16[128,256]{1,0:T(8,128)(2,1)S(1)}, bf16[128,256]{1,0:T(8,128)(2,1)S(1)}, u32[]{:S(2)}, u32[]{:S(2)}) collective-permute-start(bf16[128,256]{1,0:T(8,128)(2,1)S(1)} %get-tuple-element.20), channel_id=1, source_target_pairs={{0,2},{1,3},{2,0},{3,1},{4,6},{5,7},{6,4},{7,5},{8,10},{9,11},{10,... | collective-permute-start | bytes 196616 | tf_op jit(solution)/shard_map/ppermute | solution.py:287
  (10 other events, 41.6 us)

commit v3 on v2

--- a/solution.py
+++ b/solution.py
@@ -16,7 +16,6 @@
 lowest = -1e30
 eps_norm = 1e-06
 VMEM = pltpu.VMEM
-SMEM = pltpu.SMEM
 
 
 PARAMS = pltpu.CompilerParams(vmem_limit_bytes=16 * 1024 * 1024)
@@ -43,38 +42,44 @@
     return jnp.concatenate([rows[:, :HEAD_SIZE], rows[:, HEAD_SIZE:]], axis=0).T
 
 
-def stage_kernel(tokens, wq, wk, wv, tokens_out, w_out):
-    tokens_out[...] = tokens[...]
+def stage_kernel(tokens, wq, wk, wv, w_out, total_out):
     for i, ref in enumerate((wq, wk, wv)):
         w_out[:, i * 128 : i * 128 + 128] = ref[...]
+    total_out[...] = term_of(0, tokens, w_out, slice(0, 384))
 
 
 def stage(tokens, weights):
     depth, width = weights[0].shape
+    arrays = [pltpu.with_memory_space_constraint(a, pltpu.HBM) for a in (tokens, *weights)]
     return pl.pallas_call(
         stage_kernel,
         out_shape=(
-            VMEM(tokens.shape, tokens.dtype),
             VMEM((depth, 3 * width), jnp.bfloat16),
+            VMEM((tokens.shape[0], 3 * width), jnp.float32),
         ),
         in_specs=[full()] * 4,
         out_specs=(full(),) * 2,
         name="stage",
         compiler_params=PARAMS,
-    )(*[pltpu.with_memory_space_constraint(a, pltpu.HBM) for a in (tokens, *weights)])
-
-
-def summed(at, pieces, weight, columns):
-    total = None
-    for s, piece in enumerate(pieces):
-        rows = pl.ds(pl.multiple_of(at[s] * 256, 256), 256)
-        term = jnp.dot(piece[...], weight[rows, columns], preferred_element_type=jnp.float32)
-        total = term if total is None else total + term
+    )(*arrays)
+
+
+def term_of(back, piece, weight, columns):
+    place = (lax.axis_index("x") + (X - back)) & (X - 1)
+    depth = piece.shape[1]
+    rows = pl.ds(pl.multiple_of(place * depth, depth), depth)
+    return jnp.dot(piece[...], weight[rows, columns], preferred_element_type=jnp.float32)
+
+
+def summed(total, pieces, weight, columns):
+    total = total[:, columns]
+    for s, piece in enumerate(pieces, 1):
+        total = total + term_of(s, piece, weight, columns)
     return total
 
 
-def project_kernel(blocks, at, t0, t1, t2, t3, weight, kv_out):
-    total = summed(at, (t0, t1, t2, t3), weight, slice(128, 384))
+def project_kernel(blocks, t0, t1, t2, t3, weight, kv_out):
+    total = summed(t0, (t1, t2, t3), weight, slice(128, 384))
     half = blocks * BLOCK
     kv_out[:half, :] = total[:, :128].astype(jnp.bfloat16)
     for b in range(blocks):
@@ -82,8 +87,8 @@
         kv_out[half + b * 64 : half + b * 64 + 64, :] = turned.astype(jnp.bfloat16)
 
 
-def query_kernel(blocks, at, t0, t1, t2, t3, weight, picks, q_out):
-    total = summed(at, (t0, t1, t2, t3), weight, slice(0, 128))
+def query_kernel(blocks, t0, t1, t2, t3, weight, picks, q_out):
+    total = summed(t0, (t1, t2, t3), weight, slice(0, 128))
     total = total.astype(jnp.bfloat16).astype(jnp.float32) * (HEAD_SIZE ** (-0.5))
     for b in range(blocks):
         here = slice(b * 64, b * 64 + 64)
@@ -91,15 +96,15 @@
     q_out[blocks * BLOCK :, :] = picks[...]
 
 
-def project(kernel, rows, at, *arrays):
+def project(kernel, rows, *arrays):
     blocks = arrays[0].shape[0] // BLOCK
     return pl.pallas_call(
         functools.partial(kernel, blocks),
         out_shape=VMEM((rows, 128), jnp.bfloat16),
-        in_specs=[full(SMEM)] + [full()] * len(arrays),
+        in_specs=[full()] * len(arrays),
         out_specs=full(),
         compiler_params=PARAMS,
-    )(at, *[vmem(a) for a in arrays])
+    )(*[vmem(a) for a in arrays])
 
 
 def spread_heads(rows, lane):
@@ -125,7 +130,7 @@
 def attend_kernel(blocks, owners, begin, last, *refs):
     refs = list(refs)
     first = begin == 0
-    table = refs.pop(0)
+    table = refs.pop(0)[...]
     q = [refs.pop(0) for _ in range(Y)]
     kv = [refs.pop(0) for _ in range(owners)]
     half = blocks * BLOCK
@@ -156,7 +161,7 @@
     for owner in range(owners):
         found = []
         for p in range(Y):
-            code = table[p * (Z * C) + begin + owner]
+            code = table[p, begin + owner]
             row = jnp.maximum(code - 1, 0)
             local = pl.multiple_of((row & 7) * BLOCK, BLOCK)
             row = row >> 3
@@ -198,11 +203,11 @@
     rows = blocks * BLOCK
     state = VMEM((Y * blocks, BLOCK + 16, 128), jnp.float32)
     outs = [VMEM((rows + 8 * blocks, 128), jnp.bfloat16)] * Y if last else [state]
-    args = [table] + [vmem(a) for a in (*q, *kv, *carry)]
+    args = [vmem(a) for a in (table, *q, *kv, *carry)]
     return pl.pallas_call(
         functools.partial(attend_kernel, blocks, len(kv), begin, last),
         out_shape=tuple(outs),
-        in_specs=[full(SMEM)] + [full()] * (len(args) - 1),
+        in_specs=[full()] * len(args),
         out_specs=(full(),) * len(outs),
         scratch_shapes=[state] if last else [],
         compiler_params=PARAMS,
@@ -277,7 +282,6 @@
     x, z, y, c = (lax.axis_index(name) for name in ("x", "z", "y", "c"))
 
     pieces = [tokens] + [lax.ppermute(tokens, "x", shift(X, s)) for s in (1, 2, 3)]
-    at = jnp.stack([(x - s) % X for s in range(X)]).astype(jnp.int32)
 
     width = out_weight.shape[1] // X
     gained = []
@@ -286,13 +290,12 @@
         gained.append((columns.astype(jnp.float32) * norm_gain[:, None]).astype(jnp.bfloat16))
     weights = [gained[0]] + [lax.ppermute(gained[s], "x", shift(X, s)) for s in (1, 2, 3)]
 
-    staged, weight = stage(tokens, (query_weight, key_weight, value_weight))
-    pieces[0] = staged
-    kv = project(project_kernel, 2 * rows, at, *pieces, weight)
+    weight, pieces[0] = stage(tokens, (query_weight, key_weight, value_weight))
+    kv = project(project_kernel, 2 * rows, *pieces, weight)
     chosen = jnp.stack([chosen_owner.reshape(-1), chosen_local.reshape(-1)])
     count = chosen.shape[1]
     chosen = jnp.pad(chosen.astype(jnp.bfloat16), ((0, 14), (0, 128 - count)))
-    q = project(query_kernel, rows + 16, at, *pieces, weight, chosen)
+    q = project(query_kernel, rows + 16, *pieces, weight, chosen)
 
     places = [(i, j) for i in range(Z) for j in range(C)]
 
@@ -312,6 +315,7 @@
         held += [(step, 1, cross[-1]), (-step, 0, swap(cross[-1]))]
     far = lax.ppermute(same[2], ("z", "c"), onward(2))
     held += [(4, 0, far), (4, 1, swap(far))]
+    held[13], held[14] = held[14], held[13]
 
     queries = [q] + [lax.ppermute(q, "y", shift(Y, s)) for s in (1, 2, 3)]
 
@@ -324,11 +328,11 @@
     local = jnp.stack([a[1, :count] for a in picks])[:, None, :]
     row = jnp.arange(count, dtype=jnp.int32) // chosen_owner.shape[1]
     hit = owner == column[None, :, None]
-    table = jnp.sum(jnp.where(hit, 1 + 8 * row + local, 0), axis=2).reshape(-1)
+    table = jnp.sum(jnp.where(hit, 1 + 8 * row + local, 0), axis=2)
 
     arrays = [a for _, _, a in held]
     carry, begin = (), 0
-    for name, end in (("early", 10), ("middle", 12), ("late", Z * C)):
+    for name, end in (("early", 10), ("middle", 12), ("nearly", 14), ("late", Z * C)):
         parts = attend(table, begin, queries, arrays[begin:end], carry, name == "late", blocks)
         carry, begin = parts[-1:], end
 

time: 83.5 us -> 74.9 us (0.90)
  the two profiles are of different devices: /device:TPU:6 before, /device:TPU:8 now
where the time goes in v3:
time: 74.9 us; the launch traced here: 73.8 us
  starting transfers between devices  41.7 us (56%)
  waiting for transfers between devices  22.7 us (30%)
  Pallas kernels  7.12 us (10%)
  local copies, waits for them, and re-layouts  1.58 us (2%)
    ppermute x3, starting transfers between devices, on_device(): same.append(lax.ppermute(same[step - reach], ('z', 'c'), onward(reach)))  7.18 us
    ppermute x3, waiting for transfers between devices, on_device(): cross.append(lax.ppermute(cross[step - reach], ('z', 'c'), onward(reach)))  6.89 us
    ppermute x3, starting transfers between devices, on_device(): lax.ppermute(tokens, 'x', shift(X, s))  5.65 us
    ppermute x3, starting transfers between devices, on_device(): lax.ppermute(attended, 'x', shift(X, s))  5.37 us
    ppermute x3, waiting for transfers between devices, on_device(): lax.ppermute(parts[s], 'y', shift(Y, -s))  5.21 us
    ppermute x3, starting transfers between devices, on_device(): queries = [q] + [lax.ppermute(q, 'y', shift(Y, s)) for s in (1, 2, 3)]  5 us
    ppermute x8, starting transfers between devices, swap(): return lax.ppermute(a, 'c', [(0, 1), (1, 0)])  4.86 us
    ppermute x3, starting transfers between devices, on_device(): cross.append(lax.ppermute(cross[step - reach], ('z', 'c'), onward(reach)))  4.68 us
  transfers between devices with their start and end apart: 30, of which 12 were waited for; matrix products, arithmetic and copies ran while one was open for 1% of the time, Pallas kernels for 7%

profile of v3, /device:TPU:8, one launch (start us, length us, event | category | flops | bytes accessed | tf_op | source)
XLA Modules:
  0.0 73.8 jit_solution(15146768844106458161)
XLA Ops:
  0.0 1.5 %collective-permute-start = (bf16[384,256]{1,0:T(8,128)(2,1)}, bf16[384,256]{1,0:T(8,128)(2,1)S(1)}, u32[]{:S(2)}, u32[]{:S(2)}) collective-permute-start(bf16[384,256]{1,0:T(8,128)(2,1)} %tokens.1), channel_id=1, source_target_pairs={{0,1},{1,2},{2,3},{3,0},{4,5},{5,6},{6,7},{7,4},{8,9},{9,10},{10,1... | collective-permute-start | bytes 589832 | tf_op jit(solution)/shard_map/ppermute | solution.py:284
  1.5 2.7 %collective-permute-start.1 = (bf16[384,256]{1,0:T(8,128)(2,1)}, bf16[384,256]{1,0:T(8,128)(2,1)S(1)}, u32[]{:S(2)}, u32[]{:S(2)}) collective-permute-start(bf16[384,256]{1,0:T(8,128)(2,1)} %tokens.1), channel_id=1, source_target_pairs={{0,2},{1,3},{2,0},{3,1},{4,6},{5,7},{6,4},{7,5},{8,10},{9,11},{10,... | collective-permute-start | bytes 589832 | tf_op jit(solution)/shard_map/ppermute | solution.py:284
  4.2 1.4 %collective-permute-start.2 = (bf16[384,256]{1,0:T(8,128)(2,1)}, bf16[384,256]{1,0:T(8,128)(2,1)S(1)}, u32[]{:S(2)}, u32[]{:S(2)}) collective-permute-start(bf16[384,256]{1,0:T(8,128)(2,1)} %tokens.1), channel_id=1, source_target_pairs={{0,3},{1,0},{2,1},{3,2},{4,7},{5,4},{6,5},{7,6},{8,11},{9,8},{10,9... | collective-permute-start | bytes 589832 | tf_op jit(solution)/shard_map/ppermute | solution.py:284
  7.1 1.6 %stage.1 = (bf16[1024,384]{1,0:T(8,128)(2,1)S(1)}, f32[384,384]{1,0:T(8,128)S(1)}) custom-call(bf16[384,256]{1,0:T(8,128)(2,1)} %tokens.1, bf16[1024,128]{1,0:T(8,128)(2,1)} %wq.1, bf16[1024,128]{1,0:T(8,128)(2,1)} %wk.1, bf16[1024,128]{1,0:T(8,128)(2,1)} %wv.1), custom_call_target="tpu_custom_call" | custom-call | tf_op jit(solution)/shard_map/stage/pallas_call | solution.py:54
  8.9 4.4 %collective-permute-done.1.t2 = bf16[384,256]{1,0:T(8,128)(2,1)S(1)} collective-permute-done((bf16[384,256]{1,0:T(8,128)(2,1)}, bf16[384,256]{1,0:T(8,128)(2,1)S(1)}, u32[]{:S(2)}, u32[]{:S(2)}) %collective-permute-start.1) | collective-permute-done | bytes 196640 | tf_op jit(solution)/shard_map/ppermute | solution.py:284
  13.8 1.7 %collective-permute-start.3 = (bf16[400,128]{1,0:T(8,128)(2,1)S(1)}, bf16[400,128]{1,0:T(8,128)(2,1)S(1)}, u32[]{:S(2)}, u32[]{:S(2)}) collective-permute-start(bf16[400,128]{1,0:T(8,128)(2,1)S(1)} %shard_map.82.refs_1_), channel_id=1, source_target_pairs={{0,8},{8,16},{16,24},{24,0},{1,9},{9,17},{17,25},{25,1},{2,10},{10... | collective-permute-start | bytes 307208 | tf_op jit(solution)/shard_map/ppermute | solution.py:320
  16.4 2.4 %collective-permute-start.5 = (bf16[400,128]{1,0:T(8,128)(2,1)S(1)}, bf16[400,128]{1,0:T(8,128)(2,1)S(1)}, u32[]{:S(2)}, u32[]{:S(2)}) collective-permute-start(bf16[400,128]{1,0:T(8,128)(2,1)S(1)} %shard_map.82.refs_1_), channel_id=1, source_target_pairs={{0,24},{8,0},{16,8},{24,16},{1,25},{9,1},{17,9},{25,17},{2,26},{10... | collective-permute-start | bytes 307208 | tf_op jit(solution)/shard_map/ppermute | solution.py:320
  19.5 3.3 %collective-permute-start.10 = (bf16[768,128]{1,0:T(8,128)(2,1)S(1)}, bf16[768,128]{1,0:T(8,128)(2,1)S(1)}, u32[]{:S(2)}, u32[]{:S(2)}) collective-permute-start(bf16[768,128]{1,0:T(8,128)(2,1)S(1)} %shard_map.83.refs_5_), channel_id=1, source_target_pairs={{0,64},{4,196},{32,96},{36,228},{64,128},{68,4},{96,160},{100,36},... | collective-permute-start | bytes 589832 | tf_op jit(solution)/shard_map/ppermute | solution.py:312
  22.9 1.9 %collective-permute-start.15 = (bf16[768,128]{1,0:T(8,128)(2,1)S(1)}, bf16[768,128]{1,0:T(8,128)(2,1)S(1)}, u32[]{:S(2)}, u32[]{:S(2)}) collective-permute-start(bf16[768,128]{1,0:T(8,128)(2,1)S(1)} %shard_map.83.refs_5_), channel_id=1, source_target_pairs={{0,32},{4,228},{32,64},{36,4},{64,96},{68,36},{96,128},{100,68},{1... | collective-permute-start | bytes 589832 | tf_op jit(solution)/shard_map/ppermute | solution.py:312
  24.8 3.7 %collective-permute-start.7 = (bf16[768,128]{1,0:T(8,128)(2,1)S(1)}, bf16[768,128]{1,0:T(8,128)(2,1)S(1)}, u32[]{:S(2)}, u32[]{:S(2)}) collective-permute-start(bf16[768,128]{1,0:T(8,128)(2,1)S(1)} %collective-permute-done.6.refs_6_), channel_id=1, source_target_pairs={{0,64},{4,196},{32,96},{36,228},{64,128},{68,4},{96,160},{100,36},... | collective-permute-start | bytes 589832 | tf_op jit(solution)/shard_map/ppermute | solution.py:313
  30.7 1.9 %collective-permute-start.13 = (bf16[768,128]{1,0:T(8,128)(2,1)S(1)}, bf16[768,128]{1,0:T(8,128)(2,1)S(1)}, u32[]{:S(2)}, u32[]{:S(2)}) collective-permute-start(bf16[768,128]{1,0:T(8,128)(2,1)S(1)} %collective-permute-done.10.refs_11_), channel_id=1, source_target_pairs={{0,32},{4,228},{32,64},{36,4},{64,96},{68,36},{96,128},{100,68},{1... | collective-permute-start | bytes 589832 | tf_op jit(solution)/shard_map/ppermute | solution.py:312
  33.3 1.5 %collective-permute-start.11 = (bf16[768,128]{1,0:T(8,128)(2,1)S(1)}, bf16[768,128]{1,0:T(8,128)(2,1)S(1)}, u32[]{:S(2)}, u32[]{:S(2)}) collective-permute-start(bf16[768,128]{1,0:T(8,128)(2,1)S(1)} %collective-permute-done.10.refs_11_), channel_id=1, source_target_pairs={{0,64},{4,196},{32,96},{36,228},{64,128},{68,4},{96,160},{100,36},... | collective-permute-start | bytes 589832 | tf_op jit(solution)/shard_map/ppermute | solution.py:316
  34.7 1.8 %collective-permute-done.7.refs_13_ = bf16[768,128]{1,0:T(8,128)(2,1)S(1)} collective-permute-done((bf16[768,128]{1,0:T(8,128)(2,1)S(1)}, bf16[768,128]{1,0:T(8,128)(2,1)S(1)}, u32[]{:S(2)}, u32[]{:S(2)}) %collective-permute-start.7) | collective-permute-done | bytes 196640 | tf_op jit(solution)/shard_map/ppermute | solution.py:313
  37.1 2.6 %collective-permute-done.17.refs_9_ = bf16[768,128]{1,0:T(8,128)(2,1)S(1)} collective-permute-done((bf16[768,128]{1,0:T(8,128)(2,1)S(1)}, bf16[768,128]{1,0:T(8,128)(2,1)S(1)}, u32[]{:S(2)}, u32[]{:S(2)}) %collective-permute-start.17) | collective-permute-done | bytes 196640 | tf_op jit(solution)/shard_map/ppermute | solution.py:313
  39.6 2.7 %collective-permute-start.20 = (bf16[768,128]{1,0:T(8,128)(2,1)S(1)}, bf16[768,128]{1,0:T(8,128)(2,1)S(1)}, u32[]{:S(2)}, u32[]{:S(2)}) collective-permute-start(bf16[768,128]{1,0:T(8,128)(2,1)S(1)} %collective-permute-done.7.refs_13_), channel_id=1, source_target_pairs={{0,4},{4,0},{1,5},{5,1},{2,6},{6,2},{3,7},{7,3},{8,12},{12,8},{9,1... | collective-permute-start | bytes 589832 | tf_op jit(solution)/shard_map/ppermute | solution.py:306
  42.8 2.2 %collective-permute-done.11.refs_6_ = bf16[768,128]{1,0:T(8,128)(2,1)S(1)} collective-permute-done((bf16[768,128]{1,0:T(8,128)(2,1)S(1)}, bf16[768,128]{1,0:T(8,128)(2,1)S(1)}, u32[]{:S(2)}, u32[]{:S(2)}) %collective-permute-start.11) | collective-permute-done | bytes 196640 | tf_op jit(solution)/shard_map/ppermute | solution.py:316
  45.5 2.6 %collective-permute-done.8.refs_5_ = bf16[768,128]{1,0:T(8,128)(2,1)S(1)} collective-permute-done((bf16[768,128]{1,0:T(8,128)(2,1)S(1)}, bf16[768,128]{1,0:T(8,128)(2,1)S(1)}, u32[]{:S(2)}, u32[]{:S(2)}) %collective-permute-start.8) | collective-permute-done | bytes 196640 | tf_op jit(solution)/shard_map/ppermute | solution.py:313
  52.8 1.6 %collective-permute-start.23 = (bf16[432,128]{1,0:T(8,128)(2,1)S(1)}, bf16[432,128]{1,0:T(8,128)(2,1)S(1)}, u32[]{:S(2)}, u32[]{:S(2)}) collective-permute-start(bf16[432,128]{1,0:T(8,128)(2,1)S(1)} %get-tuple-element.16), channel_id=1, source_target_pairs={{0,8},{8,16},{16,24},{24,0},{1,9},{9,17},{17,25},{25,1},{2,10},{10... | collective-permute-start | bytes 331784 | tf_op jit(solution)/shard_map/ppermute | solution.py:339
  56.9 2.6 %collective-permute-done.22.refs_2_ = bf16[432,128]{1,0:T(8,128)(2,1)S(1)} collective-permute-done((bf16[432,128]{1,0:T(8,128)(2,1)S(1)}, bf16[432,128]{1,0:T(8,128)(2,1)S(1)}, u32[]{:S(2)}, u32[]{:S(2)}) %collective-permute-start.22) | collective-permute-done | bytes 110624 | tf_op jit(solution)/shard_map/ppermute | solution.py:339
  59.5 1.6 %collective-permute-done.23.refs_3_ = bf16[432,128]{1,0:T(8,128)(2,1)S(1)} collective-permute-done((bf16[432,128]{1,0:T(8,128)(2,1)S(1)}, bf16[432,128]{1,0:T(8,128)(2,1)S(1)}, u32[]{:S(2)}, u32[]{:S(2)}) %collective-permute-start.23) | collective-permute-done | bytes 110624 | tf_op jit(solution)/shard_map/ppermute | solution.py:339
  62.9 2.4 %collective-permute-start.25 = (bf16[384,128]{1,0:T(8,128)(2,1)S(1)}, bf16[384,128]{1,0:T(8,128)(2,1)S(1)}, u32[]{:S(2)}, u32[]{:S(2)}) collective-permute-start(bf16[384,128]{1,0:T(8,128)(2,1)S(1)} %merge.1.a0), channel_id=1, source_target_pairs={{0,2},{1,3},{2,0},{3,1},{4,6},{5,7},{6,4},{7,5},{8,10},{9,11},{10,... | collective-permute-start | bytes 294920 | tf_op jit(solution)/shard_map/ppermute | solution.py:341
  65.3 1.6 %collective-permute-start.26 = (bf16[384,128]{1,0:T(8,128)(2,1)S(1)}, bf16[384,128]{1,0:T(8,128)(2,1)S(1)}, u32[]{:S(2)}, u32[]{:S(2)}) collective-permute-start(bf16[384,128]{1,0:T(8,128)(2,1)S(1)} %merge.1.a0), channel_id=1, source_target_pairs={{0,3},{1,0},{2,1},{3,2},{4,7},{5,4},{6,5},{7,6},{8,11},{9,8},{10,9... | collective-permute-start | bytes 294920 | tf_op jit(solution)/shard_map/ppermute | solution.py:341
  67.7 2.3 %collective-permute-start.29 = (bf16[128,256]{1,0:T(8,128)(2,1)S(1)}, bf16[128,256]{1,0:T(8,128)(2,1)S(1)}, u32[]{:S(2)}, u32[]{:S(2)}) collective-permute-start(bf16[128,256]{1,0:T(8,128)(2,1)S(1)} %get-tuple-element.17), channel_id=1, source_target_pairs={{0,3},{1,0},{2,1},{3,2},{4,7},{5,4},{6,5},{7,6},{8,11},{9,8},{10,9... | collective-permute-start | bytes 196616 | tf_op jit(solution)/shard_map/ppermute | solution.py:291
  70.0 2.6 %collective-permute-done.28.w2 = bf16[128,256]{1,0:T(8,128)(2,1)S(1)} collective-permute-done((bf16[128,256]{1,0:T(8,128)(2,1)S(1)}, bf16[128,256]{1,0:T(8,128)(2,1)S(1)}, u32[]{:S(2)}, u32[]{:S(2)}) %collective-permute-start.28) | collective-permute-done | bytes 65568 | tf_op jit(solution)/shard_map/ppermute | solution.py:291
  (71 shorter events, 19.1 us)
Async XLA Ops:
  0.0 8.9 %collective-permute-start = (bf16[384,256]{1,0:T(8,128)(2,1)}, bf16[384,256]{1,0:T(8,128)(2,1)S(1)}, u32[]{:S(2)}, u32[]{:S(2)}) collective-permute-start(bf16[384,256]{1,0:T(8,128)(2,1)} %tokens.1), channel_id=1, source_target_pairs={{0,1},{1,2},{2,3},{3,0},{4,5},{5,6},{6,7},{7,4},{8,9},{9,10},{10,1... | collective-permute-start | bytes 589832 | tf_op jit(solution)/shard_map/ppermute | solution.py:284
  1.5 11.8 %collective-permute-start.1 = (bf16[384,256]{1,0:T(8,128)(2,1)}, bf16[384,256]{1,0:T(8,128)(2,1)S(1)}, u32[]{:S(2)}, u32[]{:S(2)}) collective-permute-start(bf16[384,256]{1,0:T(8,128)(2,1)} %tokens.1), channel_id=1, source_target_pairs={{0,2},{1,3},{2,0},{3,1},{4,6},{5,7},{6,4},{7,5},{8,10},{9,11},{10,... | collective-permute-start | bytes 589832 | tf_op jit(solution)/shard_map/ppermute | solution.py:284
  4.2 9.0 %collective-permute-start.2 = (bf16[384,256]{1,0:T(8,128)(2,1)}, bf16[384,256]{1,0:T(8,128)(2,1)S(1)}, u32[]{:S(2)}, u32[]{:S(2)}) collective-permute-start(bf16[384,256]{1,0:T(8,128)(2,1)} %tokens.1), channel_id=1, source_target_pairs={{0,3},{1,0},{2,1},{3,2},{4,7},{5,4},{6,5},{7,6},{8,11},{9,8},{10,9... | collective-permute-start | bytes 589832 | tf_op jit(solution)/shard_map/ppermute | solution.py:284
  13.8 9.0 %collective-permute-start.3 = (bf16[400,128]{1,0:T(8,128)(2,1)S(1)}, bf16[400,128]{1,0:T(8,128)(2,1)S(1)}, u32[]{:S(2)}, u32[]{:S(2)}) collective-permute-start(bf16[400,128]{1,0:T(8,128)(2,1)S(1)} %shard_map.82.refs_1_), channel_id=1, source_target_pairs={{0,8},{8,16},{16,24},{24,0},{1,9},{9,17},{17,25},{25,1},{2,10},{10... | collective-permute-start | bytes 307208 | tf_op jit(solution)/shard_map/ppermute | solution.py:320
  15.5 9.3 %collective-permute-start.4 = (bf16[400,128]{1,0:T(8,128)(2,1)S(1)}, bf16[400,128]{1,0:T(8,128)(2,1)S(1)}, u32[]{:S(2)}, u32[]{:S(2)}) collective-permute-start(bf16[400,128]{1,0:T(8,128)(2,1)S(1)} %shard_map.82.refs_1_), channel_id=1, source_target_pairs={{0,16},{8,24},{16,0},{24,8},{1,17},{9,25},{17,1},{25,9},{2,18},{10... | collective-permute-start | bytes 307208 | tf_op jit(solution)/shard_map/ppermute | solution.py:320
  16.4 8.4 %collective-permute-start.5 = (bf16[400,128]{1,0:T(8,128)(2,1)S(1)}, bf16[400,128]{1,0:T(8,128)(2,1)S(1)}, u32[]{:S(2)}, u32[]{:S(2)}) collective-permute-start(bf16[400,128]{1,0:T(8,128)(2,1)S(1)} %shard_map.82.refs_1_), channel_id=1, source_target_pairs={{0,24},{8,0},{16,8},{24,16},{1,25},{9,1},{17,9},{25,17},{2,26},{10... | collective-permute-start | bytes 307208 | tf_op jit(solution)/shard_map/ppermute | solution.py:320
  19.5 10.6 %collective-permute-start.10 = (bf16[768,128]{1,0:T(8,128)(2,1)S(1)}, bf16[768,128]{1,0:T(8,128)(2,1)S(1)}, u32[]{:S(2)}, u32[]{:S(2)}) collective-permute-start(bf16[768,128]{1,0:T(8,128)(2,1)S(1)} %shard_map.83.refs_5_), channel_id=1, source_target_pairs={{0,64},{4,196},{32,96},{36,228},{64,128},{68,4},{96,160},{100,36},... | collective-permute-start | bytes 589832 | tf_op jit(solution)/shard_map/ppermute | solution.py:312
  22.9 10.4 %collective-permute-start.15 = (bf16[768,128]{1,0:T(8,128)(2,1)S(1)}, bf16[768,128]{1,0:T(8,128)(2,1)S(1)}, u32[]{:S(2)}, u32[]{:S(2)}) collective-permute-start(bf16[768,128]{1,0:T(8,128)(2,1)S(1)} %shard_map.83.refs_5_), channel_id=1, source_target_pairs={{0,32},{4,228},{32,64},{36,4},{64,96},{68,36},{96,128},{100,68},{1... | collective-permute-start | bytes 589832 | tf_op jit(solution)/shard_map/ppermute | solution.py:312
  24.8 11.7 %collective-permute-start.7 = (bf16[768,128]{1,0:T(8,128)(2,1)S(1)}, bf16[768,128]{1,0:T(8,128)(2,1)S(1)}, u32[]{:S(2)}, u32[]{:S(2)}) collective-permute-start(bf16[768,128]{1,0:T(8,128)(2,1)S(1)} %collective-permute-done.6.refs_6_), channel_id=1, source_target_pairs={{0,64},{4,196},{32,96},{36,228},{64,128},{68,4},{96,160},{100,36},... | collective-permute-start | bytes 589832 | tf_op jit(solution)/shard_map/ppermute | solution.py:313
  28.5 11.1 %collective-permute-start.17 = (bf16[768,128]{1,0:T(8,128)(2,1)S(1)}, bf16[768,128]{1,0:T(8,128)(2,1)S(1)}, u32[]{:S(2)}, u32[]{:S(2)}) collective-permute-start(bf16[768,128]{1,0:T(8,128)(2,1)S(1)} %collective-permute-done.6.refs_6_), channel_id=1, source_target_pairs={{0,32},{4,228},{32,64},{36,4},{64,96},{68,36},{96,128},{100,68},{1... | collective-permute-start | bytes 589832 | tf_op jit(solution)/shard_map/ppermute | solution.py:313
  30.1 9.5 %collective-permute-start.19 = (bf16[768,128]{1,0:T(8,128)(2,1)S(1)}, bf16[768,128]{1,0:T(8,128)(2,1)S(1)}, u32[]{:S(2)}, u32[]{:S(2)}) collective-permute-start(bf16[768,128]{1,0:T(8,128)(2,1)S(1)} %collective-permute-done.10.refs_11_), channel_id=1, source_target_pairs={{0,4},{4,0},{1,5},{5,1},{2,6},{6,2},{3,7},{7,3},{8,12},{12,8},{9,1... | collective-permute-start | bytes 589832 | tf_op jit(solution)/shard_map/ppermute | solution.py:306
  30.7 11.7 %collective-permute-start.13 = (bf16[768,128]{1,0:T(8,128)(2,1)S(1)}, bf16[768,128]{1,0:T(8,128)(2,1)S(1)}, u32[]{:S(2)}, u32[]{:S(2)}) collective-permute-start(bf16[768,128]{1,0:T(8,128)(2,1)S(1)} %collective-permute-done.10.refs_11_), channel_id=1, source_target_pairs={{0,32},{4,228},{32,64},{36,4},{64,96},{68,36},{96,128},{100,68},{1... | collective-permute-start | bytes 589832 | tf_op jit(solution)/shard_map/ppermute | solution.py:312
  33.3 11.8 %collective-permute-start.11 = (bf16[768,128]{1,0:T(8,128)(2,1)S(1)}, bf16[768,128]{1,0:T(8,128)(2,1)S(1)}, u32[]{:S(2)}, u32[]{:S(2)}) collective-permute-start(bf16[768,128]{1,0:T(8,128)(2,1)S(1)} %collective-permute-done.10.refs_11_), channel_id=1, source_target_pairs={{0,64},{4,196},{32,96},{36,228},{64,128},{68,4},{96,160},{100,36},... | collective-permute-start | bytes 589832 | tf_op jit(solution)/shard_map/ppermute | solution.py:316
  39.6 8.4 %collective-permute-start.8 = (bf16[768,128]{1,0:T(8,128)(2,1)S(1)}, bf16[768,128]{1,0:T(8,128)(2,1)S(1)}, u32[]{:S(2)}, u32[]{:S(2)}) collective-permute-start(bf16[768,128]{1,0:T(8,128)(2,1)S(1)} %collective-permute-done.7.refs_13_), channel_id=1, source_target_pairs={{0,32},{4,228},{32,64},{36,4},{64,96},{68,36},{96,128},{100,68},{1... | collective-permute-start | bytes 589832 | tf_op jit(solution)/shard_map/ppermute | solution.py:313
  39.6 8.6 %collective-permute-start.20 = (bf16[768,128]{1,0:T(8,128)(2,1)S(1)}, bf16[768,128]{1,0:T(8,128)(2,1)S(1)}, u32[]{:S(2)}, u32[]{:S(2)}) collective-permute-start(bf16[768,128]{1,0:T(8,128)(2,1)S(1)} %collective-permute-done.7.refs_13_), channel_id=1, source_target_pairs={{0,4},{4,0},{1,5},{5,1},{2,6},{6,2},{3,7},{7,3},{8,12},{12,8},{9,1... | collective-permute-start | bytes 589832 | tf_op jit(solution)/shard_map/ppermute | solution.py:306
  42.3 6.0 %collective-permute-start.18 = (bf16[768,128]{1,0:T(8,128)(2,1)S(1)}, bf16[768,128]{1,0:T(8,128)(2,1)S(1)}, u32[]{:S(2)}, u32[]{:S(2)}) collective-permute-start(bf16[768,128]{1,0:T(8,128)(2,1)S(1)} %collective-permute-done.17.refs_9_), channel_id=1, source_target_pairs={{0,4},{4,0},{1,5},{5,1},{2,6},{6,2},{3,7},{7,3},{8,12},{12,8},{9,1... | collective-permute-start | bytes 589832 | tf_op jit(solution)/shard_map/ppermute | solution.py:306
  42.4 7.2 %collective-permute-start.14 = (bf16[768,128]{1,0:T(8,128)(2,1)S(1)}, bf16[768,128]{1,0:T(8,128)(2,1)S(1)}, u32[]{:S(2)}, u32[]{:S(2)}) collective-permute-start(bf16[768,128]{1,0:T(8,128)(2,1)S(1)} %collective-permute-done.13.refs_5_), channel_id=1, source_target_pairs={{0,4},{4,0},{1,5},{5,1},{2,6},{6,2},{3,7},{7,3},{8,12},{12,8},{9,1... | collective-permute-start | bytes 589832 | tf_op jit(solution)/shard_map/ppermute | solution.py:306
  52.8 6.7 %collective-permute-start.22 = (bf16[432,128]{1,0:T(8,128)(2,1)S(1)}, bf16[432,128]{1,0:T(8,128)(2,1)S(1)}, u32[]{:S(2)}, u32[]{:S(2)}) collective-permute-start(bf16[432,128]{1,0:T(8,128)(2,1)S(1)} %get-tuple-element.15), channel_id=1, source_target_pairs={{0,16},{8,24},{16,0},{24,8},{1,17},{9,25},{17,1},{25,9},{2,18},{10... | collective-permute-start | bytes 331784 | tf_op jit(solution)/shard_map/ppermute | solution.py:339
  52.8 8.3 %collective-permute-start.23 = (bf16[432,128]{1,0:T(8,128)(2,1)S(1)}, bf16[432,128]{1,0:T(8,128)(2,1)S(1)}, u32[]{:S(2)}, u32[]{:S(2)}) collective-permute-start(bf16[432,128]{1,0:T(8,128)(2,1)S(1)} %get-tuple-element.16), channel_id=1, source_target_pairs={{0,8},{8,16},{16,24},{24,0},{1,9},{9,17},{17,25},{25,1},{2,10},{10... | collective-permute-start | bytes 331784 | tf_op jit(solution)/shard_map/ppermute | solution.py:339
  54.5 13.2 %collective-permute-start.27 = (bf16[128,256]{1,0:T(8,128)(2,1)S(1)}, bf16[128,256]{1,0:T(8,128)(2,1)S(1)}, u32[]{:S(2)}, u32[]{:S(2)}) collective-permute-start(bf16[128,256]{1,0:T(8,128)(2,1)S(1)} %get-tuple-element.18), channel_id=1, source_target_pairs={{0,1},{1,2},{2,3},{3,0},{4,5},{5,6},{6,7},{7,4},{8,9},{9,10},{10,1... | collective-permute-start | bytes 196616 | tf_op jit(solution)/shard_map/ppermute | solution.py:291
  61.5 11.2 %collective-permute-start.24 = (bf16[384,128]{1,0:T(8,128)(2,1)S(1)}, bf16[384,128]{1,0:T(8,128)(2,1)S(1)}, u32[]{:S(2)}, u32[]{:S(2)}) collective-permute-start(bf16[384,128]{1,0:T(8,128)(2,1)S(1)} %merge.1.a0), channel_id=1, source_target_pairs={{0,1},{1,2},{2,3},{3,0},{4,5},{5,6},{6,7},{7,4},{8,9},{9,10},{10,1... | collective-permute-start | bytes 294920 | tf_op jit(solution)/shard_map/ppermute | solution.py:341
  62.9 9.8 %collective-permute-start.25 = (bf16[384,128]{1,0:T(8,128)(2,1)S(1)}, bf16[384,128]{1,0:T(8,128)(2,1)S(1)}, u32[]{:S(2)}, u32[]{:S(2)}) collective-permute-start(bf16[384,128]{1,0:T(8,128)(2,1)S(1)} %merge.1.a0), channel_id=1, source_target_pairs={{0,2},{1,3},{2,0},{3,1},{4,6},{5,7},{6,4},{7,5},{8,10},{9,11},{10,... | collective-permute-start | bytes 294920 | tf_op jit(solution)/shard_map/ppermute | solution.py:341
  65.3 7.4 %collective-permute-start.26 = (bf16[384,128]{1,0:T(8,128)(2,1)S(1)}, bf16[384,128]{1,0:T(8,128)(2,1)S(1)}, u32[]{:S(2)}, u32[]{:S(2)}) collective-permute-start(bf16[384,128]{1,0:T(8,128)(2,1)S(1)} %merge.1.a0), channel_id=1, source_target_pairs={{0,3},{1,0},{2,1},{3,2},{4,7},{5,4},{6,5},{7,6},{8,11},{9,8},{10,9... | collective-permute-start | bytes 294920 | tf_op jit(solution)/shard_map/ppermute | solution.py:341
  66.9 5.8 %collective-permute-start.28 = (bf16[128,256]{1,0:T(8,128)(2,1)S(1)}, bf16[128,256]{1,0:T(8,128)(2,1)S(1)}, u32[]{:S(2)}, u32[]{:S(2)}) collective-permute-start(bf16[128,256]{1,0:T(8,128)(2,1)S(1)} %get-tuple-element.20), channel_id=1, source_target_pairs={{0,2},{1,3},{2,0},{3,1},{4,6},{5,7},{6,4},{7,5},{8,10},{9,11},{10,... | collective-permute-start | bytes 196616 | tf_op jit(solution)/shard_map/ppermute | solution.py:291
  (10 other events, 36.7 us)

commit v4 on v3

--- a/solution.py
+++ b/solution.py
@@ -243,20 +243,38 @@
     )(*[vmem(a) for a in parts])
 
 
-def finish_kernel(a0, a1, a2, a3, w0, w1, w2, w3, out):
-    squares, summed = None, None
-    for a, w in ((a0, w0), (a1, w1), (a2, w2), (a3, w3)):
+def begin_kernel(a, w, total, squares):
+    rows = a[...]
+    total[...] = jnp.dot(rows, w[...], preferred_element_type=jnp.float32)
+    wide = rows.astype(jnp.float32)
+    squares[...] = wide * wide
+
+
+def open_output(piece, weight):
+    rows, cols = piece.shape[0], weight.shape[1]
+    return pl.pallas_call(
+        begin_kernel,
+        out_shape=(VMEM((rows, cols), jnp.float32), VMEM(piece.shape, jnp.float32)),
+        in_specs=[full()] * 2,
+        out_specs=(full(),) * 2,
+        name="begin",
+        compiler_params=PARAMS,
+    )(vmem(piece), vmem(weight))
+
+
+def finish_kernel(t, q, a1, a2, a3, w1, w2, w3, out):
+    total, squares = t[...], q[...]
+    for a, w in ((a1, w1), (a2, w2), (a3, w3)):
         rows = a[...]
         wide = rows.astype(jnp.float32)
-        term = jnp.dot(rows, w[...], preferred_element_type=jnp.float32)
-        squares = wide * wide if squares is None else squares + wide * wide
-        summed = term if summed is None else summed + term
+        squares = squares + wide * wide
+        total = total + jnp.dot(rows, w[...], preferred_element_type=jnp.float32)
     mean_sq = jnp.sum(squares, axis=1, keepdims=True) / (HEADS * HEAD_SIZE)
-    out[...] = (summed * lax.rsqrt(mean_sq + eps_norm)).astype(jnp.bfloat16)
-
-
-def finish(pieces, weights):
-    rows, cols = pieces[0].shape[0], weights[0].shape[1]
+    out[...] = (total * lax.rsqrt(mean_sq + eps_norm)).astype(jnp.bfloat16)
+
+
+def finish(started, pieces, weights):
+    rows, cols = started[0].shape
     return pl.pallas_call(
         finish_kernel,
         out_shape=jax.ShapeDtypeStruct((rows, cols), jnp.bfloat16),
@@ -264,7 +282,7 @@
         out_specs=full(),
         name="finish",
         compiler_params=PARAMS,
-    )(*[vmem(a) for a in (*pieces, *weights)])
+    )(*[vmem(a) for a in (*started, *pieces, *weights)])
 
 
 def on_device(
@@ -339,7 +357,8 @@
     back = [parts[0]] + [lax.ppermute(parts[s], "y", shift(Y, -s)) for s in (1, 2, 3)]
     attended = merge(back, blocks)
     spread = [attended] + [lax.ppermute(attended, "x", shift(X, s)) for s in (1, 2, 3)]
-    return finish(spread, weights)
+    started = open_output(attended, weights[0])
+    return finish(started, spread[1:], weights[1:])
 
 
 def solution(mesh):

time: 74.9 us -> 74.8 us (level)
  no operation moved by 1% of the time
where the time goes in v4:
time: 74.8 us; the launch traced here: 73.7 us
  starting transfers between devices  41.7 us (56%)
  waiting for transfers between devices  22.5 us (30%)
  Pallas kernels  7.26 us (10%)
  local copies, waits for them, and re-layouts  1.58 us (2%)
    ppermute x3, starting transfers between devices, on_device(): same.append(lax.ppermute(same[step - reach], ('z', 'c'), onward(reach)))  7.18 us
    ppermute x3, waiting for transfers between devices, on_device(): cross.append(lax.ppermute(cross[step - reach], ('z', 'c'), onward(reach)))  6.89 us
    ppermute x3, starting transfers between devices, on_device(): lax.ppermute(tokens, 'x', shift(X, s))  5.65 us
    ppermute x3, starting transfers between devices, on_device(): lax.ppermute(attended, 'x', shift(X, s))  5.37 us
    ppermute x3, waiting for transfers between devices, on_device(): lax.ppermute(parts[s], 'y', shift(Y, -s))  5.21 us
    ppermute x3, starting transfers between devices, on_device(): queries = [q] + [lax.ppermute(q, 'y', shift(Y, s)) for s in (1, 2, 3)]  5 us
    ppermute x8, starting transfers between devices, swap(): return lax.ppermute(a, 'c', [(0, 1), (1, 0)])  4.86 us
    ppermute x3, starting transfers between devices, on_device(): cross.append(lax.ppermute(cross[step - reach], ('z', 'c'), onward(reach)))  4.68 us
  transfers between devices with their start and end apart: 30, of which 12 were waited for; matrix products, arithmetic and copies ran while one was open for 1% of the time, Pallas kernels for 7%

profile of v4, /device:TPU:8, one launch (start us, length us, event | category | flops | bytes accessed | tf_op | source)
XLA Modules:
  0.0 73.7 jit_solution(9073179640657618919)
XLA Ops:
  0.0 1.5 %collective-permute-start = (bf16[384,256]{1,0:T(8,128)(2,1)}, bf16[384,256]{1,0:T(8,128)(2,1)S(1)}, u32[]{:S(2)}, u32[]{:S(2)}) collective-permute-start(bf16[384,256]{1,0:T(8,128)(2,1)} %tokens.1), channel_id=1, source_target_pairs={{0,1},{1,2},{2,3},{3,0},{4,5},{5,6},{6,7},{7,4},{8,9},{9,10},{10,1... | collective-permute-start | bytes 589832 | tf_op jit(solution)/shard_map/ppermute | solution.py:302
  1.5 2.7 %collective-permute-start.1 = (bf16[384,256]{1,0:T(8,128)(2,1)}, bf16[384,256]{1,0:T(8,128)(2,1)S(1)}, u32[]{:S(2)}, u32[]{:S(2)}) collective-permute-start(bf16[384,256]{1,0:T(8,128)(2,1)} %tokens.1), channel_id=1, source_target_pairs={{0,2},{1,3},{2,0},{3,1},{4,6},{5,7},{6,4},{7,5},{8,10},{9,11},{10,... | collective-permute-start | bytes 589832 | tf_op jit(solution)/shard_map/ppermute | solution.py:302
  4.2 1.4 %collective-permute-start.2 = (bf16[384,256]{1,0:T(8,128)(2,1)}, bf16[384,256]{1,0:T(8,128)(2,1)S(1)}, u32[]{:S(2)}, u32[]{:S(2)}) collective-permute-start(bf16[384,256]{1,0:T(8,128)(2,1)} %tokens.1), channel_id=1, source_target_pairs={{0,3},{1,0},{2,1},{3,2},{4,7},{5,4},{6,5},{7,6},{8,11},{9,8},{10,9... | collective-permute-start | bytes 589832 | tf_op jit(solution)/shard_map/ppermute | solution.py:302
  7.1 1.6 %stage.1 = (bf16[1024,384]{1,0:T(8,128)(2,1)S(1)}, f32[384,384]{1,0:T(8,128)S(1)}) custom-call(bf16[384,256]{1,0:T(8,128)(2,1)} %tokens.1, bf16[1024,128]{1,0:T(8,128)(2,1)} %wq.1, bf16[1024,128]{1,0:T(8,128)(2,1)} %wk.1, bf16[1024,128]{1,0:T(8,128)(2,1)} %wv.1), custom_call_target="tpu_custom_call" | custom-call | tf_op jit(solution)/shard_map/stage/pallas_call | solution.py:54
  8.9 4.4 %collective-permute-done.1.t2 = bf16[384,256]{1,0:T(8,128)(2,1)S(1)} collective-permute-done((bf16[384,256]{1,0:T(8,128)(2,1)}, bf16[384,256]{1,0:T(8,128)(2,1)S(1)}, u32[]{:S(2)}, u32[]{:S(2)}) %collective-permute-start.1) | collective-permute-done | bytes 196640 | tf_op jit(solution)/shard_map/ppermute | solution.py:302
  13.8 1.7 %collective-permute-start.3 = (bf16[400,128]{1,0:T(8,128)(2,1)S(1)}, bf16[400,128]{1,0:T(8,128)(2,1)S(1)}, u32[]{:S(2)}, u32[]{:S(2)}) collective-permute-start(bf16[400,128]{1,0:T(8,128)(2,1)S(1)} %shard_map.82.refs_1_), channel_id=1, source_target_pairs={{0,8},{8,16},{16,24},{24,0},{1,9},{9,17},{17,25},{25,1},{2,10},{10... | collective-permute-start | bytes 307208 | tf_op jit(solution)/shard_map/ppermute | solution.py:338
  16.4 2.4 %collective-permute-start.5 = (bf16[400,128]{1,0:T(8,128)(2,1)S(1)}, bf16[400,128]{1,0:T(8,128)(2,1)S(1)}, u32[]{:S(2)}, u32[]{:S(2)}) collective-permute-start(bf16[400,128]{1,0:T(8,128)(2,1)S(1)} %shard_map.82.refs_1_), channel_id=1, source_target_pairs={{0,24},{8,0},{16,8},{24,16},{1,25},{9,1},{17,9},{25,17},{2,26},{10... | collective-permute-start | bytes 307208 | tf_op jit(solution)/shard_map/ppermute | solution.py:338
  19.5 3.3 %collective-permute-start.10 = (bf16[768,128]{1,0:T(8,128)(2,1)S(1)}, bf16[768,128]{1,0:T(8,128)(2,1)S(1)}, u32[]{:S(2)}, u32[]{:S(2)}) collective-permute-start(bf16[768,128]{1,0:T(8,128)(2,1)S(1)} %shard_map.83.refs_5_), channel_id=1, source_target_pairs={{0,64},{4,196},{32,96},{36,228},{64,128},{68,4},{96,160},{100,36},... | collective-permute-start | bytes 589832 | tf_op jit(solution)/shard_map/ppermute | solution.py:330
  22.9 1.9 %collective-permute-start.15 = (bf16[768,128]{1,0:T(8,128)(2,1)S(1)}, bf16[768,128]{1,0:T(8,128)(2,1)S(1)}, u32[]{:S(2)}, u32[]{:S(2)}) collective-permute-start(bf16[768,128]{1,0:T(8,128)(2,1)S(1)} %shard_map.83.refs_5_), channel_id=1, source_target_pairs={{0,32},{4,228},{32,64},{36,4},{64,96},{68,36},{96,128},{100,68},{1... | collective-permute-start | bytes 589832 | tf_op jit(solution)/shard_map/ppermute | solution.py:330
  24.8 3.7 %collective-permute-start.7 = (bf16[768,128]{1,0:T(8,128)(2,1)S(1)}, bf16[768,128]{1,0:T(8,128)(2,1)S(1)}, u32[]{:S(2)}, u32[]{:S(2)}) collective-permute-start(bf16[768,128]{1,0:T(8,128)(2,1)S(1)} %collective-permute-done.6.refs_6_), channel_id=1, source_target_pairs={{0,64},{4,196},{32,96},{36,228},{64,128},{68,4},{96,160},{100,36},... | collective-permute-start | bytes 589832 | tf_op jit(solution)/shard_map/ppermute | solution.py:331
  30.7 1.9 %collective-permute-start.13 = (bf16[768,128]{1,0:T(8,128)(2,1)S(1)}, bf16[768,128]{1,0:T(8,128)(2,1)S(1)}, u32[]{:S(2)}, u32[]{:S(2)}) collective-permute-start(bf16[768,128]{1,0:T(8,128)(2,1)S(1)} %collective-permute-done.10.refs_11_), channel_id=1, source_target_pairs={{0,32},{4,228},{32,64},{36,4},{64,96},{68,36},{96,128},{100,68},{1... | collective-permute-start | bytes 589832 | tf_op jit(solution)/shard_map/ppermute | solution.py:330
  33.3 1.5 %collective-permute-start.11 = (bf16[768,128]{1,0:T(8,128)(2,1)S(1)}, bf16[768,128]{1,0:T(8,128)(2,1)S(1)}, u32[]{:S(2)}, u32[]{:S(2)}) collective-permute-start(bf16[768,128]{1,0:T(8,128)(2,1)S(1)} %collective-permute-done.10.refs_11_), channel_id=1, source_target_pairs={{0,64},{4,196},{32,96},{36,228},{64,128},{68,4},{96,160},{100,36},... | collective-permute-start | bytes 589832 | tf_op jit(solution)/shard_map/ppermute | solution.py:334
  34.7 1.8 %collective-permute-done.7.refs_13_ = bf16[768,128]{1,0:T(8,128)(2,1)S(1)} collective-permute-done((bf16[768,128]{1,0:T(8,128)(2,1)S(1)}, bf16[768,128]{1,0:T(8,128)(2,1)S(1)}, u32[]{:S(2)}, u32[]{:S(2)}) %collective-permute-start.7) | collective-permute-done | bytes 196640 | tf_op jit(solution)/shard_map/ppermute | solution.py:331
  37.1 2.6 %collective-permute-done.17.refs_9_ = bf16[768,128]{1,0:T(8,128)(2,1)S(1)} collective-permute-done((bf16[768,128]{1,0:T(8,128)(2,1)S(1)}, bf16[768,128]{1,0:T(8,128)(2,1)S(1)}, u32[]{:S(2)}, u32[]{:S(2)}) %collective-permute-start.17) | collective-permute-done | bytes 196640 | tf_op jit(solution)/shard_map/ppermute | solution.py:331
  39.6 2.7 %collective-permute-start.20 = (bf16[768,128]{1,0:T(8,128)(2,1)S(1)}, bf16[768,128]{1,0:T(8,128)(2,1)S(1)}, u32[]{:S(2)}, u32[]{:S(2)}) collective-permute-start(bf16[768,128]{1,0:T(8,128)(2,1)S(1)} %collective-permute-done.7.refs_13_), channel_id=1, source_target_pairs={{0,4},{4,0},{1,5},{5,1},{2,6},{6,2},{3,7},{7,3},{8,12},{12,8},{9,1... | collective-permute-start | bytes 589832 | tf_op jit(solution)/shard_map/ppermute | solution.py:324
  42.8 2.2 %collective-permute-done.11.refs_6_ = bf16[768,128]{1,0:T(8,128)(2,1)S(1)} collective-permute-done((bf16[768,128]{1,0:T(8,128)(2,1)S(1)}, bf16[768,128]{1,0:T(8,128)(2,1)S(1)}, u32[]{:S(2)}, u32[]{:S(2)}) %collective-permute-start.11) | collective-permute-done | bytes 196640 | tf_op jit(solution)/shard_map/ppermute | solution.py:334
  45.5 2.6 %collective-permute-done.8.refs_5_ = bf16[768,128]{1,0:T(8,128)(2,1)S(1)} collective-permute-done((bf16[768,128]{1,0:T(8,128)(2,1)S(1)}, bf16[768,128]{1,0:T(8,128)(2,1)S(1)}, u32[]{:S(2)}, u32[]{:S(2)}) %collective-permute-start.8) | collective-permute-done | bytes 196640 | tf_op jit(solution)/shard_map/ppermute | solution.py:331
  52.8 1.6 %collective-permute-start.23 = (bf16[432,128]{1,0:T(8,128)(2,1)S(1)}, bf16[432,128]{1,0:T(8,128)(2,1)S(1)}, u32[]{:S(2)}, u32[]{:S(2)}) collective-permute-start(bf16[432,128]{1,0:T(8,128)(2,1)S(1)} %get-tuple-element.18), channel_id=1, source_target_pairs={{0,8},{8,16},{16,24},{24,0},{1,9},{9,17},{17,25},{25,1},{2,10},{10... | collective-permute-start | bytes 331784 | tf_op jit(solution)/shard_map/ppermute | solution.py:357
  56.9 2.6 %collective-permute-done.22.refs_2_ = bf16[432,128]{1,0:T(8,128)(2,1)S(1)} collective-permute-done((bf16[432,128]{1,0:T(8,128)(2,1)S(1)}, bf16[432,128]{1,0:T(8,128)(2,1)S(1)}, u32[]{:S(2)}, u32[]{:S(2)}) %collective-permute-start.22) | collective-permute-done | bytes 110624 | tf_op jit(solution)/shard_map/ppermute | solution.py:357
  59.5 1.6 %collective-permute-done.23.refs_3_ = bf16[432,128]{1,0:T(8,128)(2,1)S(1)} collective-permute-done((bf16[432,128]{1,0:T(8,128)(2,1)S(1)}, bf16[432,128]{1,0:T(8,128)(2,1)S(1)}, u32[]{:S(2)}, u32[]{:S(2)}) %collective-permute-start.23) | collective-permute-done | bytes 110624 | tf_op jit(solution)/shard_map/ppermute | solution.py:357
  62.9 2.4 %collective-permute-start.25 = (bf16[384,128]{1,0:T(8,128)(2,1)S(1)}, bf16[384,128]{1,0:T(8,128)(2,1)S(1)}, u32[]{:S(2)}, u32[]{:S(2)}) collective-permute-start(bf16[384,128]{1,0:T(8,128)(2,1)S(1)} %merge.1.a), channel_id=1, source_target_pairs={{0,2},{1,3},{2,0},{3,1},{4,6},{5,7},{6,4},{7,5},{8,10},{9,11},{10,... | collective-permute-start | bytes 294920 | tf_op jit(solution)/shard_map/ppermute | solution.py:359
  65.3 1.6 %collective-permute-start.26 = (bf16[384,128]{1,0:T(8,128)(2,1)S(1)}, bf16[384,128]{1,0:T(8,128)(2,1)S(1)}, u32[]{:S(2)}, u32[]{:S(2)}) collective-permute-start(bf16[384,128]{1,0:T(8,128)(2,1)S(1)} %merge.1.a), channel_id=1, source_target_pairs={{0,3},{1,0},{2,1},{3,2},{4,7},{5,4},{6,5},{7,6},{8,11},{9,8},{10,9... | collective-permute-start | bytes 294920 | tf_op jit(solution)/shard_map/ppermute | solution.py:359
  67.7 2.3 %collective-permute-start.29 = (bf16[128,256]{1,0:T(8,128)(2,1)S(1)}, bf16[128,256]{1,0:T(8,128)(2,1)S(1)}, u32[]{:S(2)}, u32[]{:S(2)}) collective-permute-start(bf16[128,256]{1,0:T(8,128)(2,1)S(1)} %get-tuple-element.21), channel_id=1, source_target_pairs={{0,3},{1,0},{2,1},{3,2},{4,7},{5,4},{6,5},{7,6},{8,11},{9,8},{10,9... | collective-permute-start | bytes 196616 | tf_op jit(solution)/shard_map/ppermute | solution.py:309
  70.2 2.4 %collective-permute-done.28.w2 = bf16[128,256]{1,0:T(8,128)(2,1)S(1)} collective-permute-done((bf16[128,256]{1,0:T(8,128)(2,1)S(1)}, bf16[128,256]{1,0:T(8,128)(2,1)S(1)}, u32[]{:S(2)}, u32[]{:S(2)}) %collective-permute-start.28) | collective-permute-done | bytes 65568 | tf_op jit(solution)/shard_map/ppermute | solution.py:309
  (72 shorter events, 19.3 us)
Async XLA Ops:
  0.0 8.9 %collective-permute-start = (bf16[384,256]{1,0:T(8,128)(2,1)}, bf16[384,256]{1,0:T(8,128)(2,1)S(1)}, u32[]{:S(2)}, u32[]{:S(2)}) collective-permute-start(bf16[384,256]{1,0:T(8,128)(2,1)} %tokens.1), channel_id=1, source_target_pairs={{0,1},{1,2},{2,3},{3,0},{4,5},{5,6},{6,7},{7,4},{8,9},{9,10},{10,1... | collective-permute-start | bytes 589832 | tf_op jit(solution)/shard_map/ppermute | solution.py:302
  1.5 11.8 %collective-permute-start.1 = (bf16[384,256]{1,0:T(8,128)(2,1)}, bf16[384,256]{1,0:T(8,128)(2,1)S(1)}, u32[]{:S(2)}, u32[]{:S(2)}) collective-permute-start(bf16[384,256]{1,0:T(8,128)(2,1)} %tokens.1), channel_id=1, source_target_pairs={{0,2},{1,3},{2,0},{3,1},{4,6},{5,7},{6,4},{7,5},{8,10},{9,11},{10,... | collective-permute-start | bytes 589832 | tf_op jit(solution)/shard_map/ppermute | solution.py:302
  4.2 9.0 %collective-permute-start.2 = (bf16[384,256]{1,0:T(8,128)(2,1)}, bf16[384,256]{1,0:T(8,128)(2,1)S(1)}, u32[]{:S(2)}, u32[]{:S(2)}) collective-permute-start(bf16[384,256]{1,0:T(8,128)(2,1)} %tokens.1), channel_id=1, source_target_pairs={{0,3},{1,0},{2,1},{3,2},{4,7},{5,4},{6,5},{7,6},{8,11},{9,8},{10,9... | collective-permute-start | bytes 589832 | tf_op jit(solution)/shard_map/ppermute | solution.py:302
  13.8 9.0 %collective-permute-start.3 = (bf16[400,128]{1,0:T(8,128)(2,1)S(1)}, bf16[400,128]{1,0:T(8,128)(2,1)S(1)}, u32[]{:S(2)}, u32[]{:S(2)}) collective-permute-start(bf16[400,128]{1,0:T(8,128)(2,1)S(1)} %shard_map.82.refs_1_), channel_id=1, source_target_pairs={{0,8},{8,16},{16,24},{24,0},{1,9},{9,17},{17,25},{25,1},{2,10},{10... | collective-permute-start | bytes 307208 | tf_op jit(solution)/shard_map/ppermute | solution.py:338
  15.5 9.3 %collective-permute-start.4 = (bf16[400,128]{1,0:T(8,128)(2,1)S(1)}, bf16[400,128]{1,0:T(8,128)(2,1)S(1)}, u32[]{:S(2)}, u32[]{:S(2)}) collective-permute-start(bf16[400,128]{1,0:T(8,128)(2,1)S(1)} %shard_map.82.refs_1_), channel_id=1, source_target_pairs={{0,16},{8,24},{16,0},{24,8},{1,17},{9,25},{17,1},{25,9},{2,18},{10... | collective-permute-start | bytes 307208 | tf_op jit(solution)/shard_map/ppermute | solution.py:338
  16.4 8.4 %collective-permute-start.5 = (bf16[400,128]{1,0:T(8,128)(2,1)S(1)}, bf16[400,128]{1,0:T(8,128)(2,1)S(1)}, u32[]{:S(2)}, u32[]{:S(2)}) collective-permute-start(bf16[400,128]{1,0:T(8,128)(2,1)S(1)} %shard_map.82.refs_1_), channel_id=1, source_target_pairs={{0,24},{8,0},{16,8},{24,16},{1,25},{9,1},{17,9},{25,17},{2,26},{10... | collective-permute-start | bytes 307208 | tf_op jit(solution)/shard_map/ppermute | solution.py:338
  19.5 10.6 %collective-permute-start.10 = (bf16[768,128]{1,0:T(8,128)(2,1)S(1)}, bf16[768,128]{1,0:T(8,128)(2,1)S(1)}, u32[]{:S(2)}, u32[]{:S(2)}) collective-permute-start(bf16[768,128]{1,0:T(8,128)(2,1)S(1)} %shard_map.83.refs_5_), channel_id=1, source_target_pairs={{0,64},{4,196},{32,96},{36,228},{64,128},{68,4},{96,160},{100,36},... | collective-permute-start | bytes 589832 | tf_op jit(solution)/shard_map/ppermute | solution.py:330
  22.9 10.4 %collective-permute-start.15 = (bf16[768,128]{1,0:T(8,128)(2,1)S(1)}, bf16[768,128]{1,0:T(8,128)(2,1)S(1)}, u32[]{:S(2)}, u32[]{:S(2)}) collective-permute-start(bf16[768,128]{1,0:T(8,128)(2,1)S(1)} %shard_map.83.refs_5_), channel_id=1, source_target_pairs={{0,32},{4,228},{32,64},{36,4},{64,96},{68,36},{96,128},{100,68},{1... | collective-permute-start | bytes 589832 | tf_op jit(solution)/shard_map/ppermute | solution.py:330
  24.8 11.7 %collective-permute-start.7 = (bf16[768,128]{1,0:T(8,128)(2,1)S(1)}, bf16[768,128]{1,0:T(8,128)(2,1)S(1)}, u32[]{:S(2)}, u32[]{:S(2)}) collective-permute-start(bf16[768,128]{1,0:T(8,128)(2,1)S(1)} %collective-permute-done.6.refs_6_), channel_id=1, source_target_pairs={{0,64},{4,196},{32,96},{36,228},{64,128},{68,4},{96,160},{100,36},... | collective-permute-start | bytes 589832 | tf_op jit(solution)/shard_map/ppermute | solution.py:331
  28.5 11.1 %collective-permute-start.17 = (bf16[768,128]{1,0:T(8,128)(2,1)S(1)}, bf16[768,128]{1,0:T(8,128)(2,1)S(1)}, u32[]{:S(2)}, u32[]{:S(2)}) collective-permute-start(bf16[768,128]{1,0:T(8,128)(2,1)S(1)} %collective-permute-done.6.refs_6_), channel_id=1, source_target_pairs={{0,32},{4,228},{32,64},{36,4},{64,96},{68,36},{96,128},{100,68},{1... | collective-permute-start | bytes 589832 | tf_op jit(solution)/shard_map/ppermute | solution.py:331
  30.1 9.5 %collective-permute-start.19 = (bf16[768,128]{1,0:T(8,128)(2,1)S(1)}, bf16[768,128]{1,0:T(8,128)(2,1)S(1)}, u32[]{:S(2)}, u32[]{:S(2)}) collective-permute-start(bf16[768,128]{1,0:T(8,128)(2,1)S(1)} %collective-permute-done.10.refs_11_), channel_id=1, source_target_pairs={{0,4},{4,0},{1,5},{5,1},{2,6},{6,2},{3,7},{7,3},{8,12},{12,8},{9,1... | collective-permute-start | bytes 589832 | tf_op jit(solution)/shard_map/ppermute | solution.py:324
  30.7 11.7 %collective-permute-start.13 = (bf16[768,128]{1,0:T(8,128)(2,1)S(1)}, bf16[768,128]{1,0:T(8,128)(2,1)S(1)}, u32[]{:S(2)}, u32[]{:S(2)}) collective-permute-start(bf16[768,128]{1,0:T(8,128)(2,1)S(1)} %collective-permute-done.10.refs_11_), channel_id=1, source_target_pairs={{0,32},{4,228},{32,64},{36,4},{64,96},{68,36},{96,128},{100,68},{1... | collective-permute-start | bytes 589832 | tf_op jit(solution)/shard_map/ppermute | solution.py:330
  33.3 11.8 %collective-permute-start.11 = (bf16[768,128]{1,0:T(8,128)(2,1)S(1)}, bf16[768,128]{1,0:T(8,128)(2,1)S(1)}, u32[]{:S(2)}, u32[]{:S(2)}) collective-permute-start(bf16[768,128]{1,0:T(8,128)(2,1)S(1)} %collective-permute-done.10.refs_11_), channel_id=1, source_target_pairs={{0,64},{4,196},{32,96},{36,228},{64,128},{68,4},{96,160},{100,36},... | collective-permute-start | bytes 589832 | tf_op jit(solution)/shard_map/ppermute | solution.py:334
  39.6 8.4 %collective-permute-start.8 = (bf16[768,128]{1,0:T(8,128)(2,1)S(1)}, bf16[768,128]{1,0:T(8,128)(2,1)S(1)}, u32[]{:S(2)}, u32[]{:S(2)}) collective-permute-start(bf16[768,128]{1,0:T(8,128)(2,1)S(1)} %collective-permute-done.7.refs_13_), channel_id=1, source_target_pairs={{0,32},{4,228},{32,64},{36,4},{64,96},{68,36},{96,128},{100,68},{1... | collective-permute-start | bytes 589832 | tf_op jit(solution)/shard_map/ppermute | solution.py:331
  39.6 8.6 %collective-permute-start.20 = (bf16[768,128]{1,0:T(8,128)(2,1)S(1)}, bf16[768,128]{1,0:T(8,128)(2,1)S(1)}, u32[]{:S(2)}, u32[]{:S(2)}) collective-permute-start(bf16[768,128]{1,0:T(8,128)(2,1)S(1)} %collective-permute-done.7.refs_13_), channel_id=1, source_target_pairs={{0,4},{4,0},{1,5},{5,1},{2,6},{6,2},{3,7},{7,3},{8,12},{12,8},{9,1... | collective-permute-start | bytes 589832 | tf_op jit(solution)/shard_map/ppermute | solution.py:324
  42.3 6.0 %collective-permute-start.18 = (bf16[768,128]{1,0:T(8,128)(2,1)S(1)}, bf16[768,128]{1,0:T(8,128)(2,1)S(1)}, u32[]{:S(2)}, u32[]{:S(2)}) collective-permute-start(bf16[768,128]{1,0:T(8,128)(2,1)S(1)} %collective-permute-done.17.refs_9_), channel_id=1, source_target_pairs={{0,4},{4,0},{1,5},{5,1},{2,6},{6,2},{3,7},{7,3},{8,12},{12,8},{9,1... | collective-permute-start | bytes 589832 | tf_op jit(solution)/shard_map/ppermute | solution.py:324
  42.4 7.2 %collective-permute-start.14 = (bf16[768,128]{1,0:T(8,128)(2,1)S(1)}, bf16[768,128]{1,0:T(8,128)(2,1)S(1)}, u32[]{:S(2)}, u32[]{:S(2)}) collective-permute-start(bf16[768,128]{1,0:T(8,128)(2,1)S(1)} %collective-permute-done.13.refs_5_), channel_id=1, source_target_pairs={{0,4},{4,0},{1,5},{5,1},{2,6},{6,2},{3,7},{7,3},{8,12},{12,8},{9,1... | collective-permute-start | bytes 589832 | tf_op jit(solution)/shard_map/ppermute | solution.py:324
  52.8 6.7 %collective-permute-start.22 = (bf16[432,128]{1,0:T(8,128)(2,1)S(1)}, bf16[432,128]{1,0:T(8,128)(2,1)S(1)}, u32[]{:S(2)}, u32[]{:S(2)}) collective-permute-start(bf16[432,128]{1,0:T(8,128)(2,1)S(1)} %get-tuple-element.17), channel_id=1, source_target_pairs={{0,16},{8,24},{16,0},{24,8},{1,17},{9,25},{17,1},{25,9},{2,18},{10... | collective-permute-start | bytes 331784 | tf_op jit(solution)/shard_map/ppermute | solution.py:357
  52.8 8.3 %collective-permute-start.23 = (bf16[432,128]{1,0:T(8,128)(2,1)S(1)}, bf16[432,128]{1,0:T(8,128)(2,1)S(1)}, u32[]{:S(2)}, u32[]{:S(2)}) collective-permute-start(bf16[432,128]{1,0:T(8,128)(2,1)S(1)} %get-tuple-element.18), channel_id=1, source_target_pairs={{0,8},{8,16},{16,24},{24,0},{1,9},{9,17},{17,25},{25,1},{2,10},{10... | collective-permute-start | bytes 331784 | tf_op jit(solution)/shard_map/ppermute | solution.py:357
  54.5 13.2 %collective-permute-start.27 = (bf16[128,256]{1,0:T(8,128)(2,1)S(1)}, bf16[128,256]{1,0:T(8,128)(2,1)S(1)}, u32[]{:S(2)}, u32[]{:S(2)}) collective-permute-start(bf16[128,256]{1,0:T(8,128)(2,1)S(1)} %get-tuple-element.22), channel_id=1, source_target_pairs={{0,1},{1,2},{2,3},{3,0},{4,5},{5,6},{6,7},{7,4},{8,9},{9,10},{10,1... | collective-permute-start | bytes 196616 | tf_op jit(solution)/shard_map/ppermute | solution.py:309
  61.5 11.2 %collective-permute-start.24 = (bf16[384,128]{1,0:T(8,128)(2,1)S(1)}, bf16[384,128]{1,0:T(8,128)(2,1)S(1)}, u32[]{:S(2)}, u32[]{:S(2)}) collective-permute-start(bf16[384,128]{1,0:T(8,128)(2,1)S(1)} %merge.1.a), channel_id=1, source_target_pairs={{0,1},{1,2},{2,3},{3,0},{4,5},{5,6},{6,7},{7,4},{8,9},{9,10},{10,1... | collective-permute-start | bytes 294920 | tf_op jit(solution)/shard_map/ppermute | solution.py:359
  62.9 9.8 %collective-permute-start.25 = (bf16[384,128]{1,0:T(8,128)(2,1)S(1)}, bf16[384,128]{1,0:T(8,128)(2,1)S(1)}, u32[]{:S(2)}, u32[]{:S(2)}) collective-permute-start(bf16[384,128]{1,0:T(8,128)(2,1)S(1)} %merge.1.a), channel_id=1, source_target_pairs={{0,2},{1,3},{2,0},{3,1},{4,6},{5,7},{6,4},{7,5},{8,10},{9,11},{10,... | collective-permute-start | bytes 294920 | tf_op jit(solution)/shard_map/ppermute | solution.py:359
  65.3 7.4 %collective-permute-start.26 = (bf16[384,128]{1,0:T(8,128)(2,1)S(1)}, bf16[384,128]{1,0:T(8,128)(2,1)S(1)}, u32[]{:S(2)}, u32[]{:S(2)}) collective-permute-start(bf16[384,128]{1,0:T(8,128)(2,1)S(1)} %merge.1.a), channel_id=1, source_target_pairs={{0,3},{1,0},{2,1},{3,2},{4,7},{5,4},{6,5},{7,6},{8,11},{9,8},{10,9... | collective-permute-start | bytes 294920 | tf_op jit(solution)/shard_map/ppermute | solution.py:359
  66.9 5.8 %collective-permute-start.28 = (bf16[128,256]{1,0:T(8,128)(2,1)S(1)}, bf16[128,256]{1,0:T(8,128)(2,1)S(1)}, u32[]{:S(2)}, u32[]{:S(2)}) collective-permute-start(bf16[128,256]{1,0:T(8,128)(2,1)S(1)} %get-tuple-element.24), channel_id=1, source_target_pairs={{0,2},{1,3},{2,0},{3,1},{4,6},{5,7},{6,4},{7,5},{8,10},{9,11},{10,... | collective-permute-start | bytes 196616 | tf_op jit(solution)/shard_map/ppermute | solution.py:309
  (10 other events, 36.7 us)
